TPU v7x, 32 devices: a whole 2x2x4 slice. The times are simulated.
32 devices in a mesh: ep: 8 (over z, x), tp: 4 (over y, core).
Axes of the slice: x: 2, y: 2, z: 4, core: 2. Of those that a mesh axis runs over, the one named last changes fastest.
Arguments:
- queries: bfloat16 [4096, 2048], P('ep', 'tp'), may hold values from -6 to 6
- keys: bfloat16 [4096, 2048], P('ep', 'tp'), may hold values from -12 to 12
- values: bfloat16 [4096, 2048], P('ep', 'tp'), may hold values from -8 to 8
- key_bias: bfloat16 [4096, 16], P('ep', 'tp'), may hold values from -16 to 0
- out_weight: bfloat16 [2048, 2048], P('tp'), may hold values from -0.1875 to 0.1875
- moe_input: bfloat16 [1024, 2048], P('ep'), may hold values from -6 to 6
- moe_gain: float32 [2048], replicated, may hold values from 0.1 to 1.9
- route_ids: int32 [1024, 2], P('ep'), may hold values from 0 to 7, all different within a row; in each aligned block of 128 rows (0 to 127, 128 to 255, ...) at most 48 rows name the same one
- route_scores: float32 [1024, 2], P('ep'), may hold values from 0.05 to 1
- shared_gate: bfloat16 [2048, 2048], P(None, 'tp'), may hold values from -0.125 to 0.125
- shared_up: bfloat16 [2048, 2048], P(None, 'tp'), may hold values from -0.125 to 0.125
- shared_down: bfloat16 [2048, 2048], P('tp'), may hold values from -0.1875 to 0.1875
- expert_gate: bfloat16 [8, 2048, 2048], P('ep', None, 'tp'), may hold values from -0.125 to 0.125
- expert_up: bfloat16 [8, 2048, 2048], P('ep', None, 'tp'), may hold values from -0.125 to 0.125
- expert_down: bfloat16 [8, 2048, 2048], P('ep', 'tp'), may hold values from -0.1875 to 0.1875
Outputs:
- mixed_tokens: bfloat16 [4096, 2048], P('ep', 'tp')
- expert_mix: bfloat16 [1024, 2048], P('ep', 'tp')
Inputs may be any that keep to these rules, and one draw needn't show every extreme that they name: `route_ids`: each row names 2 different experts. Among the 128 rows of one index of ep no expert is named by more than 48 rows, and in some such block one expert is named by exactly 48 rows.
All inputs are finite; a program needn't handle non-finite values.
Results may differ from a plain program's by a relative error of at most 0.019.
Values may be sent and summed in bfloat16 or wider, within the bound.
No kernel may reach another device: no remote copies, remote signals or barrier semaphores. Data moves between devices by JAX's collectives and lax.ppermute only.
A program may use at most 128 MiB of HBM per device.

v0:
```python
import jax
import jax.numpy as jnp
from jax import lax
from jax.sharding import PartitionSpec as P

SEQUENCE_COUNT = 1


EPS_NORM = 1e-06
ROUTED_SCALE = 2.5


def partner_2(array, axis, apart):
    return lax.ppermute(array, axis, [(i, i ^ 1 << apart) for i in range(lax.axis_size(axis))])


def absorb(state, query_heads, piece, visible):
    total, carried = state
    key_piece, value_piece, bias_piece = piece
    span = key_piece.shape[0]
    heads = query_heads.shape[1]
    key_heads = key_piece.reshape(span, heads, -1)
    value_heads = value_piece.reshape(span, heads, -1)
    scale = query_heads.shape[2] ** (-0.5)
    logit = (
        jnp.einsum("qhd,khd->hqk", query_heads, key_heads, preferred_element_type=jnp.float32)
        * scale
    )
    logit = logit + bias_piece.astype(jnp.float32).T[:, None, :]
    keep = jnp.where(visible[None], jax.nn.log_sigmoid(-logit), 0.0)
    stay = lax.cumsum(keep, axis=2, reverse=True) - keep + carried[:, :, None]
    weight = jnp.where(visible[None], jnp.exp(jax.nn.log_sigmoid(logit) + stay), 0.0).astype(
        jnp.bfloat16
    )
    total = total + jnp.einsum(
        "hqk,khd->qhd", weight, value_heads, preferred_element_type=jnp.float32
    )
    return (total, carried + jnp.sum(keep, axis=2))


def fresh_state(query_heads):
    return (
        jnp.zeros(query_heads.shape, jnp.float32),
        jnp.zeros((query_heads.shape[1], query_heads.shape[0]), jnp.float32),
    )


def diagonal(query_heads, piece, offset):
    count = query_heads.shape[0]
    span = piece[0].shape[0]
    key_pos = jnp.arange(span, dtype=jnp.int32)
    query_pos = offset + jnp.arange(count, dtype=jnp.int32)
    visible = key_pos[None, :] < query_pos[:, None]
    return absorb(fresh_state(query_heads), query_heads, piece, visible)


def body(
    queries,
    keys,
    values,
    key_bias,
    out_weight,
    moe_input,
    moe_gain,
    route_ids,
    route_scores,
    shared_gate,
    shared_up,
    shared_down,
    expert_gate,
    expert_up,
    expert_down,
):
    span = queries.shape[0]
    heads = key_bias.shape[1]
    query_heads = queries.reshape(span, heads, -1)
    ep_count = lax.axis_size("ep")
    seq_devices = ep_count // SEQUENCE_COUNT
    own_index = lax.axis_index("ep")
    place = own_index % seq_devices
    own_piece = (keys, values, key_bias)
    half = span // 2
    group_bits = seq_devices.bit_length() - 1

    def mirror(rows):
        for bit in range(group_bits):
            rows = partner_2(rows, "ep", bit)
        return rows

    whole = (
        lax.all_gather(own_piece[0], "ep", axis=0, tiled=True),
        lax.all_gather(own_piece[1], "ep", axis=0, tiled=True),
        lax.all_gather(own_piece[2], "ep", axis=0, tiled=True),
    )
    mirror_place = seq_devices - 1 - place
    mirror_index = own_index - place + mirror_place
    early_rows = query_heads[:half]
    late_rows = mirror(queries[half:]).reshape(half, heads, -1)
    partner = tuple(
        (lax.dynamic_slice_in_dim(member, mirror_index * span, span, 0) for member in whole)
    )
    half_visible = jnp.ones((half, span), jnp.bool_)

    def unchanged(inner):
        return inner

    def visit_both(turn, carry):
        early, late = carry
        early_source = jnp.maximum(own_index - turn, 0)
        late_source = jnp.maximum(mirror_index - turn, 0)
        early_piece = tuple(
            (lax.dynamic_slice_in_dim(member, early_source * span, span, 0) for member in whole)
        )
        late_piece = tuple(
            (lax.dynamic_slice_in_dim(member, late_source * span, span, 0) for member in whole)
        )

        def early_taken(inner):
            return absorb(inner, early_rows, early_piece, half_visible)

        def late_taken(inner):
            return absorb(inner, late_rows, late_piece, half_visible)

        early = lax.cond(place >= turn, early_taken, unchanged, early)
        late = lax.cond(mirror_place >= turn, late_taken, unchanged, late)
        return (early, late)

    early_state, late_state = lax.fori_loop(
        1,
        seq_devices,
        visit_both,
        (diagonal(early_rows, own_piece, 0), diagonal(late_rows, partner, half)),
    )
    early_out = early_state[0].astype(jnp.bfloat16).reshape(half, -1)
    late_out = mirror(late_state[0].astype(jnp.bfloat16).reshape(half, -1))
    heads_out = jnp.concatenate([early_out, late_out], axis=0)
    col_count = out_weight.shape[1] // lax.axis_size("tp")
    token_count = moe_input.shape[0]
    inputs = moe_input.astype(jnp.float32)
    normed = (
        inputs * lax.rsqrt(jnp.mean(inputs * inputs, axis=-1, keepdims=True) + EPS_NORM) * moe_gain
    ).astype(jnp.bfloat16)
    own_cols = lax.dynamic_slice_in_dim(normed, lax.axis_index("tp") * col_count, col_count, 1)
    shared_hidden = (
        jax.nn.silu(jnp.dot(normed, shared_gate, preferred_element_type=jnp.float32))
        * jnp.dot(normed, shared_up, preferred_element_type=jnp.float32)
    ).astype(jnp.bfloat16)
    local_experts = expert_gate.shape[0]
    expert_count = local_experts * ep_count
    topk = route_ids.shape[1]
    capacity = 3 * token_count * topk // (2 * expert_count)
    chosen = route_ids.reshape(-1)
    onehot = (chosen[:, None] == jnp.arange(expert_count, dtype=jnp.int32)[None, :]).astype(
        jnp.int32
    )
    place_in = jnp.sum((jnp.cumsum(onehot, axis=0) - onehot) * onehot, axis=1)
    slot_ids = chosen * capacity + place_in
    send_slots = expert_count * capacity
    matches = (
        slot_ids.reshape(token_count, topk)[None]
        == jnp.arange(send_slots, dtype=jnp.int32)[:, None, None]
    )
    dispatch = jnp.sum(matches.astype(jnp.bfloat16), axis=2)
    outgoing = jnp.dot(dispatch, own_cols, preferred_element_type=jnp.float32).astype(jnp.bfloat16)
    arrived = lax.all_to_all(outgoing, "ep", split_axis=0, concat_axis=0, tiled=True)
    piece = lax.all_gather(arrived, "tp", axis=1, tiled=True)
    width = piece.shape[1]
    grid = piece.reshape(ep_count, local_experts, capacity, width)
    gate_sum = jnp.einsum("secd,edf->secf", grid, expert_gate, preferred_element_type=jnp.float32)
    up_sum = jnp.einsum("secd,edf->secf", grid, expert_up, preferred_element_type=jnp.float32)
    expert_hidden = (jax.nn.silu(gate_sum) * up_sum).astype(jnp.bfloat16)
    routed = jnp.einsum(
        "secf,efd->dsec", expert_hidden, expert_down, preferred_element_type=jnp.float32
    ).reshape(lax.axis_size("tp") * col_count, -1)
    common = jnp.einsum("tf,fd->dt", shared_hidden, shared_down, preferred_element_type=jnp.float32)
    summed = lax.psum_scatter(
        jnp.concatenate(
            [
                jnp.einsum("rh,hd->dr", heads_out, out_weight, preferred_element_type=jnp.float32),
                jnp.concatenate([routed, common], axis=1),
            ],
            axis=1,
        ).astype(jnp.bfloat16),
        "tp",
        scatter_dimension=0,
        tiled=True,
    ).astype(jnp.float32)
    mixer_sum = summed[:, :span]
    expert_sum = summed[:, span:]
    mixed_tokens = mixer_sum.T.astype(jnp.bfloat16)
    routed_sum = expert_sum[:, :send_slots].astype(jnp.bfloat16)
    common_sum = expert_sum[:, send_slots:]
    returned = lax.all_to_all(routed_sum, "ep", split_axis=1, concat_axis=1, tiled=True)
    picked = (
        jnp.take(returned, slot_ids, axis=1)
        .astype(jnp.float32)
        .reshape(col_count, token_count, topk)
    )
    gates = route_scores / jnp.sum(route_scores, axis=-1, keepdims=True) * ROUTED_SCALE
    expert_mix = (common_sum + jnp.sum(picked * gates[None], axis=2)).T.astype(jnp.bfloat16)
    return (mixed_tokens, expert_mix)


def solution(mesh):
    return jax.shard_map(
        body,
        mesh=mesh,
        in_specs=(
            P("ep", "tp"),
            P("ep", "tp"),
            P("ep", "tp"),
            P("ep", "tp"),
            P("tp", None),
            P("ep", None),
            P(),
            P("ep", None),
            P("ep", None),
            P(None, "tp"),
            P(None, "tp"),
            P("tp", None),
            P("ep", None, "tp"),
            P("ep", None, "tp"),
            P("ep", "tp", None),
        ),
        out_specs=(P("ep", "tp"), P("ep", "tp")),
        check_vma=False,
    )
```

profile of v0, /device:TPU:0, one launch (start us, length us, event | category | flops | bytes accessed | tf_op | source)
XLA Modules:
  0.0 466.2 jit_solution(12606968122326971985)
XLA Ops:
  37.2 10.2 %fusion.104 = f32[4,256,4,128]{1,2,3,0:T(4,128)S(1)} fusion(f32[4,256,4,128]{1,2,3,0:T(4,128)} %copy.115), kind=kOutput, calls=%fused_computation.169 | output fusion | flops 66584576 | bytes 4194304 | tf_op jit(solution)/shard_map/reduce-window.4
  62.5 6.4 %convolution_bitcast_fusion.3 = f32[256,4,128]{2,0,1:T(8,128)} fusion(f32[4,256,512]{2,1,0:T(8,128)} %reduce_window_sum.66, f32[4,256,512]{2,1,0:T(8,128)} %copy-done.10, pred[256,512]{1,0:T(8,128)(4,1)S(1)} %iota_compare_fusion.1, u8[256,512]{1,0:T(8,128)(4,1)S(1)} %get-tuple-element.558, bf16[512,512]{1,0:T(8,128)(2,1)} %param.23), kind=kOutput, calls=%fused_computation.104 | convolution fusion | flops 146276352 | bytes 5505024 | tf_op jit(solution)/shard_map/hqk,khd->qhd/dot_general | solution.py:35
  69.4 31.9 %all_gather.14 = bf16[4096,4]{0,1:T(4,128)(2,1)S(1)} all-gather(bf16[512,4]{0,1:T(4,128)(2,1)S(1)} %copy-done.20), channel_id=1, replica_groups=mesh['ep'=8,'tp'=4] {'ep'}, dimensions={0}, use_global_device_ids=true | all-gather | bytes 36864 | tf_op jit(solution)/shard_map/all_gather | solution.py:93
  106.6 10.7 %collective-permute-done.1 = bf16[256,512]{0,1:T(8,128)(2,1)} collective-permute-done((bf16[256,512]{0,1:T(8,128)(2,1)}, bf16[256,512]{0,1:T(8,128)(2,1)}, u32[]{:S(2)}, u32[]{:S(2)}) %collective-permute-start.1) | collective-permute-done | bytes 262176 | tf_op jit(solution)/shard_map/ppermute | solution.py:14
  118.5 15.5 %collective-permute-done.2 = bf16[256,512]{0,1:T(8,128)(2,1)S(1)} collective-permute-done((bf16[256,512]{0,1:T(8,128)(2,1)}, bf16[256,512]{0,1:T(8,128)(2,1)S(1)}, u32[]{:S(2)}, u32[]{:S(2)}) %collective-permute-start.2) | collective-permute-done | bytes 262176 | tf_op jit(solution)/shard_map/ppermute | solution.py:14
  146.8 10.2 %fusion.105 = f32[4,256,4,128]{1,2,3,0:T(4,128)S(1)} fusion(f32[4,256,4,128]{1,2,3,0:T(4,128)} %copy.124), kind=kOutput, calls=%fused_computation.170 | output fusion | flops 66584576 | bytes 4194304 | tf_op jit(solution)/shard_map/reduce-window.6
  169.2 10.9 %all-gather.4.cloned.1.call-done = bf16[4096,512]{0,1:T(8,128)(2,1)} async-done(((bf16[512,512]{0,1:T(8,128)(2,1)}), bf16[4096,512]{0,1:T(8,128)(2,1)}) %all-gather.4.cloned.1.call-update) | async-done | bytes 4194320 | tf_op jit(solution)/shard_map/all_gather | solution.py:92
  186.9 171.1 %while.19 = (s32[]{:T(128)}, f32[256,4,128]{2,0,1:T(8,128)}, f32[4,256]{1,0:T(4,128)S(1)}, f32[256,4,128]{2,0,1:T(8,128)S(1)}, f32[4,256]{1,0:T(4,128)S(1)}, /*i...) while((s32[]{:T(128)}, f32[256,4,128]{2,0,1:T(8,128)}, ...), condition=%wide.region_17.18_spmd, body=%wide.region_6.17_spmd.sunk | while | flops 703893504 | bytes 94184160 | solution.py:128
  189.3 23.3 %conditional.5 = ((f32[256,4,128]{2,0,1:T(8,128)S(1)}, f32[4,256]{1,0:T(4,128)S(1)})) conditional(s32[]{:T(128)} %convert_element_type.140, (f32[256,4,128]{2,0,1:T(8,128)S(1)}, f32[4,256]{1,0:T(4,128)S(1)}) %tuple.82, (s32[]{:T(128)}, s32[]{:T(128)}, bf16[4096,512]{0,1:T(8,128)(2,1)}, bf16[256,4,128]{2,0,1:T(8,128)(2,1)}, ...), branch_computations={%region_12.12_spmd, %region_13.16_spmd} | conditional | flops 351946752 | bytes 45519040 | solution.py:125
  194.2 9.6 %fusion.23 = f32[4,256,4,128]{1,2,3,0:T(4,128)S(1)} fusion(f32[4,256,4,128]{1,3,2,0:T(8,128)S(1)} %bitcast.233), kind=kOutput, calls=%fused_computation.44 | output fusion | flops 66584576 | bytes 4194304 | tf_op jit(solution)/shard_map/reduce-window.20
  212.7 23.3 %conditional.5 = ((f32[256,4,128]{2,0,1:T(8,128)S(1)}, f32[4,256]{1,0:T(4,128)S(1)})) conditional(s32[]{:T(128)} %convert_element_type.140, (f32[256,4,128]{2,0,1:T(8,128)S(1)}, f32[4,256]{1,0:T(4,128)S(1)}) %tuple.82, (s32[]{:T(128)}, s32[]{:T(128)}, bf16[4096,512]{0,1:T(8,128)(2,1)}, bf16[256,4,128]{2,0,1:T(8,128)(2,1)}, ...), branch_computations={%region_12.12_spmd, %region_13.16_spmd} | conditional | flops 351946752 | bytes 45519040 | solution.py:125
  217.6 9.6 %fusion.23 = f32[4,256,4,128]{1,2,3,0:T(4,128)S(1)} fusion(f32[4,256,4,128]{1,3,2,0:T(8,128)S(1)} %bitcast.233), kind=kOutput, calls=%fused_computation.44 | output fusion | flops 66584576 | bytes 4194304 | tf_op jit(solution)/shard_map/reduce-window.20
  236.0 23.3 %conditional.5 = ((f32[256,4,128]{2,0,1:T(8,128)S(1)}, f32[4,256]{1,0:T(4,128)S(1)})) conditional(s32[]{:T(128)} %convert_element_type.140, (f32[256,4,128]{2,0,1:T(8,128)S(1)}, f32[4,256]{1,0:T(4,128)S(1)}) %tuple.82, (s32[]{:T(128)}, s32[]{:T(128)}, bf16[4096,512]{0,1:T(8,128)(2,1)}, bf16[256,4,128]{2,0,1:T(8,128)(2,1)}, ...), branch_computations={%region_12.12_spmd, %region_13.16_spmd} | conditional | flops 351946752 | bytes 45519040 | solution.py:125
  241.0 9.6 %fusion.23 = f32[4,256,4,128]{1,2,3,0:T(4,128)S(1)} fusion(f32[4,256,4,128]{1,3,2,0:T(8,128)S(1)} %bitcast.233), kind=kOutput, calls=%fused_computation.44 | output fusion | flops 66584576 | bytes 4194304 | tf_op jit(solution)/shard_map/reduce-window.20
  259.4 23.3 %conditional.5 = ((f32[256,4,128]{2,0,1:T(8,128)S(1)}, f32[4,256]{1,0:T(4,128)S(1)})) conditional(s32[]{:T(128)} %convert_element_type.140, (f32[256,4,128]{2,0,1:T(8,128)S(1)}, f32[4,256]{1,0:T(4,128)S(1)}) %tuple.82, (s32[]{:T(128)}, s32[]{:T(128)}, bf16[4096,512]{0,1:T(8,128)(2,1)}, bf16[256,4,128]{2,0,1:T(8,128)(2,1)}, ...), branch_computations={%region_12.12_spmd, %region_13.16_spmd} | conditional | flops 351946752 | bytes 45519040 | solution.py:125
  264.4 9.6 %fusion.23 = f32[4,256,4,128]{1,2,3,0:T(4,128)S(1)} fusion(f32[4,256,4,128]{1,3,2,0:T(8,128)S(1)} %bitcast.233), kind=kOutput, calls=%fused_computation.44 | output fusion | flops 66584576 | bytes 4194304 | tf_op jit(solution)/shard_map/reduce-window.20
  282.8 23.3 %conditional.5 = ((f32[256,4,128]{2,0,1:T(8,128)S(1)}, f32[4,256]{1,0:T(4,128)S(1)})) conditional(s32[]{:T(128)} %convert_element_type.140, (f32[256,4,128]{2,0,1:T(8,128)S(1)}, f32[4,256]{1,0:T(4,128)S(1)}) %tuple.82, (s32[]{:T(128)}, s32[]{:T(128)}, bf16[4096,512]{0,1:T(8,128)(2,1)}, bf16[256,4,128]{2,0,1:T(8,128)(2,1)}, ...), branch_computations={%region_12.12_spmd, %region_13.16_spmd} | conditional | flops 351946752 | bytes 45519040 | solution.py:125
  287.7 9.6 %fusion.23 = f32[4,256,4,128]{1,2,3,0:T(4,128)S(1)} fusion(f32[4,256,4,128]{1,3,2,0:T(8,128)S(1)} %bitcast.233), kind=kOutput, calls=%fused_computation.44 | output fusion | flops 66584576 | bytes 4194304 | tf_op jit(solution)/shard_map/reduce-window.20
  306.2 23.3 %conditional.5 = ((f32[256,4,128]{2,0,1:T(8,128)S(1)}, f32[4,256]{1,0:T(4,128)S(1)})) conditional(s32[]{:T(128)} %convert_element_type.140, (f32[256,4,128]{2,0,1:T(8,128)S(1)}, f32[4,256]{1,0:T(4,128)S(1)}) %tuple.82, (s32[]{:T(128)}, s32[]{:T(128)}, bf16[4096,512]{0,1:T(8,128)(2,1)}, bf16[256,4,128]{2,0,1:T(8,128)(2,1)}, ...), branch_computations={%region_12.12_spmd, %region_13.16_spmd} | conditional | flops 351946752 | bytes 45519040 | solution.py:125
  311.1 9.6 %fusion.23 = f32[4,256,4,128]{1,2,3,0:T(4,128)S(1)} fusion(f32[4,256,4,128]{1,3,2,0:T(8,128)S(1)} %bitcast.233), kind=kOutput, calls=%fused_computation.44 | output fusion | flops 66584576 | bytes 4194304 | tf_op jit(solution)/shard_map/reduce-window.20
  329.6 23.3 %conditional.5 = ((f32[256,4,128]{2,0,1:T(8,128)S(1)}, f32[4,256]{1,0:T(4,128)S(1)})) conditional(s32[]{:T(128)} %convert_element_type.140, (f32[256,4,128]{2,0,1:T(8,128)S(1)}, f32[4,256]{1,0:T(4,128)S(1)}) %tuple.82, (s32[]{:T(128)}, s32[]{:T(128)}, bf16[4096,512]{0,1:T(8,128)(2,1)}, bf16[256,4,128]{2,0,1:T(8,128)(2,1)}, ...), branch_computations={%region_12.12_spmd, %region_13.16_spmd} | conditional | flops 351946752 | bytes 45519040 | solution.py:125
  334.5 9.6 %fusion.23 = f32[4,256,4,128]{1,2,3,0:T(4,128)S(1)} fusion(f32[4,256,4,128]{1,3,2,0:T(8,128)S(1)} %bitcast.233), kind=kOutput, calls=%fused_computation.44 | output fusion | flops 66584576 | bytes 4194304 | tf_op jit(solution)/shard_map/reduce-window.20
  374.3 5.8 %collective-permute-start.5 = (bf16[256,512]{0,1:T(8,128)(2,1)S(1)}, bf16[256,512]{0,1:T(8,128)(2,1)S(1)}, u32[]{:S(2)}, u32[]{:S(2)}) collective-permute-start(bf16[256,512]{0,1:T(8,128)(2,1)S(1)} %collective-permute-done.4), channel_id=1, source_target_pairs={{0,16},{4,20},{8,24},{12,28},{16,0},{20,4},{24,8},{28,12},{1,17},{... | collective-permute-start | bytes 786440 | tf_op jit(solution)/shard_map/ppermute | solution.py:14
  392.4 44.3 %reduce-scatter.2.cloned.1.call-done = bf16[512,1024]{0,1:T(8,128)(2,1)} async-done(((bf16[2048,1024]{0,1:T(8,128)(2,1)}), bf16[512,1024]{0,1:T(8,128)(2,1)}) %reduce-scatter.2.cloned.1.call-update) | async-done | bytes 1048592 | tf_op jit(solution)/shard_map/reduce_scatter | solution.py:176
  (269 shorter events, 230.3 us)
Async XLA Ops:
  7.2 380.1 %copy-start = (bf16[512,2048]{1,0:T(8,128)(2,1)S(1)}, bf16[512,2048]{1,0:T(8,128)(2,1)}, u32[]{:S(2)}) copy-start(bf16[512,2048]{1,0:T(8,128)(2,1)} %param.25) | copy-start | bytes 6291460
  7.2 127.7 %all-gather.6.cloned.1.call-start = ((), (), s32[]{:S(2)}) async-start(), calls=%async_computation.4 | async-start | bytes 4718592 | tf_op jit(solution)/shard_map/all_gather | solution.py:91
  9.4 7.1 %copy-start.21 = (s32[128,2]{0,1:T(2,128)S(1)}, s32[128,2]{0,1:T(2,128)}, u32[]{:S(2)}) copy-start(s32[128,2]{0,1:T(2,128)} %param.28) | copy-start | bytes 3076
  9.4 9.3 %copy-start.12 = (bf16[128,2048]{1,0:T(8,128)(2,1)S(1)}, bf16[128,2048]{1,0:T(8,128)(2,1)}, u32[]{:S(2)}) copy-start(bf16[128,2048]{1,0:T(8,128)(2,1)} %param.26) | copy-start | bytes 1572868
  9.4 9.5 %copy-start.23 = (f32[2048]{0:T(1024)S(1)}, f32[2048]{0:T(1024)}, u32[]{:S(2)}) copy-start(f32[2048]{0:T(1024)} %param.27) | copy-start | bytes 24580
  9.4 170.7 %all-gather.4.cloned.1.call-start = ((), (), s32[]{:S(2)}) async-start(), calls=%async_computation.3 | async-start | bytes 4718592 | tf_op jit(solution)/shard_map/all_gather | solution.py:92
  13.5 11.7 %copy-start.20 = (bf16[512,4]{0,1:T(4,128)(2,1)S(1)}, bf16[512,4]{0,1:T(4,128)(2,1)}, u32[]{:S(2)}) copy-start(bf16[512,4]{0,1:T(4,128)(2,1)} %param.24) | copy-start | bytes 12292
  13.5 89.0 %collective-permute-start = (bf16[256,512]{0,1:T(8,128)(2,1)}, bf16[256,512]{0,1:T(8,128)(2,1)}, u32[]{:S(2)}, u32[]{:S(2)}) collective-permute-start(bf16[256,512]{0,1:T(8,128)(2,1)} %copy.148), channel_id=1, source_target_pairs={{0,4},{4,0},{8,12},{12,8},{16,20},{20,16},{24,28},{28,24},{1,5},{5... | collective-permute-start | bytes 786440 | tf_op jit(solution)/shard_map/ppermute | solution.py:14
  17.9 9.2 %copy-start.22 = (s32[256]{0:T(256)}, s32[256]{0:T(256)S(1)}, u32[]{:S(2)}) copy-start(s32[256]{0:T(256)S(1)} %fusion.90) | copy-start | bytes 3076
  20.2 97.3 %all-to-all-start = ((bf16[8,48,512]{2,1,0:T(8,128)(2,1)}), bf16[8,48,512]{2,1,0:T(8,128)(2,1)S(1)}, u32[]{:S(2)}, u32[]{:S(2)}) async-start(bf16[8,48,512]{2,1,0:T(8,128)(2,1)} %bitcast.32), calls=%async_computation | async-start | bytes 786432 | tf_op jit(solution)/shard_map/all_to_all | solution.py:165
  25.0 336.6 %all-gather.8.cloned.1.call-start = ((), (), s32[]{:S(2)}) async-start(), calls=%async_computation.5 | async-start | bytes 1966080 | tf_op jit(solution)/shard_map/all_gather | solution.py:166
  62.5 6.4 %copy-start.11 = (bf16[2048,512]{1,0:T(8,128)(2,1)S(1)}, bf16[2048,512]{1,0:T(8,128)(2,1)}, u32[]{:S(2)}) copy-start(bf16[2048,512]{1,0:T(8,128)(2,1)} %param.30) | copy-start | bytes 6291460
  102.5 14.8 %collective-permute-start.1 = (bf16[256,512]{0,1:T(8,128)(2,1)}, bf16[256,512]{0,1:T(8,128)(2,1)}, u32[]{:S(2)}, u32[]{:S(2)}) collective-permute-start(bf16[256,512]{0,1:T(8,128)(2,1)} %collective-permute-done), channel_id=1, source_target_pairs={{0,8},{4,12},{8,0},{12,4},{16,24},{20,28},{24,16},{28,20},{1,9},{5... | collective-permute-start | bytes 786440 | tf_op jit(solution)/shard_map/ppermute | solution.py:14
  106.6 29.3 %copy-start.24 = (f32[4,512]{1,0:T(4,128)S(1)}, f32[4,512]{1,0:T(4,128)}, u32[]{:S(2)}) copy-start(f32[4,512]{1,0:T(4,128)} %convert_bitcast_fusion.2) | copy-start | bytes 24580
  117.3 16.7 %collective-permute-start.2 = (bf16[256,512]{0,1:T(8,128)(2,1)}, bf16[256,512]{0,1:T(8,128)(2,1)S(1)}, u32[]{:S(2)}, u32[]{:S(2)}) collective-permute-start(bf16[256,512]{0,1:T(8,128)(2,1)} %collective-permute-done.1), channel_id=1, source_target_pairs={{0,16},{4,20},{8,24},{12,28},{16,0},{20,4},{24,8},{28,12},{1,17},{... | collective-permute-start | bytes 786440 | tf_op jit(solution)/shard_map/ppermute | solution.py:14
  118.3 318.4 %reduce-scatter.2.cloned.1.call-start = ((), (), s32[]{:S(2)}) async-start(), calls=%async_computation.6 | async-start | bytes 5242880 | tf_op jit(solution)/shard_map/reduce_scatter | solution.py:176
  358.1 7.8 %collective-permute-start.3 = (bf16[256,512]{0,1:T(8,128)(2,1)S(1)}, bf16[256,512]{0,1:T(8,128)(2,1)S(1)}, u32[]{:S(2)}, u32[]{:S(2)}) collective-permute-start(bf16[256,512]{0,1:T(8,128)(2,1)S(1)} %bitcast.244), channel_id=1, source_target_pairs={{0,4},{4,0},{8,12},{12,8},{16,20},{20,16},{24,28},{28,24},{1,5},{5... | collective-permute-start | bytes 786440 | tf_op jit(solution)/shard_map/ppermute | solution.py:14
  361.6 6.8 %copy-start.26 = (bf16[1,2048,512]{2,1,0:T(8,128)(2,1)S(1)}, bf16[1,2048,512]{2,1,0:T(8,128)(2,1)}, u32[]{:S(2)}) copy-start(bf16[1,2048,512]{2,1,0:T(8,128)(2,1)} %param.34) | copy-start | bytes 6291460
  361.6 6.8 %copy-start.28 = (bf16[384,2048]{1,0:T(8,128)(2,1)S(1)}, bf16[384,2048]{1,0:T(8,128)(2,1)}, u32[]{:S(2)}) copy-start(bf16[384,2048]{1,0:T(8,128)(2,1)} %all-gather.8.cloned.1.call-done) | copy-start | bytes 4718596
  364.8 15.3 %copy-start.27 = (bf16[1,512,2048]{2,1,0:T(8,128)(2,1)S(1)}, bf16[1,512,2048]{2,1,0:T(8,128)(2,1)}, u32[]{:S(2)}) copy-start(bf16[1,512,2048]{2,1,0:T(8,128)(2,1)} %param.35) | copy-start | bytes 6291460
  366.0 8.4 %collective-permute-start.4 = (bf16[256,512]{0,1:T(8,128)(2,1)S(1)}, bf16[256,512]{0,1:T(8,128)(2,1)S(1)}, u32[]{:S(2)}, u32[]{:S(2)}) collective-permute-start(bf16[256,512]{0,1:T(8,128)(2,1)S(1)} %collective-permute-done.3), channel_id=1, source_target_pairs={{0,8},{4,12},{8,0},{12,4},{16,24},{20,28},{24,16},{28,20},{1,9},{5... | collective-permute-start | bytes 786440 | tf_op jit(solution)/shard_map/ppermute | solution.py:14
  374.3 13.0 %collective-permute-start.5 = (bf16[256,512]{0,1:T(8,128)(2,1)S(1)}, bf16[256,512]{0,1:T(8,128)(2,1)S(1)}, u32[]{:S(2)}, u32[]{:S(2)}) collective-permute-start(bf16[256,512]{0,1:T(8,128)(2,1)S(1)} %collective-permute-done.4), channel_id=1, source_target_pairs={{0,16},{4,20},{8,24},{12,28},{16,0},{20,4},{24,8},{28,12},{1,17},{... | collective-permute-start | bytes 786440 | tf_op jit(solution)/shard_map/ppermute | solution.py:14
  436.7 13.2 %copy-start.16 = (bf16[512,1024]{0,1:T(8,128)(2,1)S(1)}, bf16[512,1024]{0,1:T(8,128)(2,1)}, u32[]{:S(2)}) copy-start(bf16[512,1024]{0,1:T(8,128)(2,1)} %reduce-scatter.2.cloned.1.call-done) | copy-start | bytes 3145732
  438.6 17.1 %all-to-all-start.1 = ((bf16[512,8,48]{0,2,1:T(8,128)(2,1)}), bf16[512,8,48]{0,2,1:T(8,128)(2,1)S(1)}, u32[]{:S(2)}, u32[]{:S(2)}) async-start(bf16[512,8,48]{0,2,1:T(8,128)(2,1)} %bitcast.52), calls=%async_computation.2 | async-start | bytes 786432 | tf_op jit(solution)/shard_map/all_to_all | solution.py:193
  (31 other events, 53.4 us)
Sparse Core Ops, SparseCore 0:
  10.0 86.2 all-gather.5
  98.3 81.8 all-gather.3
  181.8 17.8 all-gather.7
  391.2 45.4 reduce-scatter.1
where the time goes:
time: 472 us; the launch traced here: 466 us
  other arithmetic  149 us (32%)
  waiting for transfers between devices  97.3 us (21%)
  local copies, waits for them, and re-layouts  85 us (18%)
  matrix products  54.8 us (12%)
  blocking collectives  31.9 us (7%)
  starting transfers between devices  25.3 us (5%)
  between operations  14.3 us (3%)
  loops' own time  8.35 us (2%)
    another operation x20, other arithmetic  90.1 us
    reduce_scatter x1, waiting for transfers between devices, body(): lax.psum_scatter(jnp.concatenate([jnp.einsum('rh,hd->dr', heads_out, out_...  44.3 us
    ppermute x6, waiting for transfers between devices, partner_2(): lax.ppermute(array, axis, [(i, i ^ 1 << apart) for i in range(lax.axis_si...  37 us
    all_gather x1, blocking collectives, body(): lax.all_gather(own_piece[2], 'ep', axis=0, tiled=True)  31.9 us
    dot_general x9, matrix products, absorb(): jnp.einsum('qhd,khd->hqk', query_heads, key_heads, preferred_element_type...  25.4 us
    convert_element_type x7, other arithmetic, absorb(): jnp.where(visible[None], jnp.exp(jax.nn.log_sigmoid(logit) + stay), 0.0)  22.5 us
    another operation x9, other arithmetic, absorb(): stay = lax.cumsum(keep, axis=2, reverse=True) - keep + carried[:, :, None]  20.3 us
    another operation x11, local copies, waits for them, and re-layouts, absorb(): stay = lax.cumsum(keep, axis=2, reverse=True) - keep + carried[:, :, None]  17.9 us
  transfers between devices with their start and end apart: 12, of which 8 were waited for; matrix products, arithmetic and copies ran while one was open for 55% of the time, Pallas kernels for 0%

commit v1 on v0

v1 whole, which is shorter than its diff:
```python
import functools

import jax
import jax.numpy as jnp
from jax import lax
from jax.experimental import pallas as pl
from jax.experimental.pallas import tpu as pltpu
from jax.sharding import PartitionSpec as P

SEQUENCE_COUNT = 1


EPS_NORM = 1e-06
ROUTED_SCALE = 2.5
LOG2E = 1.4426950408889634


def partner_2(array, axis, apart):
    return lax.ppermute(array, axis, [(i, i ^ 1 << apart) for i in range(lax.axis_size(axis))])


def swap(array, axis, mask):
    return lax.ppermute(array, axis, [(i, i ^ mask) for i in range(lax.axis_size(axis))])


def stick_kernel(scale, half_ref, own_ref, other_ref, q_ref, out_ref, k_s, v_s, b_s, tri_s, acc_s, carry_s):
    blocks, rows, width = q_ref.shape
    bias_rows = rows // width
    mine = half_ref[0]
    for which, ref in ((mine, own_ref), (1 - mine, other_ref)):
        k_s[which] = ref[:, :rows]
        v_s[which] = ref[:, rows : 2 * rows]
        for block in range(blocks):
            lanes = [
                ref[block, pl.ds(2 * rows + r, 1), :].astype(jnp.float32) * LOG2E
                for r in range(bias_rows)
            ]
            b_s[which, block] = jnp.concatenate(lanes, axis=1)
    later = lax.broadcasted_iota(jnp.int32, (rows, rows + width), 0)
    column = lax.broadcasted_iota(jnp.int32, (rows, rows + width), 1)
    tri_s[...] = jnp.where((later > column) | (column >= rows), 1.0, 0.0).astype(jnp.bfloat16)

    def step(query, source, visible_of):
        for part in (1, 0):
            logit = lax.dot_general(
                query,
                k_s[part, source],
                (((1,), (1,)), ((), ())),
                preferred_element_type=jnp.float32,
            )
            logit = logit * scale + b_s[part, source]
            soft = jnp.maximum(logit, jnp.log2(1.0 + jnp.exp2(jnp.minimum(logit, 64.0))))
            if visible_of is not None:
                visible = visible_of(part)
                soft = jnp.where(visible, soft, 0.0)
            sums = jnp.dot(soft.astype(jnp.bfloat16), tri_s[...], preferred_element_type=jnp.float32)
            carry = carry_s[...]
            carry_s[...] = carry + sums[:, rows:]
            wide = jnp.concatenate([carry] * bias_rows, axis=1)
            weight = jnp.exp2((logit - soft) - (sums[:, :rows] + wide))
            if visible_of is not None:
                weight = jnp.where(visible, weight, 0.0)
            acc_s[...] += jnp.dot(
                weight.astype(jnp.bfloat16), v_s[part, source], preferred_element_type=jnp.float32
            )

    def one_block(block, _):
        query = q_ref[block]
        acc_s[...] = jnp.zeros_like(acc_s)
        carry_s[...] = jnp.zeros_like(carry_s)
        row = lax.broadcasted_iota(jnp.int32, (rows, rows), 0) + mine * rows
        key = lax.broadcasted_iota(jnp.int32, (rows, rows), 1)
        step(query, block, lambda part: key + part * rows < row)

        def earlier(turn, _):
            step(query, block - 1 - turn, None)
            return 0

        lax.fori_loop(0, block, earlier, 0)
        out_ref[block] = acc_s[...].astype(out_ref.dtype)
        return 0

    lax.fori_loop(0, blocks, one_block, 0)


def stick(half, own, other, query):
    blocks, rows, width = query.shape
    pairs = blocks * (blocks + 1) * rows * rows
    vmem = pl.BlockSpec(memory_space=pltpu.VMEM)
    return pl.pallas_call(
        functools.partial(stick_kernel, width**-0.5 * LOG2E),
        out_shape=jax.ShapeDtypeStruct(query.shape, jnp.bfloat16),
        in_specs=[pl.BlockSpec(memory_space=pltpu.SMEM), vmem, vmem, vmem],
        out_specs=vmem,
        scratch_shapes=[
            pltpu.VMEM((2, blocks, rows, width), jnp.bfloat16),
            pltpu.VMEM((2, blocks, rows, width), jnp.bfloat16),
            pltpu.VMEM((2, blocks, 1, rows), jnp.float32),
            pltpu.VMEM((rows, rows + width), jnp.bfloat16),
            pltpu.VMEM((rows, width), jnp.float32),
            pltpu.VMEM((rows, width), jnp.float32),
        ],
        cost_estimate=pl.CostEstimate(
            flops=2 * pairs * (rows + 3 * width),
            bytes_accessed=12 * blocks * rows * width,
            transcendentals=3 * pairs,
        ),
        name="stick",
    )(half, own, other, query)


def by_group(core, own, other, axis=0):
    return jnp.where(
        core == 0, jnp.concatenate([own, other], axis), jnp.concatenate([other, own], axis)
    )


def head_attention(queries, keys, values, key_bias, out_weight):
    span, width = queries.shape
    heads = key_bias.shape[1]
    depth = width // heads
    half = span // 2
    ep_count = lax.axis_size("ep")
    tp_count = lax.axis_size("tp")
    tp_index = lax.axis_index("tp")
    core = tp_index % 2
    pad = 16 - half // depth % 16

    def split(array):
        return (
            lax.dynamic_slice_in_dim(array, core * half, half, 0),
            lax.dynamic_slice_in_dim(array, (1 - core) * half, half, 0),
        )

    def per_head(array):
        return array.reshape(half, heads, depth).transpose(1, 0, 2)

    own, away = zip(*[split(array) for array in (keys, values, queries, key_bias)])
    got = [swap(array, "tp", 1) for array in away]

    def bias_rows(array):
        rows = array.T.reshape(heads, half // depth, depth)
        return jnp.pad(rows, ((0, 0), (0, pad), (0, 0)))

    def key_message(key_rows, value_rows, bias):
        return jnp.concatenate([per_head(key_rows), per_head(value_rows), bias_rows(bias)], axis=1)

    key_parts = by_group(
        core, key_message(own[0], own[1], own[3]), key_message(got[0], got[1], got[3])
    )
    query_parts = by_group(core, per_head(own[2]), per_head(got[2]))
    own_keys = lax.all_to_all(key_parts, "ep", split_axis=0, concat_axis=0, tiled=True)
    query_rows = lax.all_to_all(query_parts, "ep", split_axis=0, concat_axis=0, tiled=True)
    other_keys = swap(own_keys, "tp", 1)
    out = stick(core.reshape(1), own_keys, other_keys, query_rows)
    back = lax.all_to_all(out, "ep", split_axis=0, concat_axis=0, tiled=True)
    other_weight = swap(out_weight, "tp", 1)

    def project(group, weight):
        rows = lax.dynamic_slice_in_dim(back, group * heads, heads, 0)
        return jnp.dot(
            rows.transpose(1, 0, 2).reshape(half, width), weight, preferred_element_type=jnp.float32
        )

    partial = (project(core, out_weight) + project(1 - core, other_weight)).astype(jnp.bfloat16)
    cols = partial.shape[1] // tp_count

    def columns(index):
        return lax.dynamic_slice_in_dim(partial, index * cols, cols, 1)

    same = columns(tp_index).astype(jnp.float32)
    cross = jnp.zeros_like(same)
    for mask in range(1, tp_count):
        piece = swap(columns(tp_index ^ mask), "tp", mask).astype(jnp.float32)
        if mask % 2:
            cross = cross + piece
        else:
            same = same + piece
    return by_group(core, same.astype(jnp.bfloat16), cross.astype(jnp.bfloat16))


def absorb(state, query_heads, piece, visible):
    total, carried = state
    key_piece, value_piece, bias_piece = piece
    span = key_piece.shape[0]
    heads = query_heads.shape[1]
    key_heads = key_piece.reshape(span, heads, -1)
    value_heads = value_piece.reshape(span, heads, -1)
    scale = query_heads.shape[2] ** (-0.5)
    logit = (
        jnp.einsum("qhd,khd->hqk", query_heads, key_heads, preferred_element_type=jnp.float32)
        * scale
    )
    logit = logit + bias_piece.astype(jnp.float32).T[:, None, :]
    keep = jnp.where(visible[None], jax.nn.log_sigmoid(-logit), 0.0)
    stay = lax.cumsum(keep, axis=2, reverse=True) - keep + carried[:, :, None]
    weight = jnp.where(visible[None], jnp.exp(jax.nn.log_sigmoid(logit) + stay), 0.0).astype(
        jnp.bfloat16
    )
    total = total + jnp.einsum(
        "hqk,khd->qhd", weight, value_heads, preferred_element_type=jnp.float32
    )
    return (total, carried + jnp.sum(keep, axis=2))


def fresh_state(query_heads):
    return (
        jnp.zeros(query_heads.shape, jnp.float32),
        jnp.zeros((query_heads.shape[1], query_heads.shape[0]), jnp.float32),
    )


def diagonal(query_heads, piece, offset):
    count = query_heads.shape[0]
    span = piece[0].shape[0]
    key_pos = jnp.arange(span, dtype=jnp.int32)
    query_pos = offset + jnp.arange(count, dtype=jnp.int32)
    visible = key_pos[None, :] < query_pos[:, None]
    return absorb(fresh_state(query_heads), query_heads, piece, visible)


def row_attention(queries, keys, values, key_bias, out_weight):
    span = queries.shape[0]
    heads = key_bias.shape[1]
    query_heads = queries.reshape(span, heads, -1)
    ep_count = lax.axis_size("ep")
    seq_devices = ep_count // SEQUENCE_COUNT
    own_index = lax.axis_index("ep")
    place = own_index % seq_devices
    own_piece = (keys, values, key_bias)
    half = span // 2
    group_bits = seq_devices.bit_length() - 1

    def mirror(rows):
        for bit in range(group_bits):
            rows = partner_2(rows, "ep", bit)
        return rows

    whole = (
        lax.all_gather(own_piece[0], "ep", axis=0, tiled=True),
        lax.all_gather(own_piece[1], "ep", axis=0, tiled=True),
        lax.all_gather(own_piece[2], "ep", axis=0, tiled=True),
    )
    mirror_place = seq_devices - 1 - place
    mirror_index = own_index - place + mirror_place
    early_rows = query_heads[:half]
    late_rows = mirror(queries[half:]).reshape(half, heads, -1)
    partner = tuple(
        (lax.dynamic_slice_in_dim(member, mirror_index * span, span, 0) for member in whole)
    )
    half_visible = jnp.ones((half, span), jnp.bool_)

    def unchanged(inner):
        return inner

    def visit_both(turn, carry):
        early, late = carry
        early_source = jnp.maximum(own_index - turn, 0)
        late_source = jnp.maximum(mirror_index - turn, 0)
        early_piece = tuple(
            (lax.dynamic_slice_in_dim(member, early_source * span, span, 0) for member in whole)
        )
        late_piece = tuple(
            (lax.dynamic_slice_in_dim(member, late_source * span, span, 0) for member in whole)
        )

        def early_taken(inner):
            return absorb(inner, early_rows, early_piece, half_visible)

        def late_taken(inner):
            return absorb(inner, late_rows, late_piece, half_visible)

        early = lax.cond(place >= turn, early_taken, unchanged, early)
        late = lax.cond(mirror_place >= turn, late_taken, unchanged, late)
        return (early, late)

    early_state, late_state = lax.fori_loop(
        1,
        seq_devices,
        visit_both,
        (diagonal(early_rows, own_piece, 0), diagonal(late_rows, partner, half)),
    )
    early_out = early_state[0].astype(jnp.bfloat16).reshape(half, -1)
    late_out = mirror(late_state[0].astype(jnp.bfloat16).reshape(half, -1))
    heads_out = jnp.concatenate([early_out, late_out], axis=0)
    summed = lax.psum_scatter(
        jnp.dot(heads_out, out_weight, preferred_element_type=jnp.float32).astype(jnp.bfloat16),
        "tp",
        scatter_dimension=1,
        tiled=True,
    )
    return summed


def gather_columns(piece):
    count = lax.axis_size("tp")
    index = lax.axis_index("tp")
    cols = piece.shape[1]
    whole = jnp.zeros((piece.shape[0], count * cols), piece.dtype)
    held = [(0, piece)]
    for bit in reversed(range(count.bit_length() - 1)):
        held = held + [(mask | 1 << bit, swap(part, "tp", 1 << bit)) for mask, part in held]
    for mask, part in held:
        whole = lax.dynamic_update_slice(whole, part, (0, (index ^ mask) * cols))
    return whole


def scatter_sum(partial):
    count = lax.axis_size("tp")
    index = lax.axis_index("tp")
    rows = partial.shape[0]
    parts = partial.reshape(rows, count, -1)
    for bit in range(count.bit_length() - 1):
        mine = index >> bit & 1
        parts = parts.reshape(rows, parts.shape[1] // 2, 2, parts.shape[2])
        kept = lax.dynamic_index_in_dim(parts, mine, 2, False)
        sent = lax.dynamic_index_in_dim(parts, 1 - mine, 2, False)
        parts = kept.astype(jnp.float32) + swap(sent.astype(jnp.bfloat16), "tp", 1 << bit)
    return parts.reshape(rows, -1)


def expert_layer(
    moe_input,
    moe_gain,
    route_ids,
    route_scores,
    shared_gate,
    shared_up,
    shared_down,
    expert_gate,
    expert_up,
    expert_down,
):
    ep_count = lax.axis_size("ep")
    token_count, width = moe_input.shape
    cols = width // lax.axis_size("tp")
    inputs = moe_input.astype(jnp.float32)
    normed = (
        inputs * lax.rsqrt(jnp.mean(inputs * inputs, axis=-1, keepdims=True) + EPS_NORM) * moe_gain
    ).astype(jnp.bfloat16)
    own_cols = lax.dynamic_slice_in_dim(normed, lax.axis_index("tp") * cols, cols, 1)
    local_experts = expert_gate.shape[0]
    expert_count = local_experts * ep_count
    topk = route_ids.shape[1]
    capacity = 3 * token_count * topk // (2 * expert_count)
    slots = expert_count * capacity
    pairs = token_count * topk
    chosen = route_ids.reshape(-1)
    pair_at = jnp.arange(pairs, dtype=jnp.int32)
    earlier = (chosen[:, None] == chosen[None, :]) & (pair_at[None, :] < pair_at[:, None])
    place_in = jnp.sum(earlier.astype(jnp.int32), axis=1)
    slot_ids = (chosen * capacity + place_in).reshape(token_count, topk)
    slot_at = jnp.arange(slots, dtype=jnp.int32)
    picks = [(slot_ids[:, k, None] == slot_at[None, :]) for k in range(topk)]
    dispatch = functools.reduce(jnp.logical_or, picks).astype(jnp.bfloat16)
    outgoing = lax.dot_general(
        dispatch, own_cols, (((0,), (0,)), ((), ())), preferred_element_type=jnp.float32
    ).astype(jnp.bfloat16)
    arrived = lax.all_to_all(outgoing, "ep", split_axis=0, concat_axis=0, tiled=True)
    piece = gather_columns(arrived)
    shared_hidden = (
        jax.nn.silu(jnp.dot(normed, shared_gate, preferred_element_type=jnp.float32))
        * jnp.dot(normed, shared_up, preferred_element_type=jnp.float32)
    ).astype(jnp.bfloat16)
    common = jnp.dot(shared_hidden, shared_down, preferred_element_type=jnp.float32)
    if local_experts == 1:
        grid = piece
        gate_sum = jnp.dot(grid, expert_gate[0], preferred_element_type=jnp.float32)
        up_sum = jnp.dot(grid, expert_up[0], preferred_element_type=jnp.float32)
        expert_hidden = (jax.nn.silu(gate_sum) * up_sum).astype(jnp.bfloat16)
        routed = jnp.dot(expert_hidden, expert_down[0], preferred_element_type=jnp.float32)
    else:
        grid = piece.reshape(ep_count, local_experts, capacity, width)
        gate_sum = jnp.einsum("secd,edf->secf", grid, expert_gate, preferred_element_type=jnp.float32)
        up_sum = jnp.einsum("secd,edf->secf", grid, expert_up, preferred_element_type=jnp.float32)
        expert_hidden = (jax.nn.silu(gate_sum) * up_sum).astype(jnp.bfloat16)
        routed = jnp.einsum(
            "secf,efd->secd", expert_hidden, expert_down, preferred_element_type=jnp.float32
        ).reshape(slots, width)
    summed = scatter_sum(jnp.concatenate([routed, common], axis=0).astype(jnp.bfloat16))
    returned = lax.all_to_all(
        summed[:slots].astype(jnp.bfloat16), "ep", split_axis=0, concat_axis=0, tiled=True
    )
    gates = route_scores / jnp.sum(route_scores, axis=-1, keepdims=True) * ROUTED_SCALE
    mix = summed[slots:]
    for k in range(topk):
        row = jnp.dot(picks[k].astype(jnp.bfloat16), returned, preferred_element_type=jnp.float32)
        mix = mix + row * gates[:, k, None]
    return mix.astype(jnp.bfloat16)


def body(
    queries,
    keys,
    values,
    key_bias,
    out_weight,
    *moe,
):
    ep_count = lax.axis_size("ep")
    if SEQUENCE_COUNT == 1 and 2 * key_bias.shape[1] == ep_count and lax.axis_size("tp") % 2 == 0:
        mixed = head_attention(queries, keys, values, key_bias, out_weight)
    else:
        mixed = row_attention(queries, keys, values, key_bias, out_weight)
    return (mixed, expert_layer(*moe))


def solution(mesh):
    return jax.shard_map(
        body,
        mesh=mesh,
        in_specs=(
            P("ep", "tp"),
            P("ep", "tp"),
            P("ep", "tp"),
            P("ep", "tp"),
            P("tp", None),
            P("ep", None),
            P(),
            P("ep", None),
            P("ep", None),
            P(None, "tp"),
            P(None, "tp"),
            P("tp", None),
            P("ep", None, "tp"),
            P("ep", None, "tp"),
            P("ep", "tp", None),
        ),
        out_specs=(P("ep", "tp"), P("ep", "tp")),
        check_vma=False,
    )
```

time: 472 us -> 173 us (0.37)
  other arithmetic: 149 us -> 19.1 us
  waiting for transfers between devices: 97.3 us -> 28.2 us
  local copies, waits for them, and re-layouts: 85 us -> 37.7 us
  matrix products: 54.8 us -> 21.3 us
  blocking collectives: 31.9 us -> 0 us
  Pallas kernels: 0 us -> 29.2 us
  between operations: 14.3 us -> 1.05 us
  starting transfers between devices: 25.3 us -> 34.7 us
  loops' own time: 8.35 us -> 0 us
    another operation x29 -> x0, other arithmetic: 110 us -> none
    reduce_scatter x1 -> x0, waiting for transfers between devices: 44.3 us -> none  [body(): lax.psum_scatter(jnp.concatenate([jnp.einsum('rh,hd->dr', heads_out, out_...]
    another operation x35 -> x1, local copies, waits for them, and re-layouts: 34.2 us -> 0.27 us  [the longest x11 17.9 us: absorb(): stay = lax.cumsum(keep, axis=2, reverse=True) - keep + carried[:, :, None]]
    dot_general x25 -> x9, matrix products: 54.8 us -> 21.3 us  [the longest x1 5.42 us: expert_layer(): jnp.dot(expert_hidden, expert_down[0], preferred_element_type=jnp.float32)]
    all_gather x1 -> x0, blocking collectives: 31.9 us -> none  [body(): lax.all_gather(own_piece[2], 'ep', axis=0, tiled=True)]
    pallas_call x0 -> x1, Pallas kernels: none -> 29.2 us  [stick(): pl.pallas_call(functools.partial(stick_kernel, width ** (-0.5) * LOG2E),...]
    convert_element_type x10 -> x3, other arithmetic: 24.3 us -> 2.33 us  [the longest x1 1.23 us: expert_layer(): normed = (inputs * lax.rsqrt(jnp.mean(inputs * inputs, axis=-1, keepdims=...]
    ppermute x6 -> x14, waiting for transfers between devices: 37 us -> 16.6 us  [swap(): lax.ppermute(array, axis, [(i, i ^ mask) for i in range(lax.axis_size(axi...]
  transfers between devices with their start and end apart: 12 -> 19, of which waited for: 8 -> 6; matrix products, arithmetic and copies ran while one was open for 55% -> 39% of each run, Pallas kernels for 0% -> 17%
where the time goes in v1:
time: 173 us; the launch traced here: 171 us
  local copies, waits for them, and re-layouts  37.7 us (22%)
  starting transfers between devices  34.7 us (20%)
  Pallas kernels  29.2 us (17%)
  waiting for transfers between devices  28.2 us (16%)
  matrix products  21.3 us (12%)
  other arithmetic  19.1 us (11%)
    pallas_call x1, Pallas kernels, stick(): pl.pallas_call(functools.partial(stick_kernel, width ** (-0.5) * LOG2E),...  29.2 us
    ppermute x14, waiting for transfers between devices, swap(): lax.ppermute(array, axis, [(i, i ^ mask) for i in range(lax.axis_size(axi...  16.6 us
    unnamed x37, local copies, waits for them, and re-layouts  11.4 us
    select_n x3, other arithmetic, by_group(): jnp.where(core == 0, jnp.concatenate([own, other], axis), jnp.concatenate...  8.9 us
    ppermute x14, starting transfers between devices, swap(): lax.ppermute(array, axis, [(i, i ^ mask) for i in range(lax.axis_size(axi...  8.29 us
    all_to_all x1, starting transfers between devices, expert_layer(): lax.all_to_all(outgoing, 'ep', split_axis=0, concat_axis=0, tiled=True)  7.28 us
    reshape x6, local copies, waits for them, and re-layouts, per_head(): return array.reshape(half, heads, depth).transpose(1, 0, 2)  7.09 us
    all_to_all x1, waiting for transfers between devices, head_attention(): lax.all_to_all(query_parts, 'ep', split_axis=0, concat_axis=0, tiled=True)  6.35 us
  transfers between devices with their start and end apart: 19, of which 6 were waited for; matrix products, arithmetic and copies ran while one was open for 39% of the time, Pallas kernels for 17%

profile of v1, /device:TPU:0, one launch (start us, length us, event | category | flops | bytes accessed | tf_op | source)
XLA Modules:
  0.0 171.3 jit_solution(16525756876293550316)
XLA Ops:
  6.5 7.3 %all-to-all-start.3 = ((bf16[8,48,512]{2,1,0:T(8,128)(2,1)}), bf16[8,48,512]{2,1,0:T(8,128)(2,1)S(1)}, u32[]{:S(2)}, u32[]{:S(2)}) async-start(bf16[8,48,512]{2,1,0:T(8,128)(2,1)} %bitcast.21), calls=%async_computation.3 | async-start | bytes 786432 | tf_op jit(solution)/shard_map/all_to_all | solution.py:359
  13.8 2.1 %constant_dynamic-slice_fusion.4 = (bf16[256,512]{1,0:T(8,128)(2,1)}, bf16[256,512]{1,0:T(8,128)(2,1)}, bf16[256,512]{1,0:T(8,128)(2,1)S(1)}, bf16[256,512]{1,0:T(8,128)(2,1)}) fusion(bf16[512,512]{1,0:T(8,128)(2,1)} %param.15, s32[]{:T(128)S(6)} %select_n.83, s32[]{:T(128)S(6)} %select_n.84, bf16[512,512]{1,0:T(8,128)(2,1)} %param.17), kind=kLoop, calls=%fused_computation.69 | loop fusion | bytes 2097160 | tf_op jit(solution)/shard_map/dynamic_slice | solution.py:131
  19.7 1.8 %copy.100 = bf16[256,512]{0,1:T(8,128)(2,1)} copy(bf16[256,512]{1,0:T(8,128)(2,1)} %get-tuple-element.20) | data formatting | bytes 524288
  28.4 1.8 %copy.85 = bf16[256,4,128]{2,0,1:T(8,128)(2,1)} copy(bf16[256,4,128]{0,2,1:T(8,128)(2,1)} %bitcast.8) | data formatting | bytes 524288 | tf_op jit(solution)/shard_map/reshape | solution.py:136
  32.0 7.0 %maximum_select_fusion = bf16[8,528,128]{2,1,0:T(8,128)(2,1)} fusion(bf16[4,16,128]{2,1,0:T(8,128)(2,1)} %pad.8, bf16[4,256,128]{2,1,0:T(8,128)(2,1)} %bitcast.93, bf16[4,256,128]{2,1,0:T(8,128)(2,1)} %bitcast.94, bf16[4,16,128]{2,1,0:T(8,128)(2,1)S(1)} %pad.7, bf16[4,256,128]{2,1,0:T(8,128)(2,1)S(1)} %bitcast.91, bf16[4,256,128]{2,1,0:T(8,128)(2,1)S(1)} %bitcast.92, ...), kind=kLoop, calls=%fused_computation.20 | loop fusion | flops 13516800 | bytes 2162689 | tf_op jit(solution)/shard_map/jit(_where)/select_n | solution.py:113
  39.0 6.1 %all-to-all-start = ((bf16[8,528,128]{2,1,0:T(8,128)(2,1)}), bf16[8,528,128]{2,1,0:T(8,128)(2,1)}, u32[]{:S(2)}, u32[]{:S(2)}) async-start(bf16[8,528,128]{2,1,0:T(8,128)(2,1)} %maximum_select_fusion), calls=%async_computation | async-start | bytes 2162688 | tf_op jit(solution)/shard_map/all_to_all | solution.py:152
  47.7 2.0 %fusion.40 = f32[128,512]{1,0:T(8,128)S(1)} fusion(bf16[128,2048]{1,0:T(8,128)(2,1)S(1)} %fusion.8, bf16[2048,512]{1,0:T(8,128)(2,1)} %param.24), kind=kOutput, calls=%fused_computation.87 | convolution fusion | flops 268435456 | bytes 2883584 | tf_op jit(solution)/shard_map/dot_general | solution.py:362
  49.9 3.9 %convolution_convert_fusion = bf16[128,2048]{1,0:T(8,128)(2,1)} fusion(bf16[512,2048]{1,0:T(8,128)(2,1)} %param.26, bf16[128,2048]{1,0:T(8,128)(2,1)S(1)} %fusion.8, bf16[2048,512]{1,0:T(8,128)(2,1)} %param.25, f32[128,512]{1,0:T(8,128)S(1)} %fusion.40), kind=kOutput, calls=%fused_computation.4 | convolution fusion | flops 537526272 | bytes 5505024 | tf_op jit(solution)/shard_map/dot_general | solution.py:365
  53.7 4.0 %copy.98 = bf16[2048,512]{1,0:T(8,128)(2,1)} copy(bf16[2048,512]{0,1:T(8,128)(2,1)} %bitcast.85) | data formatting | bytes 4194304 | tf_op jit(solution)/shard_map/dot_general | solution.py:371
  65.8 2.0 %fusion.1 = f32[384,512]{1,0:T(8,128)} fusion(bf16[384,2048]{1,0:T(8,128)(2,1)S(1)} %constant_dynamic-update-slice_fusion, bf16[1,2048,512]{2,1,0:T(8,128)(2,1)S(1)} %copy-done.14), kind=kOutput, calls=%fused_computation.8 | convolution fusion | flops 805306368 | bytes 4456448 | tf_op jit(solution)/shard_map/dot_general | solution.py:369
  67.7 4.6 %all-to-all-done.own_ref = bf16[8,528,128]{2,1,0:T(8,128)(2,1)} async-done(((bf16[8,528,128]{2,1,0:T(8,128)(2,1)}), bf16[8,528,128]{2,1,0:T(8,128)(2,1)}, u32[]{:S(2)}, u32[]{:S(2)}) %all-to-all-start) | async-done | bytes 1081376 | tf_op jit(solution)/shard_map/all_to_all | solution.py:152
  72.4 3.7 %all-to-all-start.1 = ((bf16[8,256,128]{2,1,0:T(8,128)(2,1)}), bf16[8,256,128]{2,1,0:T(8,128)(2,1)S(1)}, u32[]{:S(2)}, u32[]{:S(2)}) async-start(bf16[8,256,128]{2,1,0:T(8,128)(2,1)} %maximum_select_fusion.1), calls=%async_computation.1 | async-start | bytes 1048576 | tf_op jit(solution)/shard_map/all_to_all | solution.py:153
  76.1 5.4 %convolution_convert_fusion.1 = bf16[384,2,2,512]{3,0,2,1:T(8,128)(2,1)} fusion(bf16[2,2,512,512]{3,2,1,0:T(8,128)(2,1)} %bitcast.86, f32[384,512]{1,0:T(8,128)} %fusion.1, bf16[384,2048]{1,0:T(8,128)(2,1)} %copy-done.4, bf16[1,2048,512]{2,1,0:T(8,128)(2,1)S(1)} %copy-done), kind=kOutput, calls=%fused_computation.12 | convolution fusion | flops 1612578816 | bytes 8126464 | tf_op jit(solution)/shard_map/dot_general | solution.py:371
  81.6 2.3 %fusion.10 = bf16[512,2,512]{2,0,1:T(8,128)(2,1)} fusion(s32[]{:T(128)S(6)} %select_n.96, bf16[384,2,2,512]{3,0,2,1:T(8,128)(2,1)} %convolution_convert_fusion.1, bf16[128,2,2,512]{3,0,2,1:T(8,128)(2,1)S(1)} %copy.96), kind=kLoop, calls=%fused_computation.25 | loop fusion | flops 2097152 | bytes 3145732 | tf_op jit(solution)/shard_map/jit(dynamic_index_in_dim)/squeeze | solution.py:317
  84.4 6.3 %all-to-all-done.1.q_ref = bf16[8,256,128]{2,1,0:T(8,128)(2,1)S(1)} async-done(((bf16[8,256,128]{2,1,0:T(8,128)(2,1)}), bf16[8,256,128]{2,1,0:T(8,128)(2,1)S(1)}, u32[]{:S(2)}, u32[]{:S(2)}) %all-to-all-start.1) | async-done | bytes 524320 | tf_op jit(solution)/shard_map/all_to_all | solution.py:153
  91.5 29.2 %stick.1 = bf16[8,256,128]{2,1,0:T(8,128)(2,1)} custom-call(s32[1]{0:T(128)} %bitcast.half_ref, bf16[8,528,128]{2,1,0:T(8,128)(2,1)} %all-to-all-done.own_ref, bf16[8,528,128]{2,1,0:T(8,128)(2,1)} %collective-permute-done.3.other_ref, bf16[8,256,128]{2,1,0:T(8,128)(2,1)} %copy-done.7), custom_call_target="tpu_custom_call" | custom-call | flops 6039797760 | bytes 3145728 | tf_op jit(solution)/shard_map/stick/pallas_call | solution.py:90
  120.7 3.6 %all-to-all-start.2 = ((bf16[8,256,128]{2,1,0:T(8,128)(2,1)}), bf16[8,256,128]{2,1,0:T(8,128)(2,1)S(1)}, u32[]{:S(2)}, u32[]{:S(2)}) async-start(bf16[8,256,128]{2,1,0:T(8,128)(2,1)} %stick.1), calls=%async_computation.2 | async-start | bytes 1048576 | tf_op jit(solution)/shard_map/all_to_all | solution.py:156
  129.2 12.1 %collective-permute-done.13 = bf16[512,1,512]{2,0,1:T(8,128)(2,1)} collective-permute-done((bf16[512,1,512]{2,0,1:T(8,128)(2,1)S(1)}, bf16[512,1,512]{2,0,1:T(8,128)(2,1)}, u32[]{:S(2)}, u32[]{:S(2)}) %collective-permute-start.13) | collective-permute-done | bytes 524320 | tf_op jit(solution)/shard_map/ppermute | solution.py:23
  144.6 5.7 %all-to-all-start.4 = ((bf16[8,48,512]{2,1,0:T(8,128)(2,1)}), bf16[8,48,512]{2,1,0:T(8,128)(2,1)S(1)}, u32[]{:S(2)}, u32[]{:S(2)}) async-start(bf16[8,48,512]{2,1,0:T(8,128)(2,1)} %bitcast.34), calls=%async_computation.4 | async-start | bytes 786432 | tf_op jit(solution)/shard_map/all_to_all | solution.py:381
  153.0 2.4 %fusion.39 = f32[256,2048]{1,0:T(8,128)S(1)} fusion(bf16[256,512]{0,1:T(8,128)(2,1)S(1)} %bitcast.95, bf16[512,2048]{1,0:T(8,128)(2,1)} %param.19), kind=kOutput, calls=%fused_computation.86 | convolution fusion | flops 536870912 | bytes 4456448 | tf_op jit(solution)/shard_map/dot_general | solution.py:161
  155.4 2.3 %fusion = bf16[256,2048]{1,0:T(8,128)(2,1)S(1)} fusion(f32[256,2048]{1,0:T(8,128)S(1)} %fusion.39, bf16[256,512]{0,1:T(8,128)(2,1)S(1)} %bitcast.101, bf16[512,2048]{1,0:T(8,128)(2,1)} %collective-permute-done.5), kind=kOutput, calls=%fused_computation.3 | convolution fusion | flops 537919488 | bytes 5505024 | tf_op jit(solution)/shard_map/dot_general | solution.py:161
  162.8 1.9 %fusion.20 = bf16[128,512]{1,0:T(8,128)(2,1)} fusion(f32[128,512]{1,0:T(8,128)S(1)} %convolution_multiply_fusion.1, f32[512,1,512]{2,0,1:T(8,128)} %copy-done.2, bf16[384,512]{1,0:T(8,128)(2,1)S(1)} %bitcast.84, f32[128]{0:T(128)S(1)} %get-tuple-element.15, s32[128]{0:T(128)S(1)} %copy-done.9), kind=kOutput, calls=%fused_computation.40 | convolution fusion | flops 50642944 | bytes 1049600 | tf_op jit(solution)/shard_map/dot_general | solution.py:387
  164.7 1.8 %collective-permute-done.6 = bf16[256,512]{1,0:T(8,128)(2,1)} collective-permute-done((bf16[256,512]{1,0:T(8,128)(2,1)}, bf16[256,512]{1,0:T(8,128)(2,1)}, u32[]{:S(2)}, u32[]{:S(2)}) %collective-permute-start.6) | collective-permute-done | bytes 262176 | tf_op jit(solution)/shard_map/ppermute | solution.py:23
  167.5 2.6 %collective-permute-done.8 = bf16[256,512]{1,0:T(8,128)(2,1)S(1)} collective-permute-done((bf16[256,512]{1,0:T(8,128)(2,1)}, bf16[256,512]{1,0:T(8,128)(2,1)S(1)}, u32[]{:S(2)}, u32[]{:S(2)}) %collective-permute-start.8) | collective-permute-done | bytes 262176 | tf_op jit(solution)/shard_map/ppermute | solution.py:23
  (108 shorter events, 48.2 us)
Async XLA Ops:
  0.6 75.5 %copy-start = (bf16[1,2048,512]{2,1,0:T(8,128)(2,1)S(1)}, bf16[1,2048,512]{2,1,0:T(8,128)(2,1)}, u32[]{:S(2)}) copy-start(bf16[1,2048,512]{2,1,0:T(8,128)(2,1)} %param.27) | copy-start | bytes 6291460
  4.1 9.7 %copy-start.8 = (s32[128]{0:T(128)}, s32[128]{0:T(128)S(1)}, u32[]{:S(2)}) copy-start(s32[128]{0:T(128)S(1)} %get-tuple-element.18) | copy-start | bytes 1540
  4.1 9.7 %copy-start.10 = (s32[128]{0:T(128)}, s32[128]{0:T(128)S(1)}, u32[]{:S(2)}) copy-start(s32[128]{0:T(128)S(1)} %get-tuple-element.17) | copy-start | bytes 1540
  6.5 32.5 %all-to-all-start.3 = ((bf16[8,48,512]{2,1,0:T(8,128)(2,1)}), bf16[8,48,512]{2,1,0:T(8,128)(2,1)S(1)}, u32[]{:S(2)}, u32[]{:S(2)}) async-start(bf16[8,48,512]{2,1,0:T(8,128)(2,1)} %bitcast.21), calls=%async_computation.3 | async-start | bytes 786432 | tf_op jit(solution)/shard_map/all_to_all | solution.py:359
  16.7 11.7 %collective-permute-start.1 = (bf16[256,512]{0,1:T(8,128)(2,1)}, bf16[256,512]{0,1:T(8,128)(2,1)}, u32[]{:S(2)}, u32[]{:S(2)}) collective-permute-start(bf16[256,512]{0,1:T(8,128)(2,1)} %copy.102), channel_id=1, source_target_pairs={{0,1},{1,0},{2,3},{3,2},{4,5},{5,4},{6,7},{7,6},{8,9},{9,8},{10,11... | collective-permute-start | bytes 786440 | tf_op jit(solution)/shard_map/ppermute | solution.py:23
  18.6 11.6 %collective-permute-start = (bf16[256,512]{0,1:T(8,128)(2,1)}, bf16[256,512]{0,1:T(8,128)(2,1)}, u32[]{:S(2)}, u32[]{:S(2)}) collective-permute-start(bf16[256,512]{0,1:T(8,128)(2,1)} %copy.101), channel_id=1, source_target_pairs={{0,1},{1,0},{2,3},{3,2},{4,5},{5,4},{6,7},{7,6},{8,9},{9,8},{10,11... | collective-permute-start | bytes 786440 | tf_op jit(solution)/shard_map/ppermute | solution.py:23
  19.7 6.1 %collective-permute-start.2 = (bf16[256,4]{0,1:T(4,128)(2,1)}, bf16[256,4]{0,1:T(4,128)(2,1)}, u32[]{:S(2)}, u32[]{:S(2)}) collective-permute-start(bf16[256,4]{0,1:T(4,128)(2,1)} %get-tuple-element.14), channel_id=1, source_target_pairs={{0,1},{1,0},{2,3},{3,2},{4,5},{5,4},{6,7},{7,6},{8,9},{9,8},{10,11... | collective-permute-start | bytes 6152 | tf_op jit(solution)/shard_map/ppermute | solution.py:23
  39.0 6.1 %copy-start.5 = (bf16[256,512]{1,0:T(8,128)(2,1)S(1)}, bf16[256,512]{1,0:T(8,128)(2,1)}, u32[]{:S(2)}) copy-start(bf16[256,512]{1,0:T(8,128)(2,1)} %get-tuple-element.8) | copy-start | bytes 786436
  39.0 33.4 %all-to-all-start = ((bf16[8,528,128]{2,1,0:T(8,128)(2,1)}), bf16[8,528,128]{2,1,0:T(8,128)(2,1)}, u32[]{:S(2)}, u32[]{:S(2)}) async-start(bf16[8,528,128]{2,1,0:T(8,128)(2,1)} %maximum_select_fusion), calls=%async_computation | async-start | bytes 2162688 | tf_op jit(solution)/shard_map/all_to_all | solution.py:152
  46.0 13.5 %collective-permute-start.4 = (bf16[256,512]{0,1:T(8,128)(2,1)}, bf16[256,512]{0,1:T(8,128)(2,1)}, u32[]{:S(2)}, u32[]{:S(2)}) collective-permute-start(bf16[256,512]{0,1:T(8,128)(2,1)} %copy.104), channel_id=1, source_target_pairs={{0,1},{1,0},{2,3},{3,2},{4,5},{5,4},{6,7},{7,6},{8,9},{9,8},{10,11... | collective-permute-start | bytes 786440 | tf_op jit(solution)/shard_map/ppermute | solution.py:23
  46.2 14.4 %collective-permute-start.9 = (bf16[384,512]{1,0:T(8,128)(2,1)S(1)}, bf16[384,512]{1,0:T(8,128)(2,1)}, u32[]{:S(2)}, u32[]{:S(2)}) collective-permute-start(bf16[384,512]{1,0:T(8,128)(2,1)S(1)} %bitcast.88), channel_id=1, source_target_pairs={{0,2},{1,3},{2,0},{3,1},{4,6},{5,7},{6,4},{7,5},{8,10},{9,11},{10,... | collective-permute-start | bytes 1179656 | tf_op jit(solution)/shard_map/ppermute | solution.py:23
  49.8 13.7 %collective-permute-start.10 = (bf16[384,512]{1,0:T(8,128)(2,1)S(1)}, bf16[384,512]{1,0:T(8,128)(2,1)}, u32[]{:S(2)}, u32[]{:S(2)}) collective-permute-start(bf16[384,512]{1,0:T(8,128)(2,1)S(1)} %bitcast.89), channel_id=1, source_target_pairs={{0,1},{1,0},{2,3},{3,2},{4,5},{5,4},{6,7},{7,6},{8,9},{9,8},{10,11... | collective-permute-start | bytes 1179656 | tf_op jit(solution)/shard_map/ppermute | solution.py:23
  60.6 3.9 %collective-permute-start.11 = (bf16[384,512]{1,0:T(8,128)(2,1)}, bf16[384,512]{1,0:T(8,128)(2,1)S(1)}, u32[]{:S(2)}, u32[]{:S(2)}) collective-permute-start(bf16[384,512]{1,0:T(8,128)(2,1)} %collective-permute-done.9), channel_id=1, source_target_pairs={{0,1},{1,0},{2,3},{3,2},{4,5},{5,4},{6,7},{7,6},{8,9},{9,8},{10,11... | collective-permute-start | bytes 1179656 | tf_op jit(solution)/shard_map/ppermute | solution.py:23
  72.4 18.3 %all-to-all-start.1 = ((bf16[8,256,128]{2,1,0:T(8,128)(2,1)}), bf16[8,256,128]{2,1,0:T(8,128)(2,1)S(1)}, u32[]{:S(2)}, u32[]{:S(2)}) async-start(bf16[8,256,128]{2,1,0:T(8,128)(2,1)} %maximum_select_fusion.1), calls=%async_computation.1 | async-start | bytes 1048576 | tf_op jit(solution)/shard_map/all_to_all | solution.py:153
  76.1 14.7 %collective-permute-start.3 = (bf16[8,528,128]{2,1,0:T(8,128)(2,1)}, bf16[8,528,128]{2,1,0:T(8,128)(2,1)}, u32[]{:S(2)}, u32[]{:S(2)}) collective-permute-start(bf16[8,528,128]{2,1,0:T(8,128)(2,1)} %all-to-all-done.own_ref), channel_id=1, source_target_pairs={{0,1},{1,0},{2,3},{3,2},{4,5},{5,4},{6,7},{7,6},{8,9},{9,8},{10,11... | collective-permute-start | bytes 3244040 | tf_op jit(solution)/shard_map/ppermute | solution.py:23
  83.9 40.5 %collective-permute-start.12 = (bf16[512,2,512]{2,0,1:T(8,128)(2,1)}, bf16[512,2,512]{2,0,1:T(8,128)(2,1)}, u32[]{:S(2)}, u32[]{:S(2)}) collective-permute-start(bf16[512,2,512]{2,0,1:T(8,128)(2,1)} %fusion.10), channel_id=1, source_target_pairs={{0,1},{1,0},{2,3},{3,2},{4,5},{5,4},{6,7},{7,6},{8,9},{9,8},{10,11... | collective-permute-start | bytes 3145736 | tf_op jit(solution)/shard_map/ppermute | solution.py:23
  84.3 71.0 %collective-permute-start.5 = (bf16[512,2048]{1,0:T(8,128)(2,1)}, bf16[512,2048]{1,0:T(8,128)(2,1)}, u32[]{:S(2)}, u32[]{:S(2)}) collective-permute-start(bf16[512,2048]{1,0:T(8,128)(2,1)} %param.19), channel_id=1, source_target_pairs={{0,1},{1,0},{2,3},{3,2},{4,5},{5,4},{6,7},{7,6},{8,9},{9,8},{10,11... | collective-permute-start | bytes 6291464 | tf_op jit(solution)/shard_map/ppermute | solution.py:23
  120.7 23.9 %all-to-all-start.2 = ((bf16[8,256,128]{2,1,0:T(8,128)(2,1)}), bf16[8,256,128]{2,1,0:T(8,128)(2,1)S(1)}, u32[]{:S(2)}, u32[]{:S(2)}) async-start(bf16[8,256,128]{2,1,0:T(8,128)(2,1)} %stick.1), calls=%async_computation.2 | async-start | bytes 1048576 | tf_op jit(solution)/shard_map/all_to_all | solution.py:156
  127.6 13.7 %collective-permute-start.13 = (bf16[512,1,512]{2,0,1:T(8,128)(2,1)S(1)}, bf16[512,1,512]{2,0,1:T(8,128)(2,1)}, u32[]{:S(2)}, u32[]{:S(2)}) collective-permute-start(bf16[512,1,512]{2,0,1:T(8,128)(2,1)S(1)} %dynamic-slice_convert_fusion), channel_id=1, source_target_pairs={{0,2},{1,3},{2,0},{3,1},{4,6},{5,7},{6,4},{7,5},{8,10},{9,11},{10,... | collective-permute-start | bytes 1572872 | tf_op jit(solution)/shard_map/ppermute | solution.py:23
  144.6 16.1 %all-to-all-start.4 = ((bf16[8,48,512]{2,1,0:T(8,128)(2,1)}), bf16[8,48,512]{2,1,0:T(8,128)(2,1)S(1)}, u32[]{:S(2)}, u32[]{:S(2)}) async-start(bf16[8,48,512]{2,1,0:T(8,128)(2,1)} %bitcast.34), calls=%async_computation.4 | async-start | bytes 786432 | tf_op jit(solution)/shard_map/all_to_all | solution.py:381
  155.4 5.4 %copy-start.11 = (s32[128]{0:T(128)S(1)}, s32[128]{0:T(128)}, u32[]{:S(2)}) copy-start(s32[128]{0:T(128)} %copy-done.10) | copy-start | bytes 1540
  158.7 7.8 %collective-permute-start.6 = (bf16[256,512]{1,0:T(8,128)(2,1)}, bf16[256,512]{1,0:T(8,128)(2,1)}, u32[]{:S(2)}, u32[]{:S(2)}) collective-permute-start(bf16[256,512]{1,0:T(8,128)(2,1)} %get-tuple-element.2), channel_id=1, source_target_pairs={{0,2},{1,3},{2,0},{3,1},{4,6},{5,7},{6,4},{7,5},{8,10},{9,11},{10,... | collective-permute-start | bytes 786440 | tf_op jit(solution)/shard_map/ppermute | solution.py:23
  161.1 6.5 %collective-permute-start.7 = (bf16[256,512]{1,0:T(8,128)(2,1)}, bf16[256,512]{1,0:T(8,128)(2,1)S(1)}, u32[]{:S(2)}, u32[]{:S(2)}) collective-permute-start(bf16[256,512]{1,0:T(8,128)(2,1)} %get-tuple-element.4), channel_id=1, source_target_pairs={{0,1},{1,0},{2,3},{3,2},{4,5},{5,4},{6,7},{7,6},{8,9},{9,8},{10,11... | collective-permute-start | bytes 786440 | tf_op jit(solution)/shard_map/ppermute | solution.py:23
  161.1 9.0 %collective-permute-start.8 = (bf16[256,512]{1,0:T(8,128)(2,1)}, bf16[256,512]{1,0:T(8,128)(2,1)S(1)}, u32[]{:S(2)}, u32[]{:S(2)}) collective-permute-start(bf16[256,512]{1,0:T(8,128)(2,1)} %get-tuple-element.3), channel_id=1, source_target_pairs={{0,3},{1,2},{2,1},{3,0},{4,7},{5,6},{6,5},{7,4},{8,11},{9,10},{10,... | collective-permute-start | bytes 786440 | tf_op jit(solution)/shard_map/ppermute | solution.py:23
  (10 other events, 29.6 us)

commit v2 on v1

--- a/solution.py
+++ b/solution.py
@@ -2,17 +2,21 @@
 
 import jax
 import jax.numpy as jnp
+import numpy as np
 from jax import lax
 from jax.experimental import pallas as pl
 from jax.experimental.pallas import tpu as pltpu
 from jax.sharding import PartitionSpec as P
 
+
 SEQUENCE_COUNT = 1
 
 
 EPS_NORM = 1e-06
 ROUTED_SCALE = 2.5
 LOG2E = 1.4426950408889634
+NEVER = -1e30
+MIB = 1 << 20
 
 
 def partner_2(array, axis, apart):
@@ -23,160 +27,324 @@
     return lax.ppermute(array, axis, [(i, i ^ mask) for i in range(lax.axis_size(axis))])
 
 
-def stick_kernel(scale, half_ref, own_ref, other_ref, q_ref, out_ref, k_s, v_s, b_s, tri_s, acc_s, carry_s):
-    blocks, rows, width = q_ref.shape
+def rounds_of(heads):
+    return [(k, s) for k in range(heads) for s in range(2)]
+
+
+def send_round(array, heads, k, s):
+    ep_count, tp_count = lax.axis_size("ep"), lax.axis_size("tp")
+    pairs = []
+    for i in range(ep_count):
+        for t in range(tp_count):
+            core = t % 2
+            to_ep = core * heads + (i + k) % heads
+            to_tp = t - core + (i // heads + s) % 2
+            pairs.append((i * tp_count + t, to_ep * tp_count + to_tp))
+    return lax.ppermute(array, ("ep", "tp"), pairs)
+
+
+def pack_kernel(heads, k_ref, v_ref, q_ref, bias_ref, *refs):
+    out_refs, bias_s = refs[:-1], refs[-1]
+    own = lax.axis_index("ep")
+    span = k_ref.shape[0]
+    half = span // 2
+    depth = k_ref.shape[1] // heads
+    bias_rows = half // depth
+    turned = bias_ref[...].astype(jnp.float32)
+    for head in range(heads):
+        for r in range(span // depth):
+            bias_s[head, r] = turned[head : head + 1, r * depth : (r + 1) * depth]
+    for (k, s), out_ref in zip(rounds_of(heads), out_refs):
+        head = lax.rem(own + k, heads)
+        part = lax.rem(own // heads + s, 2)
+        rows = pl.ds(pl.multiple_of(part * half, half), half)
+        lanes = pl.ds(pl.multiple_of(head * depth, depth), depth)
+        out_ref[:half] = k_ref[rows, lanes]
+        out_ref[half : 2 * half] = v_ref[rows, lanes]
+        pad = out_ref.shape[0] - 3 * half
+        at = lax.broadcasted_iota(jnp.int32, (pad, depth), 0)
+        bias = jnp.zeros((pad, depth), jnp.float32)
+        for r in range(bias_rows):
+            bias = jnp.where(at == r, bias_s[head, part * bias_rows + r], bias)
+        out_ref[2 * half : 2 * half + pad] = bias.astype(out_ref.dtype)
+        out_ref[2 * half + pad :] = q_ref[rows, lanes]
+
+
+def pack(keys, values, queries, bias):
+    heads, span = bias.shape
+    half, depth = span // 2, keys.shape[1] // heads
+    pad = -(-(half // depth) // 16) * 16
+    vmem = pl.BlockSpec(memory_space=pltpu.VMEM)
+    count = len(rounds_of(heads))
+    shape = jax.ShapeDtypeStruct((3 * half + pad, depth), keys.dtype)
+    return pl.pallas_call(
+        functools.partial(pack_kernel, heads),
+        out_shape=[shape] * count,
+        in_specs=[vmem] * 4,
+        out_specs=[vmem] * count,
+        scratch_shapes=[pltpu.VMEM((heads, span // depth, 1, depth), jnp.float32)],
+        cost_estimate=pl.CostEstimate(
+            flops=keys.size * 8, bytes_accessed=12 * keys.size, transcendentals=0
+        ),
+        name="pack",
+    )(keys, values, queries, bias)
+
+
+def steps_of(groups, turns):
+    steps = [(g, source) for g in range(groups) for source in reversed(range((g + 1) * turns))]
+    return steps + [(groups, 0)] * 2
+
+
+def stick_kernel(scale, heads, turn, turns, spot, table_ref, *refs):
+    count = 2 * heads
+    messages, out_ref = refs[: 2 * count], refs[2 * count]
+    mes_s, q_s, b_s, tri_s, reach_s, soft_s, log_s, prod_s, acc_s, carry_s, sems = refs[2 * count + 1 :]
+    blocks, piece, width = out_ref.shape
+    groups = blocks // turns
+    rows = piece * turns
     bias_rows = rows // width
-    mine = half_ref[0]
-    for which, ref in ((mine, own_ref), (1 - mine, other_ref)):
-        k_s[which] = ref[:, :rows]
-        v_s[which] = ref[:, rows : 2 * rows]
-        for block in range(blocks):
-            lanes = [
-                ref[block, pl.ds(2 * rows + r, 1), :].astype(jnp.float32) * LOG2E
-                for r in range(bias_rows)
+    pad = mes_s.shape[2] - 3 * rows
+    place, mine = spot()
+    for at, which in enumerate((mine, 1 - mine)):
+        for (k, s), ref in zip(rounds_of(heads), messages[at * count : (at + 1) * count]):
+            block = lax.rem(which + s, 2) * heads + lax.rem(place + heads - k, heads)
+            pltpu.make_async_copy(ref, mes_s.at[which, block], sems.at[which, block]).start()
+    later = lax.broadcasted_iota(jnp.int32, (2 * rows, rows), 0)
+    column = lax.broadcasted_iota(jnp.int32, (2 * rows, rows), 1)
+    tri_s[...] = jnp.where(later > column, 1.0, 0.0).astype(jnp.bfloat16)
+    row = lax.broadcasted_iota(jnp.int32, (rows, rows), 0)
+    row = row // piece * (2 * rows) + row % piece + (mine * rows + turn * piece)
+    reach_s[...] = lax.broadcasted_iota(jnp.int32, (rows, rows), 1) - row
+    query_at = 2 * rows + pad + turn * piece
+
+    def arrive(group):
+        for at in range(turns):
+            block = group * turns + at
+            for which in (0, 1):
+                pltpu.make_async_copy(
+                    messages[0], mes_s.at[which, block], sems.at[which, block]
+                ).wait()
+                lanes = [
+                    mes_s[which, block, 2 * rows + r : 2 * rows + r + 1, :].astype(jnp.float32)
+                    for r in range(bias_rows)
+                ]
+                b_s[which, block] = jnp.concatenate(lanes, axis=1) * LOG2E
+            q_s[group, at * piece : (at + 1) * piece] = mes_s[
+                mine, block, query_at : query_at + piece
             ]
-            b_s[which, block] = jnp.concatenate(lanes, axis=1)
-    later = lax.broadcasted_iota(jnp.int32, (rows, rows + width), 0)
-    column = lax.broadcasted_iota(jnp.int32, (rows, rows + width), 1)
-    tri_s[...] = jnp.where((later > column) | (column >= rows), 1.0, 0.0).astype(jnp.bfloat16)
-
-    def step(query, source, visible_of):
-        for part in (1, 0):
-            logit = lax.dot_general(
-                query,
-                k_s[part, source],
+
+    arrive(0)
+    arrive(1)
+    q_s[groups] = q_s[0]
+    parts = (1, 0)
+
+    def scores(group, source):
+        return [
+            lax.dot_general(
+                q_s[group],
+                mes_s[part, source, :rows],
                 (((1,), (1,)), ((), ())),
                 preferred_element_type=jnp.float32,
             )
-            logit = logit * scale + b_s[part, source]
+            for part in parts
+        ]
+
+    def soften(slot, group, source):
+        ahead = (group * turns - source) * (2 * rows)
+        for part in parts:
+            logit = prod_s[part] * scale + b_s[part, source]
+            logit = jnp.where(reach_s[...] < ahead - part * rows, logit, NEVER)
             soft = jnp.maximum(logit, jnp.log2(1.0 + jnp.exp2(jnp.minimum(logit, 64.0))))
-            if visible_of is not None:
-                visible = visible_of(part)
-                soft = jnp.where(visible, soft, 0.0)
-            sums = jnp.dot(soft.astype(jnp.bfloat16), tri_s[...], preferred_element_type=jnp.float32)
-            carry = carry_s[...]
-            carry_s[...] = carry + sums[:, rows:]
+            soft_s[slot, part] = soft.astype(jnp.bfloat16)
+            log_s[slot, part] = logit - soft
+
+    def sums(slot):
+        one = jnp.dot(soft_s[slot, 1], tri_s[:rows], preferred_element_type=jnp.float32)
+        both = jnp.concatenate([soft_s[slot, 0], soft_s[slot, 1]], axis=1)
+        return [one, jnp.dot(both, tri_s[...], preferred_element_type=jnp.float32)]
+
+    def entry(t):
+        return table_ref[0, 2 * t], table_ref[0, 2 * t + 1]
+
+    def put(products):
+        for part, product in zip(parts, products):
+            prod_s[part] = product
+
+    put(scores(*entry(0)))
+    soften(0, *entry(0))
+    put(scores(*entry(1)))
+
+    def pair(at, _):
+        acc = acc_s[...]
+        carry = carry_s[...]
+        for slot in range(2):
+            t = 2 * at + slot
+            totals = sums(slot)
+            products = scores(*entry(t + 2))
+            soften(1 - slot, *entry(t + 1))
+            put(products)
             wide = jnp.concatenate([carry] * bias_rows, axis=1)
-            weight = jnp.exp2((logit - soft) - (sums[:, :rows] + wide))
-            if visible_of is not None:
-                weight = jnp.where(visible, weight, 0.0)
-            acc_s[...] += jnp.dot(
-                weight.astype(jnp.bfloat16), v_s[part, source], preferred_element_type=jnp.float32
-            )
-
-    def one_block(block, _):
-        query = q_ref[block]
-        acc_s[...] = jnp.zeros_like(acc_s)
-        carry_s[...] = jnp.zeros_like(carry_s)
-        row = lax.broadcasted_iota(jnp.int32, (rows, rows), 0) + mine * rows
-        key = lax.broadcasted_iota(jnp.int32, (rows, rows), 1)
-        step(query, block, lambda part: key + part * rows < row)
-
-        def earlier(turn, _):
-            step(query, block - 1 - turn, None)
-            return 0
-
-        lax.fori_loop(0, block, earlier, 0)
-        out_ref[block] = acc_s[...].astype(out_ref.dtype)
+            source = entry(t)[1]
+            for part, total in zip(parts, totals):
+                weight = jnp.exp2(log_s[slot, part] - (total + wide)).astype(jnp.bfloat16)
+                values = mes_s[part, source, rows : 2 * rows]
+                acc = acc + jnp.dot(weight, values, preferred_element_type=jnp.float32)
+            whole = totals[1][:, :1] + soft_s[slot, 0, :, :width].astype(jnp.float32)[:, :1]
+            carry = carry + jnp.broadcast_to(whole, (rows, width))
+        acc_s[...] = acc
+        carry_s[...] = carry
+        group = entry(2 * at)[0]
+
+        @pl.when(group != entry(2 * at + 2)[0])
+        def _():
+            for turn_at in range(turns):
+                part = acc_s[turn_at * piece : (turn_at + 1) * piece]
+                out_ref[group * turns + turn_at] = part.astype(out_ref.dtype)
+            acc_s[...] = jnp.zeros_like(acc_s)
+            carry_s[...] = jnp.zeros_like(carry_s)
+
+            @pl.when(group + 2 < groups)
+            def _():
+                arrive(group + 2)
+
         return 0
 
-    lax.fori_loop(0, blocks, one_block, 0)
-
-
-def stick(half, own, other, query):
-    blocks, rows, width = query.shape
-    pairs = blocks * (blocks + 1) * rows * rows
-    vmem = pl.BlockSpec(memory_space=pltpu.VMEM)
+    acc_s[...] = jnp.zeros_like(acc_s)
+    carry_s[...] = jnp.zeros_like(carry_s)
+    lax.fori_loop(0, table_ref.shape[1] // 4 - 1, pair, 0)
+
+
+def here():
+    return lax.axis_index("ep"), lax.rem(lax.axis_index("tp"), 2)
+
+
+def stick(own, other, blocks, rows, width, turn, turns, spot=here):
+    length = own[0].shape[0]
+    groups = blocks // turns
+    piece = rows // turns
+    table = np.array(steps_of(groups, turns), np.int32).reshape(1, -1)
+    pairs = 2 * rows * rows * (table.shape[1] // 2 - 2)
     return pl.pallas_call(
-        functools.partial(stick_kernel, width**-0.5 * LOG2E),
-        out_shape=jax.ShapeDtypeStruct(query.shape, jnp.bfloat16),
-        in_specs=[pl.BlockSpec(memory_space=pltpu.SMEM), vmem, vmem, vmem],
-        out_specs=vmem,
+        functools.partial(stick_kernel, width**-0.5 * LOG2E, len(own) // 2, turn, turns, spot),
+        out_shape=jax.ShapeDtypeStruct((blocks, piece, width), jnp.bfloat16),
+        in_specs=[pl.BlockSpec(memory_space=pltpu.SMEM)]
+        + [pl.BlockSpec(memory_space=pl.ANY)] * (2 * len(own)),
+        out_specs=pl.BlockSpec(memory_space=pltpu.VMEM),
         scratch_shapes=[
-            pltpu.VMEM((2, blocks, rows, width), jnp.bfloat16),
-            pltpu.VMEM((2, blocks, rows, width), jnp.bfloat16),
+            pltpu.VMEM((2, blocks, length, width), jnp.bfloat16),
+            pltpu.VMEM((groups + 1, rows, width), jnp.bfloat16),
             pltpu.VMEM((2, blocks, 1, rows), jnp.float32),
-            pltpu.VMEM((rows, rows + width), jnp.bfloat16),
+            pltpu.VMEM((2 * rows, rows), jnp.bfloat16),
+            pltpu.VMEM((rows, rows), jnp.int32),
+            pltpu.VMEM((2, 2, rows, rows), jnp.bfloat16),
+            pltpu.VMEM((2, 2, rows, rows), jnp.float32),
+            pltpu.VMEM((2, rows, rows), jnp.float32),
             pltpu.VMEM((rows, width), jnp.float32),
             pltpu.VMEM((rows, width), jnp.float32),
+            pltpu.SemaphoreType.DMA((2, blocks)),
         ],
         cost_estimate=pl.CostEstimate(
             flops=2 * pairs * (rows + 3 * width),
-            bytes_accessed=12 * blocks * rows * width,
+            bytes_accessed=10 * blocks * rows * width,
             transcendentals=3 * pairs,
         ),
-        name="stick",
-    )(half, own, other, query)
-
-
-def by_group(core, own, other, axis=0):
-    return jnp.where(
-        core == 0, jnp.concatenate([own, other], axis), jnp.concatenate([other, own], axis)
-    )
-
-
-def head_attention(queries, keys, values, key_bias, out_weight):
-    span, width = queries.shape
-    heads = key_bias.shape[1]
-    depth = width // heads
-    half = span // 2
+    )(jnp.asarray(table), *own, *other)
+
+
+def project_kernel(back_ref, own_ref, other_ref, first_ref, *rest):
+    out_refs, rows_s = rest[:-1], rest[-1]
+    tp_index = lax.axis_index("tp")
+    core = lax.rem(tp_index, 2)
+    heads, _, depth = back_ref.shape
+    width = own_ref.shape[0]
+    cols = first_ref.shape[1]
+    for head in range(heads):
+        rows_s[head * depth // width, :, head * depth % width : (head * depth % width) + depth] = back_ref[head]
+    own_rows = rows_s[core]
+    other_rows = rows_s[1 - core]
+    for mask in range(len(out_refs), -1, -1):
+        at = pl.ds(pl.multiple_of((tp_index ^ mask) * cols, cols), cols)
+        part = jnp.dot(own_rows, own_ref[:, at], preferred_element_type=jnp.float32)
+        part += jnp.dot(other_rows, other_ref[:, at], preferred_element_type=jnp.float32)
+        ref = out_refs[mask - 1] if mask else first_ref
+        ref[...] = part.astype(ref.dtype)
+
+
+def project(back, own_weight, other_weight, tp_count):
+    heads, half, depth = back.shape
+    cols = own_weight.shape[1] // tp_count
+    vmem = pl.BlockSpec(memory_space=pltpu.VMEM)
+    shape = jax.ShapeDtypeStruct((half, cols), jnp.bfloat16)
+    return pl.pallas_call(
+        project_kernel,
+        out_shape=[shape] * tp_count,
+        in_specs=[vmem] * 3,
+        out_specs=[vmem] * tp_count,
+        scratch_shapes=[pltpu.VMEM((2, half, own_weight.shape[0]), jnp.bfloat16)],
+        cost_estimate=pl.CostEstimate(
+            flops=2 * half * heads * depth * own_weight.shape[1],
+            bytes_accessed=4 * own_weight.size + 4 * half * own_weight.shape[1],
+            transcendentals=0,
+        ),
+        compiler_params=pltpu.CompilerParams(vmem_limit_bytes=16 * MIB),
+        name="project",
+    )(back, own_weight, other_weight)
+
+
+def finish_kernel(turns, *refs):
+    out_ref = refs[-1]
+    core = lax.rem(lax.axis_index("tp"), 2)
+    piece = refs[0].shape[0]
+    count = (len(refs) - 1) // turns
+    for turn in range(turns):
+        for bit in range(2):
+            mine = [ref[...].astype(jnp.float32) for ref in refs[turn * count + bit : (turn + 1) * count : 2]]
+            total = functools.reduce(jnp.add, mine)
+            part = core if bit == 0 else 1 - core
+            at = pl.multiple_of((part * turns + turn) * piece, piece)
+            out_ref[pl.ds(at, piece)] = total.astype(out_ref.dtype)
+
+
+def finish(pieces):
+    turns = len(pieces)
+    flat = sum(pieces, [])
+    rows, cols = flat[0].shape
+    vmem = pl.BlockSpec(memory_space=pltpu.VMEM)
+    return pl.pallas_call(
+        functools.partial(finish_kernel, turns),
+        out_shape=jax.ShapeDtypeStruct((2 * turns * rows, cols), jnp.bfloat16),
+        in_specs=[vmem] * len(flat),
+        out_specs=vmem,
+        cost_estimate=pl.CostEstimate(
+            flops=8 * rows * turns * cols, bytes_accessed=12 * rows * turns * cols, transcendentals=0
+        ),
+        compiler_params=pltpu.CompilerParams(vmem_limit_bytes=8 * MIB),
+        name="finish",
+    )(*flat)
+
+
+TURNS = 2
+
+
+def head_attention(messages, out_weight, heads):
     ep_count = lax.axis_size("ep")
     tp_count = lax.axis_size("tp")
-    tp_index = lax.axis_index("tp")
-    core = tp_index % 2
-    pad = 16 - half // depth % 16
-
-    def split(array):
-        return (
-            lax.dynamic_slice_in_dim(array, core * half, half, 0),
-            lax.dynamic_slice_in_dim(array, (1 - core) * half, half, 0),
-        )
-
-    def per_head(array):
-        return array.reshape(half, heads, depth).transpose(1, 0, 2)
-
-    own, away = zip(*[split(array) for array in (keys, values, queries, key_bias)])
-    got = [swap(array, "tp", 1) for array in away]
-
-    def bias_rows(array):
-        rows = array.T.reshape(heads, half // depth, depth)
-        return jnp.pad(rows, ((0, 0), (0, pad), (0, 0)))
-
-    def key_message(key_rows, value_rows, bias):
-        return jnp.concatenate([per_head(key_rows), per_head(value_rows), bias_rows(bias)], axis=1)
-
-    key_parts = by_group(
-        core, key_message(own[0], own[1], own[3]), key_message(got[0], got[1], got[3])
-    )
-    query_parts = by_group(core, per_head(own[2]), per_head(got[2]))
-    own_keys = lax.all_to_all(key_parts, "ep", split_axis=0, concat_axis=0, tiled=True)
-    query_rows = lax.all_to_all(query_parts, "ep", split_axis=0, concat_axis=0, tiled=True)
-    other_keys = swap(own_keys, "tp", 1)
-    out = stick(core.reshape(1), own_keys, other_keys, query_rows)
-    back = lax.all_to_all(out, "ep", split_axis=0, concat_axis=0, tiled=True)
+    own, other = [], []
+    for (k, s), message in zip(rounds_of(heads), messages):
+        own.append(send_round(message, heads, k, s))
+        other.append(swap(own[-1], "tp", 1))
+    depth = out_weight.shape[0] // heads
+    half = messages[0].shape[0] // 3 // 16 * 16
     other_weight = swap(out_weight, "tp", 1)
-
-    def project(group, weight):
-        rows = lax.dynamic_slice_in_dim(back, group * heads, heads, 0)
-        return jnp.dot(
-            rows.transpose(1, 0, 2).reshape(half, width), weight, preferred_element_type=jnp.float32
-        )
-
-    partial = (project(core, out_weight) + project(1 - core, other_weight)).astype(jnp.bfloat16)
-    cols = partial.shape[1] // tp_count
-
-    def columns(index):
-        return lax.dynamic_slice_in_dim(partial, index * cols, cols, 1)
-
-    same = columns(tp_index).astype(jnp.float32)
-    cross = jnp.zeros_like(same)
-    for mask in range(1, tp_count):
-        piece = swap(columns(tp_index ^ mask), "tp", mask).astype(jnp.float32)
-        if mask % 2:
-            cross = cross + piece
-        else:
-            same = same + piece
-    return by_group(core, same.astype(jnp.bfloat16), cross.astype(jnp.bfloat16))
+    pieces = []
+    for turn in range(TURNS):
+        out = stick(own, other, ep_count, half, depth, turn, TURNS)
+        back = lax.all_to_all(out, "ep", split_axis=0, concat_axis=0, tiled=True)
+        parts = list(project(back, out_weight, other_weight, tp_count))
+        for mask in range(1, tp_count):
+            parts[mask] = swap(parts[mask], "tp", mask)
+        pieces.append(parts)
+    return finish(pieces)
 
 
 def absorb(state, query_heads, piece, visible):
@@ -389,20 +557,209 @@
     return mix.astype(jnp.bfloat16)
 
 
-def body(
-    queries,
-    keys,
-    values,
-    key_bias,
-    out_weight,
-    *moe,
+def gather_pieces(piece):
+    pieces = [piece]
+    for mask in range(1, lax.axis_size("tp")):
+        pieces.append(swap(piece, "tp", mask))
+    return pieces
+
+
+def scatter_rest(kept, sent):
+    index = lax.axis_index("tp")
+    parts = kept.astype(jnp.float32) + swap(sent, "tp", 1)
+    for bit in range(1, lax.axis_size("tp").bit_length() - 1):
+        mine = index >> bit & 1
+        parts = parts.reshape(parts.shape[0] // 2, 2, *parts.shape[1:])
+        stay = lax.dynamic_index_in_dim(parts, mine, 1, False)
+        leave = lax.dynamic_index_in_dim(parts, 1 - mine, 1, False)
+        parts = stay + swap(leave.astype(jnp.bfloat16), "tp", 1 << bit)
+    return parts[0]
+
+
+def route_kernel(capacity, input_ref, gain_ref, ids_ref, out_ref, normed_ref, slots_ref):
+    tokens, _ = input_ref.shape
+    slots, cols = out_ref.shape
+    topk = ids_ref.shape[0]
+    inputs = input_ref[...].astype(jnp.float32)
+    mean = jnp.mean(inputs * inputs, axis=-1, keepdims=True)
+    normed_ref[...] = (inputs * lax.rsqrt(mean + EPS_NORM) * gain_ref[...]).astype(jnp.bfloat16)
+    experts_at = -(-(slots // capacity) // 16) * 16
+    expert = lax.broadcasted_iota(jnp.int32, (experts_at, tokens), 0)
+    named = [ids_ref[k : k + 1] == expert for k in range(topk)]
+    count = functools.reduce(jnp.add, [jnp.where(n, 1.0, 0.0) for n in named]).astype(jnp.bfloat16)
+    row = lax.broadcasted_iota(jnp.int32, (tokens, tokens), 0)
+    column = lax.broadcasted_iota(jnp.int32, (tokens, tokens), 1)
+    before = jnp.where(row < column, 1.0, 0.0).astype(jnp.bfloat16)
+    earlier = jnp.dot(count, before, preferred_element_type=jnp.float32)
+    slot_at = lax.broadcasted_iota(jnp.int32, (slots, tokens), 0)
+    taken = None
+    for k in range(topk):
+        place = jnp.sum(jnp.where(named[k], earlier, 0.0), axis=0, keepdims=True)
+        slot = ids_ref[k : k + 1] * capacity + place.astype(jnp.int32)
+        slots_ref[k : k + 1] = slot
+        taken = slot_at == slot if taken is None else taken | (slot_at == slot)
+    own = normed_ref[:, pl.ds(pl.multiple_of(lax.axis_index("tp") * cols, cols), cols)]
+    out_ref[...] = jnp.dot(
+        jnp.where(taken, 1.0, 0.0).astype(jnp.bfloat16), own, preferred_element_type=jnp.float32
+    ).astype(out_ref.dtype)
+
+
+def route(moe_input, moe_gain, route_ids, capacity, slots, cols):
+    tokens, width = moe_input.shape
+    vmem = pl.BlockSpec(memory_space=pltpu.VMEM)
+    return pl.pallas_call(
+        functools.partial(route_kernel, capacity),
+        out_shape=[
+            jax.ShapeDtypeStruct((slots, cols), jnp.bfloat16),
+            jax.ShapeDtypeStruct((tokens, width), jnp.bfloat16),
+            jax.ShapeDtypeStruct(route_ids.shape, jnp.int32),
+        ],
+        in_specs=[vmem] * 3,
+        out_specs=[vmem] * 3,
+        cost_estimate=pl.CostEstimate(
+            flops=2 * slots * tokens * cols, bytes_accessed=6 * moe_input.size, transcendentals=tokens
+        ),
+        name="route",
+    )(moe_input, moe_gain.reshape(1, width), route_ids)
+
+
+def silu_product(gate_sum, up_sum):
+    return (gate_sum / (1.0 + jnp.exp(-gate_sum)) * up_sum).astype(jnp.bfloat16)
+
+
+def experts_kernel(shared_ref, shared_down_ref, gate_ref, up_ref, down_ref, *refs):
+    pieces, (kept_ref, sent_ref) = refs[:-2], refs[-2:]
+    tp_index = lax.axis_index("tp")
+    core = lax.rem(tp_index, 2)
+    slots, cols = pieces[0].shape
+    gate_sum = up_sum = None
+    for mask, piece in enumerate(pieces):
+        at = pl.ds(pl.multiple_of((tp_index ^ mask) * cols, cols), cols)
+        gate = jnp.dot(piece[...], gate_ref[0, at], preferred_element_type=jnp.float32)
+        up = jnp.dot(piece[...], up_ref[0, at], preferred_element_type=jnp.float32)
+        gate_sum = gate if gate_sum is None else gate_sum + gate
+        up_sum = up if up_sum is None else up_sum + up
+    hidden = silu_product(gate_sum, up_sum)
+    for far in range(kept_ref.shape[0]):
+        for ref, near in ((kept_ref, core), (sent_ref, 1 - core)):
+            at = pl.ds(pl.multiple_of((2 * far + near) * cols, cols), cols)
+            ref[far, :slots] = jnp.dot(
+                hidden, down_ref[0, :, at], preferred_element_type=jnp.float32
+            ).astype(ref.dtype)
+            ref[far, slots:] = jnp.dot(
+                shared_ref[...], shared_down_ref[:, at], preferred_element_type=jnp.float32
+            ).astype(ref.dtype)
+
+
+def experts(shared_hidden, shared_down, gate, up, down, pieces):
+    slots, cols = pieces[0].shape
+    rows = slots + shared_hidden.shape[0]
+    vmem = pl.BlockSpec(memory_space=pltpu.VMEM)
+    shape = jax.ShapeDtypeStruct((len(pieces) // 2, rows, cols), jnp.bfloat16)
+    return pl.pallas_call(
+        experts_kernel,
+        out_shape=[shape, shape],
+        in_specs=[vmem] * (5 + len(pieces)),
+        out_specs=[vmem, vmem],
+        cost_estimate=pl.CostEstimate(
+            flops=6 * slots * gate.size + 2 * shared_hidden.size * shared_down.shape[1],
+            bytes_accessed=2 * (3 * gate.size + shared_down.size + 2 * rows * cols * len(pieces)),
+            transcendentals=slots * gate.shape[2],
+        ),
+        compiler_params=pltpu.CompilerParams(vmem_limit_bytes=30 * MIB),
+        name="experts",
+    )(shared_hidden, shared_down, gate, up, down, *pieces)
+
+
+def combine_kernel(common_ref, returned_ref, slots_ref, scores_ref, out_ref):
+    scores = scores_ref[...]
+    gates = scores / jnp.sum(scores, axis=0, keepdims=True) * ROUTED_SCALE
+    tokens = out_ref.shape[0]
+    slot_at = lax.broadcasted_iota(jnp.int32, (returned_ref.shape[0], tokens), 0)
+    share = jnp.zeros(slot_at.shape, jnp.float32)
+    for k in range(scores.shape[0]):
+        share = share + jnp.where(slot_at == slots_ref[k : k + 1], gates[k : k + 1], 0.0)
+    high = share.astype(jnp.bfloat16)
+    low = (share - high.astype(jnp.float32)).astype(jnp.bfloat16)
+    mix = common_ref[...]
+    for part in (high, low):
+        mix = mix + lax.dot_general(
+            part, returned_ref[...], (((0,), (0,)), ((), ())), preferred_element_type=jnp.float32
+        )
+    out_ref[...] = mix.astype(out_ref.dtype)
+
+
+def combine(common, returned, slot_ids, route_scores):
+    vmem = pl.BlockSpec(memory_space=pltpu.VMEM)
+    return pl.pallas_call(
+        combine_kernel,
+        out_shape=jax.ShapeDtypeStruct(common.shape, jnp.bfloat16),
+        in_specs=[vmem] * 4,
+        out_specs=vmem,
+        cost_estimate=pl.CostEstimate(
+            flops=4 * common.size * returned.shape[0],
+            bytes_accessed=6 * common.size + 2 * returned.size,
+            transcendentals=0,
+        ),
+        compiler_params=pltpu.CompilerParams(vmem_limit_bytes=8 * MIB),
+        name="combine",
+    )(common, returned, slot_ids, route_scores)
+
+
+def expert_layer_near(
+    moe_input,
+    moe_gain,
+    route_ids,
+    route_scores,
+    shared_gate,
+    shared_up,
+    shared_down,
+    expert_gate,
+    expert_up,
+    expert_down,
 ):
     ep_count = lax.axis_size("ep")
-    if SEQUENCE_COUNT == 1 and 2 * key_bias.shape[1] == ep_count and lax.axis_size("tp") % 2 == 0:
-        mixed = head_attention(queries, keys, values, key_bias, out_weight)
-    else:
-        mixed = row_attention(queries, keys, values, key_bias, out_weight)
-    return (mixed, expert_layer(*moe))
+    token_count, width = moe_input.shape
+    cols = width // lax.axis_size("tp")
+    expert_count = expert_gate.shape[0] * ep_count
+    capacity = 3 * token_count * route_ids.shape[1] // (2 * expert_count)
+    slots = expert_count * capacity
+    outgoing, normed, slot_ids = route(
+        moe_input, moe_gain, route_ids.T, capacity, slots, cols
+    )
+    arrived = lax.all_to_all(outgoing, "ep", split_axis=0, concat_axis=0, tiled=True)
+    pieces = gather_pieces(arrived)
+    shared_hidden = silu_product(
+        jnp.dot(normed, shared_gate, preferred_element_type=jnp.float32),
+        jnp.dot(normed, shared_up, preferred_element_type=jnp.float32),
+    )
+    kept, sent = experts(
+        shared_hidden, shared_down, expert_gate, expert_up, expert_down, pieces
+    )
+    summed = scatter_rest(kept, sent)
+    returned = lax.all_to_all(
+        summed[:slots].astype(jnp.bfloat16), "ep", split_axis=0, concat_axis=0, tiled=True
+    )
+    return combine(summed[slots:], returned, slot_ids, route_scores.T)
+
+
+def body(queries, keys, values, key_bias, out_weight, *moe):
+    ep_count, tp_count = lax.axis_size("ep"), lax.axis_size("tp")
+    span, width = queries.shape
+    heads = key_bias.shape[1]
+    cols = out_weight.shape[1] // tp_count
+    tokens = moe[0].shape[0]
+    slots = 3 * tokens * moe[2].shape[1] // 2
+    aligned = span % 512 == 0 and width % (128 * heads) == 0 and cols % 256 == 0 and slots % 16 == 0
+    near = SEQUENCE_COUNT == 1 and 2 * heads == ep_count and tp_count % 2 == 0 and aligned
+    if not near or moe[7].shape[0] != 1 or slots % ep_count or tokens % 128:
+        return (
+            row_attention(queries, keys, values, key_bias, out_weight),
+            expert_layer(*moe),
+        )
+    messages = pack(keys, values, queries, key_bias.T)
+    mixed = head_attention(messages, out_weight, heads)
+    return (mixed, expert_layer_near(*moe))
 
 
 def solution(mesh):

time: 173 us -> 147 us (0.85)
  local copies, waits for them, and re-layouts: 37.7 us -> 6.9 us
  matrix products: 21.3 us -> 2.73 us
  other arithmetic: 19.1 us -> 3.41 us
  waiting for transfers between devices: 28.2 us -> 42.9 us
  Pallas kernels: 29.2 us -> 42.6 us
  starting transfers between devices: 34.7 us -> 46.4 us
    dot_general x9 -> x2, matrix products: 21.3 us -> 2.73 us  [the longest x1 2.28 us: expert_layer_near(): jnp.dot(normed, shared_up, preferred_element_type=jnp.float32)]
    pallas_call x1 -> x9, Pallas kernels: 29.2 us -> 42.6 us  [the longest x2 25.6 us: stick(): pl.pallas_call(functools.partial(stick_kernel, width ** (-0.5) * LOG2E, l...]
    ppermute x0 -> x8, starting transfers between devices: none -> 13 us  [send_round(): return lax.ppermute(array, ('ep', 'tp'), pairs)]
    all_to_all x4 -> x2, starting transfers between devices: 22.8 us -> 11 us  [the longest x1 7.41 us: expert_layer_near(): lax.all_to_all(outgoing, 'ep', split_axis=0, concat_axis=0, tiled=True)]
    reshape x8 -> x0, local copies, waits for them, and re-layouts: 8.94 us -> none  [the longest x6 7.09 us: per_head(): return array.reshape(half, heads, depth).transpose(1, 0, 2)]
    select_n x3 -> x0, other arithmetic: 8.9 us -> none  [by_group(): jnp.where(core == 0, jnp.concatenate([own, other], axis), jnp.concatenate...]
    ppermute x14 -> x20, waiting for transfers between devices: 16.6 us -> 23.7 us  [swap(): lax.ppermute(array, axis, [(i, i ^ mask) for i in range(lax.axis_size(axi...]
    all_to_all x1 -> x2, starting transfers between devices: 3.63 us -> 10.2 us  [head_attention(): back = lax.all_to_all(out, 'ep', split_axis=0, concat_axis=0, tiled=True)]
  transfers between devices with their start and end apart: 19 -> 32, of which waited for: 6 -> 14; matrix products, arithmetic and copies ran while one was open for 39% -> 5% of each run, Pallas kernels for 17% -> 27%
where the time goes in v2:
time: 147 us; the launch traced here: 146 us
  starting transfers between devices  46.4 us (32%)
  waiting for transfers between devices  42.9 us (29%)
  Pallas kernels  42.6 us (29%)
  local copies, waits for them, and re-layouts  6.9 us (5%)
  other arithmetic  3.41 us (2%)
  matrix products  2.73 us (2%)
    pallas_call x2, Pallas kernels, stick(): pl.pallas_call(functools.partial(stick_kernel, width ** (-0.5) * LOG2E, l...  25.6 us
    ppermute x20, waiting for transfers between devices, swap(): lax.ppermute(array, axis, [(i, i ^ mask) for i in range(lax.axis_size(axi...  23.7 us
    ppermute x8, starting transfers between devices, send_round(): return lax.ppermute(array, ('ep', 'tp'), pairs)  13 us
    ppermute x20, starting transfers between devices, swap(): lax.ppermute(array, axis, [(i, i ^ mask) for i in range(lax.axis_size(axi...  12.2 us
    all_to_all x2, starting transfers between devices, head_attention(): back = lax.all_to_all(out, 'ep', split_axis=0, concat_axis=0, tiled=True)  10.2 us
    all_to_all x1, waiting for transfers between devices, expert_layer_near(): lax.all_to_all(outgoing, 'ep', split_axis=0, concat_axis=0, tiled=True)  8.34 us
    all_to_all x1, starting transfers between devices, expert_layer_near(): lax.all_to_all(outgoing, 'ep', split_axis=0, concat_axis=0, tiled=True)  7.41 us
    pallas_call x2, Pallas kernels, project(): pl.pallas_call(project_kernel, out_shape=[shape] * tp_count, in_specs=[vm...  5.97 us
  transfers between devices with their start and end apart: 32, of which 14 were waited for; matrix products, arithmetic and copies ran while one was open for 5% of the time, Pallas kernels for 27%

profile of v2, /device:TPU:0, one launch (start us, length us, event | category | flops | bytes accessed | tf_op | source)
XLA Modules:
  0.0 145.8 jit_solution(3386370459729166632)
XLA Ops:
  0.6 2.4 %route.1 = (bf16[384,512]{1,0:T(8,128)(2,1)}, bf16[128,2048]{1,0:T(8,128)(2,1)}, s32[2,128]{1,0:T(2,128)}) custom-call(bf16[128,2048]{1,0:T(8,128)(2,1)} %input_ref.1, f32[1,2048]{1,0:T(1,128)} %bitcast.21, s32[2,128]{1,0:T(2,128)} %bitcast.23), custom_call_target="tpu_custom_call" | custom-call | flops 50331648 | bytes 1572864 | tf_op jit(solution)/shard_map/route/pallas_call | solution.py:610
  3.1 7.4 %all-to-all-start.2 = ((bf16[8,48,512]{2,1,0:T(8,128)(2,1)}), bf16[8,48,512]{2,1,0:T(8,128)(2,1)S(1)}, u32[]{:S(2)}, u32[]{:S(2)}) async-start(bf16[8,48,512]{2,1,0:T(8,128)(2,1)} %bitcast.20), calls=%async_computation.2 | async-start | bytes 786432 | tf_op jit(solution)/shard_map/all_to_all | solution.py:730
  10.5 2.6 %pack.1 = (bf16[784,128]{1,0:T(8,128)(2,1)}, bf16[784,128]{1,0:T(8,128)(2,1)}, bf16[784,128]{1,0:T(8,128)(2,1)}, bf16[784,128]{1,0:T(8,128)(2,1)}, bf16[784,128]...) custom-call(bf16[512,512]{1,0:T(8,128)(2,1)} %k_ref.1, ...), custom_call_target="tpu_custom_call" | custom-call | flops 2097152 | bytes 3145728 | tf_op jit(solution)/shard_map/pack/pallas_call | solution.py:80
  14.7 3.4 %collective-permute-start.1 = (bf16[784,128]{1,0:T(8,128)(2,1)}, bf16[784,128]{1,0:T(8,128)(2,1)S(1)}, u32[]{:S(2)}, u32[]{:S(2)}) collective-permute-start(bf16[784,128]{1,0:T(8,128)(2,1)} %get-tuple-element.24), channel_id=1, source_target_pairs={{0,1},{1,17},{2,3},{3,19},{4,5},{5,21},{6,7},{7,23},{8,9},{9,25},{... | collective-permute-start | bytes 602120 | tf_op jit(solution)/shard_map/ppermute | solution.py:43
  18.1 8.3 %all-to-all-done.2 = bf16[8,48,512]{2,1,0:T(8,128)(2,1)S(1)} async-done(((bf16[8,48,512]{2,1,0:T(8,128)(2,1)}), bf16[8,48,512]{2,1,0:T(8,128)(2,1)S(1)}, u32[]{:S(2)}, u32[]{:S(2)}) %all-to-all-start.2) | async-done | bytes 393248 | tf_op jit(solution)/shard_map/all_to_all | solution.py:730
  28.8 2.3 %fusion.shared_ref = bf16[128,512]{1,0:T(8,128)(2,1)S(1)} fusion(bf16[128,2048]{1,0:T(8,128)(2,1)S(1)} %copy-done.10, bf16[2048,512]{1,0:T(8,128)(2,1)} %param.27, f32[128,512]{1,0:T(8,128)S(1)} %fusion.1), kind=kOutput, calls=%fused_computation.2 | convolution fusion | flops 268763136 | bytes 3014656 | tf_op jit(solution)/shard_map/dot_general | solution.py:734
  32.7 5.2 %collective-permute-done.25.refs_3_ = bf16[384,512]{1,0:T(8,128)(2,1)S(1)} collective-permute-done((bf16[384,512]{1,0:T(8,128)(2,1)S(1)}, bf16[384,512]{1,0:T(8,128)(2,1)S(1)}, u32[]{:S(2)}, u32[]{:S(2)}) %collective-permute-start.25) | collective-permute-done | bytes 393248 | tf_op jit(solution)/shard_map/ppermute | solution.py:27
  39.0 7.3 %collective-permute-done.24.refs_2_ = bf16[384,512]{1,0:T(8,128)(2,1)S(1)} collective-permute-done((bf16[384,512]{1,0:T(8,128)(2,1)S(1)}, bf16[384,512]{1,0:T(8,128)(2,1)S(1)}, u32[]{:S(2)}, u32[]{:S(2)}) %collective-permute-start.24) | collective-permute-done | bytes 393248 | tf_op jit(solution)/shard_map/ppermute | solution.py:27
  48.9 3.9 %experts.1 = (bf16[2,512,512]{2,1,0:T(8,128)(2,1)S(1)}, bf16[2,512,512]{2,1,0:T(8,128)(2,1)}) custom-call(bf16[128,512]{1,0:T(8,128)(2,1)S(1)} %fusion.shared_ref, bf16[512,2048]{1,0:T(8,128)(2,1)S(1)} %copy-done.1, bf16[1,2048,512]{2,1,0:T(8,128)(2,1)S(1)} %copy-done.2, bf16[1,2048,512]{2,1,0:T(8,128)(2,1)S(1)} %copy-done.3, ...), custom_call_target="tpu_custom_call" | custom-call | flops 2684354560 | bytes 12582912 | tf_op jit(solution)/shard_map/experts/pallas_call | solution.py:659
  54.6 2.8 %collective-permute-start.6 = (bf16[784,128]{1,0:T(8,128)(2,1)S(1)}, bf16[784,128]{1,0:T(8,128)(2,1)S(1)}, u32[]{:S(2)}, u32[]{:S(2)}) collective-permute-start(bf16[784,128]{1,0:T(8,128)(2,1)S(1)} %copy-done.20), channel_id=1, source_target_pairs={{0,12},{1,28},{2,14},{3,30},{4,0},{5,16},{6,2},{7,18},{8,4},{9,20}... | collective-permute-start | bytes 602120 | tf_op jit(solution)/shard_map/ppermute | solution.py:43
  59.5 3.3 %collective-permute-done.6.refs_6_ = bf16[784,128]{1,0:T(8,128)(2,1)S(1)} collective-permute-done((bf16[784,128]{1,0:T(8,128)(2,1)S(1)}, bf16[784,128]{1,0:T(8,128)(2,1)S(1)}, u32[]{:S(2)}, u32[]{:S(2)}) %collective-permute-start.6) | collective-permute-done | bytes 200736 | tf_op jit(solution)/shard_map/ppermute | solution.py:43
  62.8 3.1 %collective-permute-start.10 = (bf16[784,128]{1,0:T(8,128)(2,1)S(1)}, bf16[784,128]{1,0:T(8,128)(2,1)S(1)}, u32[]{:S(2)}, u32[]{:S(2)}) collective-permute-start(bf16[784,128]{1,0:T(8,128)(2,1)S(1)} %collective-permute-done.2.refs_2_), channel_id=1, source_target_pairs={{0,1},{1,0},{2,3},{3,2},{4,5},{5,4},{6,7},{7,6},{8,9},{9,8},{10,11... | collective-permute-start | bytes 602120 | tf_op jit(solution)/shard_map/ppermute | solution.py:27
  65.9 2.4 %collective-permute-done.7.refs_7_ = bf16[784,128]{1,0:T(8,128)(2,1)} collective-permute-done((bf16[784,128]{1,0:T(8,128)(2,1)S(1)}, bf16[784,128]{1,0:T(8,128)(2,1)}, u32[]{:S(2)}, u32[]{:S(2)}) %collective-permute-start.7) | collective-permute-done | bytes 200736 | tf_op jit(solution)/shard_map/ppermute | solution.py:43
  70.5 3.2 %collective-permute-done.13.refs_13_ = bf16[784,128]{1,0:T(8,128)(2,1)} collective-permute-done((bf16[784,128]{1,0:T(8,128)(2,1)}, bf16[784,128]{1,0:T(8,128)(2,1)}, u32[]{:S(2)}, u32[]{:S(2)}) %collective-permute-start.13) | collective-permute-done | bytes 200736 | tf_op jit(solution)/shard_map/ppermute | solution.py:27
  74.3 12.8 %shard_map.176 = bf16[8,128,128]{2,1,0:T(8,128)(2,1)} custom-call(s32[1,44]{1,0:T(1,128)} %constant.20.clone.table_ref, bf16[784,128]{1,0:T(8,128)(2,1)} %copy-done.11, bf16[784,128]{1,0:T(8,128)(2,1)} %copy-done.12, bf16[784,128]{1,0:T(8,128)(2,1)} %copy-done.13, bf16[784,128]{1,0:T(8,128)(2,1)} %copy-done.14, bf16[784,128]{1,0:T(8,128)(2,1)} %copy-done.15, ...), custom_call_target="tpu_custom_call" | custom-call | flops 3355443200 | bytes 2621440 | tf_op jit(solution)/shard_map/pallas_call | solution.py:227
  87.1 4.1 %all-to-all-start = ((bf16[8,128,128]{2,1,0:T(8,128)(2,1)}), bf16[8,128,128]{2,1,0:T(8,128)(2,1)S(1)}, u32[]{:S(2)}, u32[]{:S(2)}) async-start(bf16[8,128,128]{2,1,0:T(8,128)(2,1)} %shard_map.176), calls=%async_computation | async-start | bytes 524288 | tf_op jit(solution)/shard_map/all_to_all | solution.py:342
  91.2 1.9 %convert_add_fusion = f32[2,512,512]{2,1,0:T(8,128)S(1)} fusion(bf16[2,512,512]{2,1,0:T(8,128)(2,1)} %collective-permute-done.26, bf16[2,512,512]{2,1,0:T(8,128)(2,1)} %copy-done.5), kind=kLoop, calls=%fused_computation | loop fusion | flops 1572864 | bytes 4194304 | tf_op jit(solution)/shard_map/add | solution.py:569
  95.0 12.8 %shard_map.177 = bf16[8,128,128]{2,1,0:T(8,128)(2,1)} custom-call(s32[1,44]{1,0:T(1,128)} %constant.20.clone.table_ref, bf16[784,128]{1,0:T(8,128)(2,1)} %copy-done.11, bf16[784,128]{1,0:T(8,128)(2,1)} %copy-done.12, bf16[784,128]{1,0:T(8,128)(2,1)} %copy-done.13, bf16[784,128]{1,0:T(8,128)(2,1)} %copy-done.14, bf16[784,128]{1,0:T(8,128)(2,1)} %copy-done.15, ...), custom_call_target="tpu_custom_call" | custom-call | flops 3355443200 | bytes 2621440 | tf_op jit(solution)/shard_map/pallas_call | solution.py:227
  107.9 6.0 %all-to-all-start.1 = ((bf16[8,128,128]{2,1,0:T(8,128)(2,1)}), bf16[8,128,128]{2,1,0:T(8,128)(2,1)S(1)}, u32[]{:S(2)}, u32[]{:S(2)}) async-start(bf16[8,128,128]{2,1,0:T(8,128)(2,1)} %shard_map.177), calls=%async_computation.1 | async-start | bytes 524288 | tf_op jit(solution)/shard_map/all_to_all | solution.py:342
  117.2 5.2 %all-to-all-done.1.back_ref = bf16[8,128,128]{2,1,0:T(8,128)(2,1)S(1)} async-done(((bf16[8,128,128]{2,1,0:T(8,128)(2,1)}), bf16[8,128,128]{2,1,0:T(8,128)(2,1)S(1)}, u32[]{:S(2)}, u32[]{:S(2)}) %all-to-all-start.1) | async-done | bytes 262176 | tf_op jit(solution)/shard_map/all_to_all | solution.py:342
  122.4 3.6 %all-to-all-start.3 = ((bf16[8,48,512]{2,1,0:T(8,128)(2,1)}), bf16[8,48,512]{2,1,0:T(8,128)(2,1)S(1)}, u32[]{:S(2)}, u32[]{:S(2)}) async-start(bf16[8,48,512]{2,1,0:T(8,128)(2,1)} %bitcast.6), calls=%async_computation.3 | async-start | bytes 786432 | tf_op jit(solution)/shard_map/all_to_all | solution.py:740
  126.0 3.0 %project.3 = (bf16[128,512]{1,0:T(8,128)(2,1)S(1)}, bf16[128,512]{1,0:T(8,128)(2,1)S(1)}, bf16[128,512]{1,0:T(8,128)(2,1)S(1)}, bf16[128,512]{1,0:T(8,128)(2,1)S(1)}) custom-call(bf16[8,128,128]{2,1,0:T(8,128)(2,1)S(1)} %all-to-all-done.1.back_ref, bf16[512,2048]{1,0:T(8,128)(2,1)} %own_ref.3, bf16[512,2048]{1,0:T(8,128)(2,1)} %collective-permute-done.16.other_ref), custom_call_target="tpu_custom_call" | custom-call | flops 536870912 | bytes 5242880 | tf_op jit(solution)/shard_map/project/pallas_call | solution.py:278
  130.9 3.0 %project.2 = (bf16[128,512]{1,0:T(8,128)(2,1)S(1)}, bf16[128,512]{1,0:T(8,128)(2,1)S(1)}, bf16[128,512]{1,0:T(8,128)(2,1)S(1)}, bf16[128,512]{1,0:T(8,128)(2,1)S(1)}) custom-call(bf16[8,128,128]{2,1,0:T(8,128)(2,1)S(1)} %all-to-all-done.back_ref, bf16[512,2048]{1,0:T(8,128)(2,1)} %own_ref.3, bf16[512,2048]{1,0:T(8,128)(2,1)} %collective-permute-done.16.other_ref), custom_call_target="tpu_custom_call" | custom-call | flops 536870912 | bytes 5242880 | tf_op jit(solution)/shard_map/project/pallas_call | solution.py:278
  137.5 3.7 %collective-permute-done.18.refs_2_ = bf16[128,512]{1,0:T(8,128)(2,1)S(1)} collective-permute-done((bf16[128,512]{1,0:T(8,128)(2,1)S(1)}, bf16[128,512]{1,0:T(8,128)(2,1)S(1)}, u32[]{:S(2)}, u32[]{:S(2)}) %collective-permute-start.18) | collective-permute-done | bytes 131104 | tf_op jit(solution)/shard_map/ppermute | solution.py:27
  (104 shorter events, 31.0 us)
Async XLA Ops:
  3.1 23.4 %all-to-all-start.2 = ((bf16[8,48,512]{2,1,0:T(8,128)(2,1)}), bf16[8,48,512]{2,1,0:T(8,128)(2,1)S(1)}, u32[]{:S(2)}, u32[]{:S(2)}) async-start(bf16[8,48,512]{2,1,0:T(8,128)(2,1)} %bitcast.20), calls=%async_computation.2 | async-start | bytes 786432 | tf_op jit(solution)/shard_map/all_to_all | solution.py:730
  13.1 18.0 %collective-permute-start = (bf16[784,128]{1,0:T(8,128)(2,1)}, bf16[784,128]{1,0:T(8,128)(2,1)S(1)}, u32[]{:S(2)}, u32[]{:S(2)}) collective-permute-start(bf16[784,128]{1,0:T(8,128)(2,1)} %get-tuple-element.23), channel_id=1, source_target_pairs={{0,0},{1,16},{2,2},{3,18},{4,4},{5,20},{6,6},{7,22},{8,8},{9,24},{... | collective-permute-start | bytes 602120 | tf_op jit(solution)/shard_map/ppermute | solution.py:43
  14.7 39.1 %collective-permute-start.1 = (bf16[784,128]{1,0:T(8,128)(2,1)}, bf16[784,128]{1,0:T(8,128)(2,1)S(1)}, u32[]{:S(2)}, u32[]{:S(2)}) collective-permute-start(bf16[784,128]{1,0:T(8,128)(2,1)} %get-tuple-element.24), channel_id=1, source_target_pairs={{0,1},{1,17},{2,3},{3,19},{4,5},{5,21},{6,7},{7,23},{8,9},{9,25},{... | collective-permute-start | bytes 602120 | tf_op jit(solution)/shard_map/ppermute | solution.py:43
  26.5 11.3 %collective-permute-start.25 = (bf16[384,512]{1,0:T(8,128)(2,1)S(1)}, bf16[384,512]{1,0:T(8,128)(2,1)S(1)}, u32[]{:S(2)}, u32[]{:S(2)}) collective-permute-start(bf16[384,512]{1,0:T(8,128)(2,1)S(1)} %bitcast.14), channel_id=1, source_target_pairs={{0,3},{1,2},{2,1},{3,0},{4,7},{5,6},{6,5},{7,4},{8,11},{9,10},{10,... | collective-permute-start | bytes 1179656 | tf_op jit(solution)/shard_map/ppermute | solution.py:27
  26.5 19.8 %collective-permute-start.24 = (bf16[384,512]{1,0:T(8,128)(2,1)S(1)}, bf16[384,512]{1,0:T(8,128)(2,1)S(1)}, u32[]{:S(2)}, u32[]{:S(2)}) collective-permute-start(bf16[384,512]{1,0:T(8,128)(2,1)S(1)} %bitcast.15), channel_id=1, source_target_pairs={{0,2},{1,3},{2,0},{3,1},{4,6},{5,7},{6,4},{7,5},{8,10},{9,11},{10,... | collective-permute-start | bytes 1179656 | tf_op jit(solution)/shard_map/ppermute | solution.py:27
  28.0 19.2 %collective-permute-start.23 = (bf16[384,512]{1,0:T(8,128)(2,1)S(1)}, bf16[384,512]{1,0:T(8,128)(2,1)S(1)}, u32[]{:S(2)}, u32[]{:S(2)}) collective-permute-start(bf16[384,512]{1,0:T(8,128)(2,1)S(1)} %bitcast.16), channel_id=1, source_target_pairs={{0,1},{1,0},{2,3},{3,2},{4,5},{5,4},{6,7},{7,6},{8,9},{9,8},{10,11... | collective-permute-start | bytes 1179656 | tf_op jit(solution)/shard_map/ppermute | solution.py:27
  31.1 23.5 %collective-permute-start.2 = (bf16[784,128]{1,0:T(8,128)(2,1)}, bf16[784,128]{1,0:T(8,128)(2,1)S(1)}, u32[]{:S(2)}, u32[]{:S(2)}) collective-permute-start(bf16[784,128]{1,0:T(8,128)(2,1)} %get-tuple-element.25), channel_id=1, source_target_pairs={{0,4},{1,20},{2,6},{3,22},{4,8},{5,24},{6,10},{7,26},{8,12},{9,28}... | collective-permute-start | bytes 602120 | tf_op jit(solution)/shard_map/ppermute | solution.py:43
  37.8 19.6 %collective-permute-start.3 = (bf16[784,128]{1,0:T(8,128)(2,1)}, bf16[784,128]{1,0:T(8,128)(2,1)S(1)}, u32[]{:S(2)}, u32[]{:S(2)}) collective-permute-start(bf16[784,128]{1,0:T(8,128)(2,1)} %get-tuple-element.26), channel_id=1, source_target_pairs={{0,5},{1,21},{2,7},{3,23},{4,9},{5,25},{6,11},{7,27},{8,13},{9,29}... | collective-permute-start | bytes 602120 | tf_op jit(solution)/shard_map/ppermute | solution.py:43
  46.3 12.6 %collective-permute-start.4 = (bf16[784,128]{1,0:T(8,128)(2,1)}, bf16[784,128]{1,0:T(8,128)(2,1)S(1)}, u32[]{:S(2)}, u32[]{:S(2)}) collective-permute-start(bf16[784,128]{1,0:T(8,128)(2,1)} %get-tuple-element.27), channel_id=1, source_target_pairs={{0,8},{1,24},{2,10},{3,26},{4,12},{5,28},{6,14},{7,30},{8,0},{9,16... | collective-permute-start | bytes 602120 | tf_op jit(solution)/shard_map/ppermute | solution.py:43
  47.3 11.9 %collective-permute-start.5 = (bf16[784,128]{1,0:T(8,128)(2,1)}, bf16[784,128]{1,0:T(8,128)(2,1)}, u32[]{:S(2)}, u32[]{:S(2)}) collective-permute-start(bf16[784,128]{1,0:T(8,128)(2,1)} %get-tuple-element.28), channel_id=1, source_target_pairs={{0,9},{1,25},{2,11},{3,27},{4,13},{5,29},{6,15},{7,31},{8,1},{9,17... | collective-permute-start | bytes 602120 | tf_op jit(solution)/shard_map/ppermute | solution.py:43
  53.8 37.4 %collective-permute-start.26 = (bf16[2,512,512]{2,1,0:T(8,128)(2,1)}, bf16[2,512,512]{2,1,0:T(8,128)(2,1)}, u32[]{:S(2)}, u32[]{:S(2)}) collective-permute-start(bf16[2,512,512]{2,1,0:T(8,128)(2,1)} %get-tuple-element.42), channel_id=1, source_target_pairs={{0,1},{1,0},{2,3},{3,2},{4,5},{5,4},{6,7},{7,6},{8,9},{9,8},{10,11... | collective-permute-start | bytes 3145736 | tf_op jit(solution)/shard_map/ppermute | solution.py:27
  54.6 8.2 %collective-permute-start.6 = (bf16[784,128]{1,0:T(8,128)(2,1)S(1)}, bf16[784,128]{1,0:T(8,128)(2,1)S(1)}, u32[]{:S(2)}, u32[]{:S(2)}) collective-permute-start(bf16[784,128]{1,0:T(8,128)(2,1)S(1)} %copy-done.20), channel_id=1, source_target_pairs={{0,12},{1,28},{2,14},{3,30},{4,0},{5,16},{6,2},{7,18},{8,4},{9,20}... | collective-permute-start | bytes 602120 | tf_op jit(solution)/shard_map/ppermute | solution.py:43
  57.4 10.9 %collective-permute-start.7 = (bf16[784,128]{1,0:T(8,128)(2,1)S(1)}, bf16[784,128]{1,0:T(8,128)(2,1)}, u32[]{:S(2)}, u32[]{:S(2)}) collective-permute-start(bf16[784,128]{1,0:T(8,128)(2,1)S(1)} %copy-done.18), channel_id=1, source_target_pairs={{0,13},{1,29},{2,15},{3,31},{4,1},{5,17},{6,3},{7,19},{8,5},{9,21}... | collective-permute-start | bytes 602120 | tf_op jit(solution)/shard_map/ppermute | solution.py:43
  59.0 9.4 %collective-permute-start.8 = (bf16[784,128]{1,0:T(8,128)(2,1)S(1)}, bf16[784,128]{1,0:T(8,128)(2,1)S(1)}, u32[]{:S(2)}, u32[]{:S(2)}) collective-permute-start(bf16[784,128]{1,0:T(8,128)(2,1)S(1)} %collective-permute-done.refs_0_), channel_id=1, source_target_pairs={{0,1},{1,0},{2,3},{3,2},{4,5},{5,4},{6,7},{7,6},{8,9},{9,8},{10,11... | collective-permute-start | bytes 602120 | tf_op jit(solution)/shard_map/ppermute | solution.py:27
  59.2 9.7 %collective-permute-start.9 = (bf16[784,128]{1,0:T(8,128)(2,1)S(1)}, bf16[784,128]{1,0:T(8,128)(2,1)S(1)}, u32[]{:S(2)}, u32[]{:S(2)}) collective-permute-start(bf16[784,128]{1,0:T(8,128)(2,1)S(1)} %collective-permute-done.1.refs_1_), channel_id=1, source_target_pairs={{0,1},{1,0},{2,3},{3,2},{4,5},{5,4},{6,7},{7,6},{8,9},{9,8},{10,11... | collective-permute-start | bytes 602120 | tf_op jit(solution)/shard_map/ppermute | solution.py:27
  68.9 57.1 %collective-permute-start.16 = (bf16[512,2048]{1,0:T(8,128)(2,1)}, bf16[512,2048]{1,0:T(8,128)(2,1)}, u32[]{:S(2)}, u32[]{:S(2)}) collective-permute-start(bf16[512,2048]{1,0:T(8,128)(2,1)} %own_ref.3), channel_id=1, source_target_pairs={{0,1},{1,0},{2,3},{3,2},{4,5},{5,4},{6,7},{7,6},{8,9},{9,8},{10,11... | collective-permute-start | bytes 6291464 | tf_op jit(solution)/shard_map/ppermute | solution.py:27
  87.1 20.7 %all-to-all-start = ((bf16[8,128,128]{2,1,0:T(8,128)(2,1)}), bf16[8,128,128]{2,1,0:T(8,128)(2,1)S(1)}, u32[]{:S(2)}, u32[]{:S(2)}) async-start(bf16[8,128,128]{2,1,0:T(8,128)(2,1)} %shard_map.176), calls=%async_computation | async-start | bytes 524288 | tf_op jit(solution)/shard_map/all_to_all | solution.py:342
  94.6 19.3 %collective-permute-start.27 = (bf16[1,512,512]{2,1,0:T(8,128)(2,1)S(1)}, bf16[1,512,512]{2,1,0:T(8,128)(2,1)}, u32[]{:S(2)}, u32[]{:S(2)}) collective-permute-start(bf16[1,512,512]{2,1,0:T(8,128)(2,1)S(1)} %dynamic-slice_convert_fusion), channel_id=1, source_target_pairs={{0,2},{1,3},{2,0},{3,1},{4,6},{5,7},{6,4},{7,5},{8,10},{9,11},{10,... | collective-permute-start | bytes 1572872 | tf_op jit(solution)/shard_map/ppermute | solution.py:27
  107.9 14.6 %all-to-all-start.1 = ((bf16[8,128,128]{2,1,0:T(8,128)(2,1)}), bf16[8,128,128]{2,1,0:T(8,128)(2,1)S(1)}, u32[]{:S(2)}, u32[]{:S(2)}) async-start(bf16[8,128,128]{2,1,0:T(8,128)(2,1)} %shard_map.177), calls=%async_computation.1 | async-start | bytes 524288 | tf_op jit(solution)/shard_map/all_to_all | solution.py:342
  122.4 22.3 %all-to-all-start.3 = ((bf16[8,48,512]{2,1,0:T(8,128)(2,1)}), bf16[8,48,512]{2,1,0:T(8,128)(2,1)S(1)}, u32[]{:S(2)}, u32[]{:S(2)}) async-start(bf16[8,48,512]{2,1,0:T(8,128)(2,1)} %bitcast.6), calls=%async_computation.3 | async-start | bytes 786432 | tf_op jit(solution)/shard_map/all_to_all | solution.py:740
  129.0 7.0 %collective-permute-start.20 = (bf16[128,512]{1,0:T(8,128)(2,1)S(1)}, bf16[128,512]{1,0:T(8,128)(2,1)S(1)}, u32[]{:S(2)}, u32[]{:S(2)}) collective-permute-start(bf16[128,512]{1,0:T(8,128)(2,1)S(1)} %get-tuple-element.36), channel_id=1, source_target_pairs={{0,1},{1,0},{2,3},{3,2},{4,5},{5,4},{6,7},{7,6},{8,9},{9,8},{10,11... | collective-permute-start | bytes 393224 | tf_op jit(solution)/shard_map/ppermute | solution.py:27
  129.1 6.9 %collective-permute-start.21 = (bf16[128,512]{1,0:T(8,128)(2,1)S(1)}, bf16[128,512]{1,0:T(8,128)(2,1)S(1)}, u32[]{:S(2)}, u32[]{:S(2)}) collective-permute-start(bf16[128,512]{1,0:T(8,128)(2,1)S(1)} %get-tuple-element.37), channel_id=1, source_target_pairs={{0,2},{1,3},{2,0},{3,1},{4,6},{5,7},{6,4},{7,5},{8,10},{9,11},{10,... | collective-permute-start | bytes 393224 | tf_op jit(solution)/shard_map/ppermute | solution.py:27
  134.4 6.8 %collective-permute-start.18 = (bf16[128,512]{1,0:T(8,128)(2,1)S(1)}, bf16[128,512]{1,0:T(8,128)(2,1)S(1)}, u32[]{:S(2)}, u32[]{:S(2)}) collective-permute-start(bf16[128,512]{1,0:T(8,128)(2,1)S(1)} %get-tuple-element.33), channel_id=1, source_target_pairs={{0,2},{1,3},{2,0},{3,1},{4,6},{5,7},{6,4},{7,5},{8,10},{9,11},{10,... | collective-permute-start | bytes 393224 | tf_op jit(solution)/shard_map/ppermute | solution.py:27
  136.0 6.9 %collective-permute-start.19 = (bf16[128,512]{1,0:T(8,128)(2,1)S(1)}, bf16[128,512]{1,0:T(8,128)(2,1)S(1)}, u32[]{:S(2)}, u32[]{:S(2)}) collective-permute-start(bf16[128,512]{1,0:T(8,128)(2,1)S(1)} %get-tuple-element.34), channel_id=1, source_target_pairs={{0,3},{1,2},{2,1},{3,0},{4,7},{5,6},{6,5},{7,4},{8,11},{9,10},{10,... | collective-permute-start | bytes 393224 | tf_op jit(solution)/shard_map/ppermute | solution.py:27
  (32 other events, 299.3 us)

commit v3 on v2

--- a/solution.py
+++ b/solution.py
@@ -90,20 +90,21 @@
     )(keys, values, queries, bias)
 
 
-def steps_of(groups, turns):
-    steps = [(g, source) for g in range(groups) for source in reversed(range((g + 1) * turns))]
-    return steps + [(groups, 0)] * 2
-
-
-def stick_kernel(scale, heads, turn, turns, spot, table_ref, *refs):
+def steps_of(blocks):
+    steps = [(block, source) for block in range(blocks) for source in reversed(range(block + 1))]
+    return steps + [(blocks, 0)] * (2 + len(steps) % 2)
+
+
+def stick_kernel(scale, heads, turns, spot, table_ref, *refs):
     count = 2 * heads
-    messages, out_ref = refs[: 2 * count], refs[2 * count]
-    mes_s, q_s, b_s, tri_s, reach_s, soft_s, log_s, prod_s, acc_s, carry_s, sems = refs[2 * count + 1 :]
-    blocks, piece, width = out_ref.shape
-    groups = blocks // turns
-    rows = piece * turns
+    messages, out_refs = refs[: 2 * count], refs[2 * count : 2 * count + turns]
+    mes_s, q_s, b_s, tri_s, reach_s, soft_s, log_s, prod_s, acc_s, carry_s, sems = refs[
+        2 * count + turns :
+    ]
+    _, blocks, length, width = mes_s.shape
+    rows = turns * out_refs[0].shape[1]
     bias_rows = rows // width
-    pad = mes_s.shape[2] - 3 * rows
+    pad = length - 3 * rows
     place, mine = spot()
     for at, which in enumerate((mine, 1 - mine)):
         for (k, s), ref in zip(rounds_of(heads), messages[at * count : (at + 1) * count]):
@@ -113,35 +114,23 @@
     column = lax.broadcasted_iota(jnp.int32, (2 * rows, rows), 1)
     tri_s[...] = jnp.where(later > column, 1.0, 0.0).astype(jnp.bfloat16)
     row = lax.broadcasted_iota(jnp.int32, (rows, rows), 0)
-    row = row // piece * (2 * rows) + row % piece + (mine * rows + turn * piece)
-    reach_s[...] = lax.broadcasted_iota(jnp.int32, (rows, rows), 1) - row
-    query_at = 2 * rows + pad + turn * piece
-
-    def arrive(group):
-        for at in range(turns):
-            block = group * turns + at
-            for which in (0, 1):
-                pltpu.make_async_copy(
-                    messages[0], mes_s.at[which, block], sems.at[which, block]
-                ).wait()
-                lanes = [
-                    mes_s[which, block, 2 * rows + r : 2 * rows + r + 1, :].astype(jnp.float32)
-                    for r in range(bias_rows)
-                ]
-                b_s[which, block] = jnp.concatenate(lanes, axis=1) * LOG2E
-            q_s[group, at * piece : (at + 1) * piece] = mes_s[
-                mine, block, query_at : query_at + piece
+    reach_s[...] = lax.broadcasted_iota(jnp.int32, (rows, rows), 1) - row - mine * rows
+    for block in range(blocks):
+        for which in (0, 1):
+            pltpu.make_async_copy(messages[0], mes_s.at[which, block], sems.at[which, block]).wait()
+            lanes = [
+                mes_s[which, block, 2 * rows + r : 2 * rows + r + 1, :].astype(jnp.float32)
+                for r in range(bias_rows)
             ]
-
-    arrive(0)
-    arrive(1)
-    q_s[groups] = q_s[0]
+            b_s[which, block] = jnp.concatenate(lanes, axis=1) * LOG2E
+        q_s[block] = mes_s[mine, block, 2 * rows + pad :]
+    q_s[blocks] = q_s[0]
     parts = (1, 0)
 
-    def scores(group, source):
+    def scores(block, source):
         return [
             lax.dot_general(
-                q_s[group],
+                q_s[block],
                 mes_s[part, source, :rows],
                 (((1,), (1,)), ((), ())),
                 preferred_element_type=jnp.float32,
@@ -149,8 +138,8 @@
             for part in parts
         ]
 
-    def soften(slot, group, source):
-        ahead = (group * turns - source) * (2 * rows)
+    def soften(slot, block, source):
+        ahead = (block - source) * (2 * rows)
         for part in parts:
             logit = prod_s[part] * scale + b_s[part, source]
             logit = jnp.where(reach_s[...] < ahead - part * rows, logit, NEVER)
@@ -179,60 +168,53 @@
         carry = carry_s[...]
         for slot in range(2):
             t = 2 * at + slot
+            soften(1 - slot, *entry(t + 1))
+            products = scores(*entry(t + 2))
             totals = sums(slot)
-            products = scores(*entry(t + 2))
-            soften(1 - slot, *entry(t + 1))
             put(products)
             wide = jnp.concatenate([carry] * bias_rows, axis=1)
-            source = entry(t)[1]
+            block, source = entry(t)
             for part, total in zip(parts, totals):
                 weight = jnp.exp2(log_s[slot, part] - (total + wide)).astype(jnp.bfloat16)
                 values = mes_s[part, source, rows : 2 * rows]
                 acc = acc + jnp.dot(weight, values, preferred_element_type=jnp.float32)
             whole = totals[1][:, :1] + soft_s[slot, 0, :, :width].astype(jnp.float32)[:, :1]
             carry = carry + jnp.broadcast_to(whole, (rows, width))
+            for turn, out_ref in enumerate(out_refs):
+                piece = out_ref.shape[1]
+                out_ref[block] = acc[turn * piece : (turn + 1) * piece].astype(out_ref.dtype)
+            more = source > 0
+            acc = jnp.where(more, acc, 0.0)
+            carry = jnp.where(more, carry, 0.0)
         acc_s[...] = acc
         carry_s[...] = carry
-        group = entry(2 * at)[0]
-
-        @pl.when(group != entry(2 * at + 2)[0])
-        def _():
-            for turn_at in range(turns):
-                part = acc_s[turn_at * piece : (turn_at + 1) * piece]
-                out_ref[group * turns + turn_at] = part.astype(out_ref.dtype)
-            acc_s[...] = jnp.zeros_like(acc_s)
-            carry_s[...] = jnp.zeros_like(carry_s)
-
-            @pl.when(group + 2 < groups)
-            def _():
-                arrive(group + 2)
-
         return 0
 
     acc_s[...] = jnp.zeros_like(acc_s)
     carry_s[...] = jnp.zeros_like(carry_s)
-    lax.fori_loop(0, table_ref.shape[1] // 4 - 1, pair, 0)
+    pairs = table_ref.shape[1] // 4 - 1
+    unroll = max(u for u in range(1, 10) if pairs % u == 0)
+    lax.fori_loop(0, pairs, pair, 0, unroll=unroll)
 
 
 def here():
     return lax.axis_index("ep"), lax.rem(lax.axis_index("tp"), 2)
 
 
-def stick(own, other, blocks, rows, width, turn, turns, spot=here):
+def stick(own, other, blocks, rows, width, turns, spot=here):
     length = own[0].shape[0]
-    groups = blocks // turns
-    piece = rows // turns
-    table = np.array(steps_of(groups, turns), np.int32).reshape(1, -1)
+    table = np.array(steps_of(blocks), np.int32).reshape(1, -1)
     pairs = 2 * rows * rows * (table.shape[1] // 2 - 2)
+    shape = jax.ShapeDtypeStruct((blocks, rows // turns, width), jnp.bfloat16)
     return pl.pallas_call(
-        functools.partial(stick_kernel, width**-0.5 * LOG2E, len(own) // 2, turn, turns, spot),
-        out_shape=jax.ShapeDtypeStruct((blocks, piece, width), jnp.bfloat16),
+        functools.partial(stick_kernel, width**-0.5 * LOG2E, len(own) // 2, turns, spot),
+        out_shape=[shape] * turns,
         in_specs=[pl.BlockSpec(memory_space=pltpu.SMEM)]
         + [pl.BlockSpec(memory_space=pl.ANY)] * (2 * len(own)),
-        out_specs=pl.BlockSpec(memory_space=pltpu.VMEM),
+        out_specs=[pl.BlockSpec(memory_space=pltpu.VMEM)] * turns,
         scratch_shapes=[
             pltpu.VMEM((2, blocks, length, width), jnp.bfloat16),
-            pltpu.VMEM((groups + 1, rows, width), jnp.bfloat16),
+            pltpu.VMEM((blocks + 1, rows, width), jnp.bfloat16),
             pltpu.VMEM((2, blocks, 1, rows), jnp.float32),
             pltpu.VMEM((2 * rows, rows), jnp.bfloat16),
             pltpu.VMEM((rows, rows), jnp.int32),
@@ -248,47 +230,54 @@
             bytes_accessed=10 * blocks * rows * width,
             transcendentals=3 * pairs,
         ),
+        name="stick",
     )(jnp.asarray(table), *own, *other)
 
 
-def project_kernel(back_ref, own_ref, other_ref, first_ref, *rest):
-    out_refs, rows_s = rest[:-1], rest[-1]
-    tp_index = lax.axis_index("tp")
+def project_kernel(masks, own_ref, other_ref, *refs):
+    count = len(masks)
+    back_refs, out_refs, rows_s = refs[: -count - 1], refs[-count - 1 : -1], refs[-1]
+    ep_index, tp_index = lax.axis_index("ep"), lax.axis_index("tp")
     core = lax.rem(tp_index, 2)
-    heads, _, depth = back_ref.shape
     width = own_ref.shape[0]
-    cols = first_ref.shape[1]
+    cols = out_refs[0].shape[1]
+    depth = back_refs[0].shape[-1]
+    heads = rows_s.shape[1] // depth
     for head in range(heads):
-        rows_s[head * depth // width, :, head * depth % width : (head * depth % width) + depth] = back_ref[head]
-    own_rows = rows_s[core]
-    other_rows = rows_s[1 - core]
-    for mask in range(len(out_refs), -1, -1):
+        if len(back_refs) == 1:
+            rows_s[:, head * depth : (head + 1) * depth] = back_refs[0][head]
+        else:
+            at = pl.ds(pl.multiple_of((ep_index ^ head) * depth, depth), depth)
+            ref = back_refs[head]
+            rows_s[:, at] = ref[...] if head else ref[ep_index]
+    own_rows = rows_s[:, pl.ds(pl.multiple_of(core * width, width), width)]
+    other_rows = rows_s[:, pl.ds(pl.multiple_of((1 - core) * width, width), width)]
+    for mask, out_ref in zip(masks, out_refs):
         at = pl.ds(pl.multiple_of((tp_index ^ mask) * cols, cols), cols)
         part = jnp.dot(own_rows, own_ref[:, at], preferred_element_type=jnp.float32)
         part += jnp.dot(other_rows, other_ref[:, at], preferred_element_type=jnp.float32)
-        ref = out_refs[mask - 1] if mask else first_ref
-        ref[...] = part.astype(ref.dtype)
-
-
-def project(back, own_weight, other_weight, tp_count):
-    heads, half, depth = back.shape
+        out_ref[...] = part.astype(out_ref.dtype)
+
+
+def project(back, own_weight, other_weight, tp_count, masks):
+    rows = back[0].shape[1]
     cols = own_weight.shape[1] // tp_count
     vmem = pl.BlockSpec(memory_space=pltpu.VMEM)
-    shape = jax.ShapeDtypeStruct((half, cols), jnp.bfloat16)
+    shape = jax.ShapeDtypeStruct((rows, cols), jnp.bfloat16)
     return pl.pallas_call(
-        project_kernel,
-        out_shape=[shape] * tp_count,
-        in_specs=[vmem] * 3,
-        out_specs=[vmem] * tp_count,
-        scratch_shapes=[pltpu.VMEM((2, half, own_weight.shape[0]), jnp.bfloat16)],
+        functools.partial(project_kernel, masks),
+        out_shape=[shape] * len(masks),
+        in_specs=[vmem] * (2 + len(back)),
+        out_specs=[vmem] * len(masks),
+        scratch_shapes=[pltpu.VMEM((rows, 2 * own_weight.shape[0]), jnp.bfloat16)],
         cost_estimate=pl.CostEstimate(
-            flops=2 * half * heads * depth * own_weight.shape[1],
-            bytes_accessed=4 * own_weight.size + 4 * half * own_weight.shape[1],
+            flops=4 * rows * own_weight.size * len(masks) // tp_count,
+            bytes_accessed=4 * own_weight.size + 4 * rows * own_weight.shape[1],
             transcendentals=0,
         ),
         compiler_params=pltpu.CompilerParams(vmem_limit_bytes=16 * MIB),
         name="project",
-    )(back, own_weight, other_weight)
+    )(own_weight, other_weight, *back)
 
 
 def finish_kernel(turns, *refs):
@@ -323,7 +312,7 @@
     )(*flat)
 
 
-TURNS = 2
+TURNS = 1
 
 
 def head_attention(messages, out_weight, heads):
@@ -336,14 +325,24 @@
     depth = out_weight.shape[0] // heads
     half = messages[0].shape[0] // 3 // 16 * 16
     other_weight = swap(out_weight, "tp", 1)
+    outs = stick(own, other, ep_count, half, depth, TURNS)
+    backs = []
+    backs.append([lax.all_to_all(outs[0], "ep", split_axis=0, concat_axis=0, tiled=True)])
+    ep_index = lax.axis_index("ep")
+    for turn in range(1, TURNS):
+        back = [outs[turn]]
+        for mask in range(1, ep_count):
+            row = lax.dynamic_index_in_dim(outs[turn], ep_index ^ mask, 0, False)
+            back.append(swap(row, "ep", mask))
+        backs.append(back)
     pieces = []
-    for turn in range(TURNS):
-        out = stick(own, other, ep_count, half, depth, turn, TURNS)
-        back = lax.all_to_all(out, "ep", split_axis=0, concat_axis=0, tiled=True)
-        parts = list(project(back, out_weight, other_weight, tp_count))
-        for mask in range(1, tp_count):
-            parts[mask] = swap(parts[mask], "tp", mask)
-        pieces.append(parts)
+    for back in backs:
+        parts = {}
+        for masks in (range(tp_count - 1, 1, -1), (1, 0)):
+            made = project(back, out_weight, other_weight, tp_count, tuple(masks))
+            for mask, part in zip(masks, made):
+                parts[mask] = swap(part, "tp", mask) if mask else part
+        pieces.append([parts[mask] for mask in range(tp_count)])
     return finish(pieces)
 
 
@@ -558,22 +557,58 @@
 
 
 def gather_pieces(piece):
-    pieces = [piece]
-    for mask in range(1, lax.axis_size("tp")):
-        pieces.append(swap(piece, "tp", mask))
-    return pieces
-
-
-def scatter_rest(kept, sent):
-    index = lax.axis_index("tp")
-    parts = kept.astype(jnp.float32) + swap(sent, "tp", 1)
-    for bit in range(1, lax.axis_size("tp").bit_length() - 1):
-        mine = index >> bit & 1
-        parts = parts.reshape(parts.shape[0] // 2, 2, *parts.shape[1:])
-        stay = lax.dynamic_index_in_dim(parts, mine, 1, False)
-        leave = lax.dynamic_index_in_dim(parts, 1 - mine, 1, False)
-        parts = stay + swap(leave.astype(jnp.bfloat16), "tp", 1 << bit)
-    return parts[0]
+    held = {0: piece}
+    for bit in reversed(range(lax.axis_size("tp").bit_length() - 1)):
+        for mask, part in list(held.items()):
+            held[mask | 1 << bit] = swap(part, "tp", 1 << bit)
+    return [held[mask] for mask in range(len(held))]
+
+
+def near_kernel(kept_ref, got_ref, stay_ref, leave_ref):
+    far = lax.axis_index("tp") // 2
+    stay_ref[...] = kept_ref[far].astype(jnp.float32) + got_ref[far].astype(jnp.float32)
+    away = kept_ref[1 - far].astype(jnp.float32) + got_ref[1 - far].astype(jnp.float32)
+    leave_ref[...] = away.astype(leave_ref.dtype)
+
+
+def far_kernel(stay_ref, got_ref, routed_ref, common_ref):
+    slots = routed_ref.shape[0]
+    total = stay_ref[...] + got_ref[...].astype(jnp.float32)
+    routed_ref[...] = total[:slots].astype(routed_ref.dtype)
+    common_ref[...] = total[slots:]
+
+
+def scatter_rest(kept, sent, slots):
+    _, rows, cols = kept.shape
+    vmem = pl.BlockSpec(memory_space=pltpu.VMEM)
+    cost = pl.CostEstimate(
+        flops=4 * rows * cols, bytes_accessed=12 * rows * cols, transcendentals=0
+    )
+    got = swap(sent, "tp", 1)
+    stay, leave = pl.pallas_call(
+        near_kernel,
+        out_shape=[
+            jax.ShapeDtypeStruct((rows, cols), jnp.float32),
+            jax.ShapeDtypeStruct((rows, cols), jnp.bfloat16),
+        ],
+        in_specs=[vmem] * 2,
+        out_specs=[vmem] * 2,
+        cost_estimate=cost,
+        name="near",
+    )(kept, got)
+    got = swap(leave, "tp", 2)
+    return pl.pallas_call(
+        far_kernel,
+        out_shape=[
+            jax.ShapeDtypeStruct((slots, cols), jnp.bfloat16),
+            jax.ShapeDtypeStruct((rows - slots, cols), jnp.float32),
+        ],
+        in_specs=[vmem] * 2,
+        out_specs=[vmem] * 2,
+        cost_estimate=cost,
+        compiler_params=pltpu.CompilerParams(vmem_limit_bytes=8 * MIB),
+        name="far",
+    )(stay, got)
 
 
 def route_kernel(capacity, input_ref, gain_ref, ids_ref, out_ref, normed_ref, slots_ref):
@@ -736,11 +771,9 @@
     kept, sent = experts(
         shared_hidden, shared_down, expert_gate, expert_up, expert_down, pieces
     )
-    summed = scatter_rest(kept, sent)
-    returned = lax.all_to_all(
-        summed[:slots].astype(jnp.bfloat16), "ep", split_axis=0, concat_axis=0, tiled=True
-    )
-    return combine(summed[slots:], returned, slot_ids, route_scores.T)
+    routed, common = scatter_rest(kept, sent, slots)
+    returned = lax.all_to_all(routed, "ep", split_axis=0, concat_axis=0, tiled=True)
+    return combine(common, returned, slot_ids, route_scores.T)
 
 
 def body(queries, keys, values, key_bias, out_weight, *moe):
@@ -751,8 +784,8 @@
     tokens = moe[0].shape[0]
     slots = 3 * tokens * moe[2].shape[1] // 2
     aligned = span % 512 == 0 and width % (128 * heads) == 0 and cols % 256 == 0 and slots % 16 == 0
-    near = SEQUENCE_COUNT == 1 and 2 * heads == ep_count and tp_count % 2 == 0 and aligned
-    if not near or moe[7].shape[0] != 1 or slots % ep_count or tokens % 128:
+    near = SEQUENCE_COUNT == 1 and 2 * heads == ep_count and tp_count == 4 and aligned
+    if not near or ep_count % 4 or moe[7].shape[0] != 1 or slots % ep_count or tokens % 128:
         return (
             row_attention(queries, keys, values, key_bias, out_weight),
             expert_layer(*moe),

time: 147 us -> 133 us (0.905)
  Pallas kernels: 42.6 us -> 37.8 us
  other arithmetic: 3.41 us -> 0 us
  waiting for transfers between devices: 42.9 us -> 39.5 us
    pallas_call x2 -> x1, Pallas kernels: 25.6 us -> 17.1 us  [stick(): pl.pallas_call(functools.partial(stick_kernel, width ** (-0.5) * LOG2E, l...]
    ppermute x20 -> x17, starting transfers between devices: 12.2 us -> 19.1 us  [swap(): lax.ppermute(array, axis, [(i, i ^ mask) for i in range(lax.axis_size(axi...]
    ppermute x8, waiting for transfers between devices: 5.7 us -> 12.2 us  [send_round(): return lax.ppermute(array, ('ep', 'tp'), pairs)]
    all_to_all x3 -> x2, waiting for transfers between devices: 5.19 us -> 0.01 us  [the longest x1 0.01 us: expert_layer_near(): lax.all_to_all(routed, 'ep', split_axis=0, concat_axis=0, tiled=True)]
    ppermute x20 -> x17, waiting for transfers between devices: 23.7 us -> 18.9 us  [swap(): lax.ppermute(array, axis, [(i, i ^ mask) for i in range(lax.axis_size(axi...]
    all_to_all x3 -> x2, starting transfers between devices: 13.7 us -> 9.15 us  [the longest x1 5.65 us: expert_layer_near(): lax.all_to_all(routed, 'ep', split_axis=0, concat_axis=0, tiled=True)]
    pallas_call x2 -> x4, Pallas kernels: 5.97 us -> 9.71 us  [the longest x2 6 us: project(): pl.pallas_call(functools.partial(project_kernel, masks), out_shape=[shape...]
    add x2 -> x0, other arithmetic: 3.41 us -> none  [the longest x1 1.86 us: scatter_rest(): parts = kept.astype(jnp.float32) + swap(sent, 'tp', 1)]
  transfers between devices with their start and end apart: 32 -> 28, of which waited for: 14 -> 8; matrix products, arithmetic and copies ran while one was open for 5% -> 2% of each run, Pallas kernels for 27% -> 26%
where the time goes in v3:
time: 133 us
  starting transfers between devices  45.8 us (34%)
  waiting for transfers between devices  39.5 us (30%)
  Pallas kernels  37.8 us (28%)
  local copies, waits for them, and re-layouts  6.14 us (5%)
  matrix products  2.49 us (2%)
    ppermute x17, starting transfers between devices, swap(): lax.ppermute(array, axis, [(i, i ^ mask) for i in range(lax.axis_size(axi...  19.1 us
    ppermute x17, waiting for transfers between devices, swap(): lax.ppermute(array, axis, [(i, i ^ mask) for i in range(lax.axis_size(axi...  18.9 us
    pallas_call x1, Pallas kernels, stick(): pl.pallas_call(functools.partial(stick_kernel, width ** (-0.5) * LOG2E, l...  17.1 us
    ppermute x8, waiting for transfers between devices, send_round(): return lax.ppermute(array, ('ep', 'tp'), pairs)  12.2 us
    ppermute x8, starting transfers between devices, send_round(): return lax.ppermute(array, ('ep', 'tp'), pairs)  10.1 us
    all_to_all x1, waiting for transfers between devices, expert_layer_near(): lax.all_to_all(outgoing, 'ep', split_axis=0, concat_axis=0, tiled=True)  8.33 us
    all_to_all x1, starting transfers between devices, expert_layer_near(): lax.all_to_all(outgoing, 'ep', split_axis=0, concat_axis=0, tiled=True)  7.41 us
    unnamed x52, local copies, waits for them, and re-layouts  6.14 us
  transfers between devices with their start and end apart: 28, of which 8 were waited for; matrix products, arithmetic and copies ran while one was open for 2% of the time, Pallas kernels for 26%

profile of v3, /device:TPU:0, one launch (start us, length us, event | category | flops | bytes accessed | tf_op | source)
XLA Modules:
  0.0 132.5 jit_solution(17227789878161962221)
XLA Ops:
  0.6 2.4 %route.1 = (bf16[384,512]{1,0:T(8,128)(2,1)}, bf16[128,2048]{1,0:T(8,128)(2,1)}, s32[2,128]{1,0:T(2,128)}) custom-call(bf16[128,2048]{1,0:T(8,128)(2,1)} %input_ref.1, f32[1,2048]{1,0:T(1,128)} %bitcast.18, s32[2,128]{1,0:T(2,128)} %bitcast.20), custom_call_target="tpu_custom_call" | custom-call | flops 50331648 | bytes 1572864 | tf_op jit(solution)/shard_map/route/pallas_call | solution.py:645
  3.1 7.4 %all-to-all-start.1 = ((bf16[8,48,512]{2,1,0:T(8,128)(2,1)}), bf16[8,48,512]{2,1,0:T(8,128)(2,1)S(1)}, u32[]{:S(2)}, u32[]{:S(2)}) async-start(bf16[8,48,512]{2,1,0:T(8,128)(2,1)} %bitcast.17), calls=%async_computation.1 | async-start | bytes 786432 | tf_op jit(solution)/shard_map/all_to_all | solution.py:765
  10.5 2.6 %pack.1 = (bf16[784,128]{1,0:T(8,128)(2,1)}, bf16[784,128]{1,0:T(8,128)(2,1)}, bf16[784,128]{1,0:T(8,128)(2,1)}, bf16[784,128]{1,0:T(8,128)(2,1)}, bf16[784,128]...) custom-call(bf16[512,512]{1,0:T(8,128)(2,1)} %k_ref.1, ...), custom_call_target="tpu_custom_call" | custom-call | flops 2097152 | bytes 3145728 | tf_op jit(solution)/shard_map/pack/pallas_call | solution.py:80
  14.7 3.4 %collective-permute-start.2 = (bf16[784,128]{1,0:T(8,128)(2,1)}, bf16[784,128]{1,0:T(8,128)(2,1)S(1)}, u32[]{:S(2)}, u32[]{:S(2)}) collective-permute-start(bf16[784,128]{1,0:T(8,128)(2,1)} %get-tuple-element.24), channel_id=1, source_target_pairs={{0,1},{1,17},{2,3},{3,19},{4,5},{5,21},{6,7},{7,23},{8,9},{9,25},{... | collective-permute-start | bytes 602120 | tf_op jit(solution)/shard_map/ppermute | solution.py:43
  18.1 8.3 %all-to-all-done.1 = bf16[8,48,512]{2,1,0:T(8,128)(2,1)S(1)} async-done(((bf16[8,48,512]{2,1,0:T(8,128)(2,1)}), bf16[8,48,512]{2,1,0:T(8,128)(2,1)S(1)}, u32[]{:S(2)}, u32[]{:S(2)}) %all-to-all-start.1) | async-done | bytes 393248 | tf_op jit(solution)/shard_map/all_to_all | solution.py:765
  30.8 2.2 %collective-permute-start.6 = (bf16[784,128]{1,0:T(8,128)(2,1)}, bf16[784,128]{1,0:T(8,128)(2,1)S(1)}, u32[]{:S(2)}, u32[]{:S(2)}) collective-permute-start(bf16[784,128]{1,0:T(8,128)(2,1)} %get-tuple-element.28), channel_id=1, source_target_pairs={{0,9},{1,25},{2,11},{3,27},{4,13},{5,29},{6,15},{7,31},{8,1},{9,17... | collective-permute-start | bytes 602120 | tf_op jit(solution)/shard_map/ppermute | solution.py:43
  33.1 4.2 %collective-permute-done.3.refs_2_ = bf16[784,128]{1,0:T(8,128)(2,1)S(1)} collective-permute-done((bf16[784,128]{1,0:T(8,128)(2,1)}, bf16[784,128]{1,0:T(8,128)(2,1)S(1)}, u32[]{:S(2)}, u32[]{:S(2)}) %collective-permute-start.3) | collective-permute-done | bytes 200736 | tf_op jit(solution)/shard_map/ppermute | solution.py:43
  37.2 3.7 %collective-permute-done.4.refs_3_ = bf16[784,128]{1,0:T(8,128)(2,1)S(1)} collective-permute-done((bf16[784,128]{1,0:T(8,128)(2,1)}, bf16[784,128]{1,0:T(8,128)(2,1)S(1)}, u32[]{:S(2)}, u32[]{:S(2)}) %collective-permute-start.4) | collective-permute-done | bytes 200736 | tf_op jit(solution)/shard_map/ppermute | solution.py:43
  41.0 4.8 %collective-permute-start.9 = (bf16[784,128]{1,0:T(8,128)(2,1)S(1)}, bf16[784,128]{1,0:T(8,128)(2,1)S(1)}, u32[]{:S(2)}, u32[]{:S(2)}) collective-permute-start(bf16[784,128]{1,0:T(8,128)(2,1)S(1)} %collective-permute-done.1.refs_0_), channel_id=1, source_target_pairs={{0,1},{1,0},{2,3},{3,2},{4,5},{5,4},{6,7},{7,6},{8,9},{9,8},{10,11... | collective-permute-start | bytes 602120 | tf_op jit(solution)/shard_map/ppermute | solution.py:27
  45.8 2.0 %collective-permute-done.6.refs_5_ = bf16[784,128]{1,0:T(8,128)(2,1)S(1)} collective-permute-done((bf16[784,128]{1,0:T(8,128)(2,1)}, bf16[784,128]{1,0:T(8,128)(2,1)S(1)}, u32[]{:S(2)}, u32[]{:S(2)}) %collective-permute-start.6) | collective-permute-done | bytes 200736 | tf_op jit(solution)/shard_map/ppermute | solution.py:43
  48.8 6.3 %collective-permute-start.10 = (bf16[784,128]{1,0:T(8,128)(2,1)S(1)}, bf16[784,128]{1,0:T(8,128)(2,1)S(1)}, u32[]{:S(2)}, u32[]{:S(2)}) collective-permute-start(bf16[784,128]{1,0:T(8,128)(2,1)S(1)} %collective-permute-done.2.refs_1_), channel_id=1, source_target_pairs={{0,1},{1,0},{2,3},{3,2},{4,5},{5,4},{6,7},{7,6},{8,9},{9,8},{10,11... | collective-permute-start | bytes 602120 | tf_op jit(solution)/shard_map/ppermute | solution.py:27
  55.2 2.3 %collective-permute-done.8.refs_7_ = bf16[784,128]{1,0:T(8,128)(2,1)S(1)} collective-permute-done((bf16[784,128]{1,0:T(8,128)(2,1)}, bf16[784,128]{1,0:T(8,128)(2,1)S(1)}, u32[]{:S(2)}, u32[]{:S(2)}) %collective-permute-start.8) | collective-permute-done | bytes 200736 | tf_op jit(solution)/shard_map/ppermute | solution.py:43
  58.7 2.0 %fusion.shared_ref = bf16[128,512]{1,0:T(8,128)(2,1)S(1)} fusion(bf16[128,2048]{1,0:T(8,128)(2,1)S(1)} %copy-done.9, bf16[2048,512]{1,0:T(8,128)(2,1)} %param.26, f32[128,512]{1,0:T(8,128)S(1)} %fusion.1), kind=kOutput, calls=%fused_computation.1 | convolution fusion | flops 268763136 | bytes 3014656 | tf_op jit(solution)/shard_map/dot_general | solution.py:769
  62.2 1.6 %copy-done.4 = bf16[1,512,2048]{2,1,0:T(8,128)(2,1)S(1)} copy-done((bf16[1,512,2048]{2,1,0:T(8,128)(2,1)S(1)}, bf16[1,512,2048]{2,1,0:T(8,128)(2,1)}, u32[]{:S(2)}) %copy-start.4) | copy-done | bytes 2097176
  63.8 4.0 %experts.1 = (bf16[2,512,512]{2,1,0:T(8,128)(2,1)S(1)}, bf16[2,512,512]{2,1,0:T(8,128)(2,1)}) custom-call(bf16[128,512]{1,0:T(8,128)(2,1)S(1)} %fusion.shared_ref, bf16[512,2048]{1,0:T(8,128)(2,1)S(1)} %copy-done.1, bf16[1,2048,512]{2,1,0:T(8,128)(2,1)S(1)} %copy-done.2, bf16[1,2048,512]{2,1,0:T(8,128)(2,1)S(1)} %copy-done.3, ...), custom_call_target="tpu_custom_call" | custom-call | flops 2684354560 | bytes 12582912 | tf_op jit(solution)/shard_map/experts/pallas_call | solution.py:694
  70.7 17.1 %stick.1 = bf16[8,256,128]{2,1,0:T(8,128)(2,1)} custom-call(s32[1,76]{1,0:T(1,128)} %constant.4.clone.table_ref, bf16[784,128]{1,0:T(8,128)(2,1)} %copy-done.10, bf16[784,128]{1,0:T(8,128)(2,1)} %copy-done.11, bf16[784,128]{1,0:T(8,128)(2,1)} %copy-done.12, bf16[784,128]{1,0:T(8,128)(2,1)} %copy-done.13, bf16[784,128]{1,0:T(8,128)(2,1)} %copy-done.14, ...), custom_call_target="tpu_custom_call" | custom-call | flops 6039797760 | bytes 2621440 | tf_op jit(solution)/shard_map/stick/pallas_call | solution.py:209
  87.8 3.5 %all-to-all-start = ((bf16[8,256,128]{2,1,0:T(8,128)(2,1)}), bf16[8,256,128]{2,1,0:T(8,128)(2,1)S(1)}, u32[]{:S(2)}, u32[]{:S(2)}) async-start(bf16[8,256,128]{2,1,0:T(8,128)(2,1)} %stick.1), calls=%async_computation | async-start | bytes 1048576 | tf_op jit(solution)/shard_map/all_to_all | solution.py:330
  91.3 2.9 %near.1 = (f32[512,512]{1,0:T(8,128)}, bf16[512,512]{1,0:T(8,128)(2,1)}) custom-call(bf16[2,512,512]{2,1,0:T(8,128)(2,1)} %copy-done.6, bf16[2,512,512]{2,1,0:T(8,128)(2,1)} %collective-permute-done.23.got_ref), custom_call_target="tpu_custom_call" | custom-call | flops 1048576 | bytes 3145728 | tf_op jit(solution)/shard_map/near/pallas_call | solution.py:588
  95.8 12.6 %collective-permute-done.24.got_ref = bf16[512,512]{1,0:T(8,128)(2,1)S(1)} collective-permute-done((bf16[512,512]{1,0:T(8,128)(2,1)}, bf16[512,512]{1,0:T(8,128)(2,1)S(1)}, u32[]{:S(2)}, u32[]{:S(2)}) %collective-permute-start.24) | collective-permute-done | bytes 524320 | tf_op jit(solution)/shard_map/ppermute | solution.py:27
  110.4 5.6 %all-to-all-start.2 = ((bf16[8,48,512]{2,1,0:T(8,128)(2,1)}), bf16[8,48,512]{2,1,0:T(8,128)(2,1)S(1)}, u32[]{:S(2)}, u32[]{:S(2)}) async-start(bf16[8,48,512]{2,1,0:T(8,128)(2,1)} %bitcast.5), calls=%async_computation.2 | async-start | bytes 786432 | tf_op jit(solution)/shard_map/all_to_all | solution.py:775
  116.0 3.0 %project.3 = (bf16[256,512]{1,0:T(8,128)(2,1)S(1)}, bf16[256,512]{1,0:T(8,128)(2,1)S(1)}) custom-call(bf16[512,2048]{1,0:T(8,128)(2,1)} %own_ref.3, bf16[512,2048]{1,0:T(8,128)(2,1)} %collective-permute-done.other_ref, bf16[8,256,128]{2,1,0:T(8,128)(2,1)S(1)} %all-to-all-done.refs_0_), custom_call_target="tpu_custom_call" | custom-call | flops 536870912 | bytes 6291456 | tf_op jit(solution)/shard_map/project/pallas_call | solution.py:267
  120.6 3.0 %project.2 = (bf16[256,512]{1,0:T(8,128)(2,1)S(1)}, bf16[256,512]{1,0:T(8,128)(2,1)S(1)}) custom-call(bf16[512,2048]{1,0:T(8,128)(2,1)} %own_ref.3, bf16[512,2048]{1,0:T(8,128)(2,1)} %collective-permute-done.other_ref, bf16[8,256,128]{2,1,0:T(8,128)(2,1)S(1)} %all-to-all-done.refs_0_), custom_call_target="tpu_custom_call" | custom-call | flops 536870912 | bytes 6291456 | tf_op jit(solution)/shard_map/project/pallas_call | solution.py:267
  124.3 4.0 %collective-permute-done.18.refs_2_ = bf16[256,512]{1,0:T(8,128)(2,1)S(1)} collective-permute-done((bf16[256,512]{1,0:T(8,128)(2,1)S(1)}, bf16[256,512]{1,0:T(8,128)(2,1)S(1)}, u32[]{:S(2)}, u32[]{:S(2)}) %collective-permute-start.18) | collective-permute-done | bytes 262176 | tf_op jit(solution)/shard_map/ppermute | solution.py:27
  128.3 2.3 %collective-permute-done.19.refs_3_ = bf16[256,512]{1,0:T(8,128)(2,1)S(1)} collective-permute-done((bf16[256,512]{1,0:T(8,128)(2,1)S(1)}, bf16[256,512]{1,0:T(8,128)(2,1)S(1)}, u32[]{:S(2)}, u32[]{:S(2)}) %collective-permute-start.19) | collective-permute-done | bytes 262176 | tf_op jit(solution)/shard_map/ppermute | solution.py:27
  (96 shorter events, 20.2 us)
Async XLA Ops:
  3.1 23.4 %all-to-all-start.1 = ((bf16[8,48,512]{2,1,0:T(8,128)(2,1)}), bf16[8,48,512]{2,1,0:T(8,128)(2,1)S(1)}, u32[]{:S(2)}, u32[]{:S(2)}) async-start(bf16[8,48,512]{2,1,0:T(8,128)(2,1)} %bitcast.17), calls=%async_computation.1 | async-start | bytes 786432 | tf_op jit(solution)/shard_map/all_to_all | solution.py:765
  13.1 17.6 %collective-permute-start.1 = (bf16[784,128]{1,0:T(8,128)(2,1)}, bf16[784,128]{1,0:T(8,128)(2,1)S(1)}, u32[]{:S(2)}, u32[]{:S(2)}) collective-permute-start(bf16[784,128]{1,0:T(8,128)(2,1)} %get-tuple-element.23), channel_id=1, source_target_pairs={{0,0},{1,16},{2,2},{3,18},{4,4},{5,20},{6,6},{7,22},{8,8},{9,24},{... | collective-permute-start | bytes 602120 | tf_op jit(solution)/shard_map/ppermute | solution.py:43
  14.7 16.1 %collective-permute-start.2 = (bf16[784,128]{1,0:T(8,128)(2,1)}, bf16[784,128]{1,0:T(8,128)(2,1)S(1)}, u32[]{:S(2)}, u32[]{:S(2)}) collective-permute-start(bf16[784,128]{1,0:T(8,128)(2,1)} %get-tuple-element.24), channel_id=1, source_target_pairs={{0,1},{1,17},{2,3},{3,19},{4,5},{5,21},{6,7},{7,23},{8,9},{9,25},{... | collective-permute-start | bytes 602120 | tf_op jit(solution)/shard_map/ppermute | solution.py:43
  26.5 21.4 %collective-permute-start.21 = (bf16[384,512]{1,0:T(8,128)(2,1)S(1)}, bf16[384,512]{1,0:T(8,128)(2,1)S(1)}, u32[]{:S(2)}, u32[]{:S(2)}) collective-permute-start(bf16[384,512]{1,0:T(8,128)(2,1)S(1)} %bitcast.12), channel_id=1, source_target_pairs={{0,2},{1,3},{2,0},{3,1},{4,6},{5,7},{6,4},{7,5},{8,10},{9,11},{10,... | collective-permute-start | bytes 1179656 | tf_op jit(solution)/shard_map/ppermute | solution.py:27
  28.0 9.2 %collective-permute-start.3 = (bf16[784,128]{1,0:T(8,128)(2,1)}, bf16[784,128]{1,0:T(8,128)(2,1)S(1)}, u32[]{:S(2)}, u32[]{:S(2)}) collective-permute-start(bf16[784,128]{1,0:T(8,128)(2,1)} %get-tuple-element.25), channel_id=1, source_target_pairs={{0,4},{1,20},{2,6},{3,22},{4,8},{5,24},{6,10},{7,26},{8,12},{9,28}... | collective-permute-start | bytes 602120 | tf_op jit(solution)/shard_map/ppermute | solution.py:43
  29.5 11.4 %collective-permute-start.4 = (bf16[784,128]{1,0:T(8,128)(2,1)}, bf16[784,128]{1,0:T(8,128)(2,1)S(1)}, u32[]{:S(2)}, u32[]{:S(2)}) collective-permute-start(bf16[784,128]{1,0:T(8,128)(2,1)} %get-tuple-element.26), channel_id=1, source_target_pairs={{0,5},{1,21},{2,7},{3,23},{4,9},{5,25},{6,11},{7,27},{8,13},{9,29}... | collective-permute-start | bytes 602120 | tf_op jit(solution)/shard_map/ppermute | solution.py:43
  30.8 10.2 %collective-permute-start.5 = (bf16[784,128]{1,0:T(8,128)(2,1)}, bf16[784,128]{1,0:T(8,128)(2,1)S(1)}, u32[]{:S(2)}, u32[]{:S(2)}) collective-permute-start(bf16[784,128]{1,0:T(8,128)(2,1)} %get-tuple-element.27), channel_id=1, source_target_pairs={{0,8},{1,24},{2,10},{3,26},{4,12},{5,28},{6,14},{7,30},{8,0},{9,16... | collective-permute-start | bytes 602120 | tf_op jit(solution)/shard_map/ppermute | solution.py:43
  30.8 17.0 %collective-permute-start.6 = (bf16[784,128]{1,0:T(8,128)(2,1)}, bf16[784,128]{1,0:T(8,128)(2,1)S(1)}, u32[]{:S(2)}, u32[]{:S(2)}) collective-permute-start(bf16[784,128]{1,0:T(8,128)(2,1)} %get-tuple-element.28), channel_id=1, source_target_pairs={{0,9},{1,25},{2,11},{3,27},{4,13},{5,29},{6,15},{7,31},{8,1},{9,17... | collective-permute-start | bytes 602120 | tf_op jit(solution)/shard_map/ppermute | solution.py:43
  37.2 11.6 %collective-permute-start.7 = (bf16[784,128]{1,0:T(8,128)(2,1)}, bf16[784,128]{1,0:T(8,128)(2,1)S(1)}, u32[]{:S(2)}, u32[]{:S(2)}) collective-permute-start(bf16[784,128]{1,0:T(8,128)(2,1)} %get-tuple-element.29), channel_id=1, source_target_pairs={{0,12},{1,28},{2,14},{3,30},{4,0},{5,16},{6,2},{7,18},{8,4},{9,20}... | collective-permute-start | bytes 602120 | tf_op jit(solution)/shard_map/ppermute | solution.py:43
  40.9 16.6 %collective-permute-start.8 = (bf16[784,128]{1,0:T(8,128)(2,1)}, bf16[784,128]{1,0:T(8,128)(2,1)S(1)}, u32[]{:S(2)}, u32[]{:S(2)}) collective-permute-start(bf16[784,128]{1,0:T(8,128)(2,1)} %get-tuple-element.30), channel_id=1, source_target_pairs={{0,13},{1,29},{2,15},{3,31},{4,1},{5,17},{6,3},{7,19},{8,5},{9,21}... | collective-permute-start | bytes 602120 | tf_op jit(solution)/shard_map/ppermute | solution.py:43
  41.0 16.5 %collective-permute-start.9 = (bf16[784,128]{1,0:T(8,128)(2,1)S(1)}, bf16[784,128]{1,0:T(8,128)(2,1)S(1)}, u32[]{:S(2)}, u32[]{:S(2)}) collective-permute-start(bf16[784,128]{1,0:T(8,128)(2,1)S(1)} %collective-permute-done.1.refs_0_), channel_id=1, source_target_pairs={{0,1},{1,0},{2,3},{3,2},{4,5},{5,4},{6,7},{7,6},{8,9},{9,8},{10,11... | collective-permute-start | bytes 602120 | tf_op jit(solution)/shard_map/ppermute | solution.py:27
  47.8 13.7 %collective-permute-start.20 = (bf16[384,512]{1,0:T(8,128)(2,1)S(1)}, bf16[384,512]{1,0:T(8,128)(2,1)S(1)}, u32[]{:S(2)}, u32[]{:S(2)}) collective-permute-start(bf16[384,512]{1,0:T(8,128)(2,1)S(1)} %bitcast.13), channel_id=1, source_target_pairs={{0,1},{1,0},{2,3},{3,2},{4,5},{5,4},{6,7},{7,6},{8,9},{9,8},{10,11... | collective-permute-start | bytes 1179656 | tf_op jit(solution)/shard_map/ppermute | solution.py:27
  47.8 14.2 %collective-permute-start.22 = (bf16[384,512]{1,0:T(8,128)(2,1)S(1)}, bf16[384,512]{1,0:T(8,128)(2,1)S(1)}, u32[]{:S(2)}, u32[]{:S(2)}) collective-permute-start(bf16[384,512]{1,0:T(8,128)(2,1)S(1)} %collective-permute-done.21.refs_2_), channel_id=1, source_target_pairs={{0,1},{1,0},{2,3},{3,2},{4,5},{5,4},{6,7},{7,6},{8,9},{9,8},{10,11... | collective-permute-start | bytes 1179656 | tf_op jit(solution)/shard_map/ppermute | solution.py:27
  48.8 11.9 %collective-permute-start.10 = (bf16[784,128]{1,0:T(8,128)(2,1)S(1)}, bf16[784,128]{1,0:T(8,128)(2,1)S(1)}, u32[]{:S(2)}, u32[]{:S(2)}) collective-permute-start(bf16[784,128]{1,0:T(8,128)(2,1)S(1)} %collective-permute-done.2.refs_1_), channel_id=1, source_target_pairs={{0,1},{1,0},{2,3},{3,2},{4,5},{5,4},{6,7},{7,6},{8,9},{9,8},{10,11... | collective-permute-start | bytes 602120 | tf_op jit(solution)/shard_map/ppermute | solution.py:27
  60.8 55.2 %collective-permute-start = (bf16[512,2048]{1,0:T(8,128)(2,1)}, bf16[512,2048]{1,0:T(8,128)(2,1)}, u32[]{:S(2)}, u32[]{:S(2)}) collective-permute-start(bf16[512,2048]{1,0:T(8,128)(2,1)} %own_ref.3), channel_id=1, source_target_pairs={{0,1},{1,0},{2,3},{3,2},{4,5},{5,4},{6,7},{7,6},{8,9},{9,8},{10,11... | collective-permute-start | bytes 6291464 | tf_op jit(solution)/shard_map/ppermute | solution.py:27
  60.9 7.8 %collective-permute-start.13 = (bf16[784,128]{1,0:T(8,128)(2,1)S(1)}, bf16[784,128]{1,0:T(8,128)(2,1)S(1)}, u32[]{:S(2)}, u32[]{:S(2)}) collective-permute-start(bf16[784,128]{1,0:T(8,128)(2,1)S(1)} %collective-permute-done.5.refs_4_), channel_id=1, source_target_pairs={{0,1},{1,0},{2,3},{3,2},{4,5},{5,4},{6,7},{7,6},{8,9},{9,8},{10,11... | collective-permute-start | bytes 602120 | tf_op jit(solution)/shard_map/ppermute | solution.py:27
  61.4 7.8 %collective-permute-start.14 = (bf16[784,128]{1,0:T(8,128)(2,1)S(1)}, bf16[784,128]{1,0:T(8,128)(2,1)S(1)}, u32[]{:S(2)}, u32[]{:S(2)}) collective-permute-start(bf16[784,128]{1,0:T(8,128)(2,1)S(1)} %collective-permute-done.6.refs_5_), channel_id=1, source_target_pairs={{0,1},{1,0},{2,3},{3,2},{4,5},{5,4},{6,7},{7,6},{8,9},{9,8},{10,11... | collective-permute-start | bytes 602120 | tf_op jit(solution)/shard_map/ppermute | solution.py:27
  61.5 7.7 %collective-permute-start.15 = (bf16[784,128]{1,0:T(8,128)(2,1)S(1)}, bf16[784,128]{1,0:T(8,128)(2,1)S(1)}, u32[]{:S(2)}, u32[]{:S(2)}) collective-permute-start(bf16[784,128]{1,0:T(8,128)(2,1)S(1)} %collective-permute-done.7.refs_6_), channel_id=1, source_target_pairs={{0,1},{1,0},{2,3},{3,2},{4,5},{5,4},{6,7},{7,6},{8,9},{9,8},{10,11... | collective-permute-start | bytes 602120 | tf_op jit(solution)/shard_map/ppermute | solution.py:27
  68.8 22.6 %collective-permute-start.23 = (bf16[2,512,512]{2,1,0:T(8,128)(2,1)}, bf16[2,512,512]{2,1,0:T(8,128)(2,1)}, u32[]{:S(2)}, u32[]{:S(2)}) collective-permute-start(bf16[2,512,512]{2,1,0:T(8,128)(2,1)} %get-tuple-element.38), channel_id=1, source_target_pairs={{0,1},{1,0},{2,3},{3,2},{4,5},{5,4},{6,7},{7,6},{8,9},{9,8},{10,11... | collective-permute-start | bytes 3145736 | tf_op jit(solution)/shard_map/ppermute | solution.py:27
  87.8 22.6 %all-to-all-start = ((bf16[8,256,128]{2,1,0:T(8,128)(2,1)}), bf16[8,256,128]{2,1,0:T(8,128)(2,1)S(1)}, u32[]{:S(2)}, u32[]{:S(2)}) async-start(bf16[8,256,128]{2,1,0:T(8,128)(2,1)} %stick.1), calls=%async_computation | async-start | bytes 1048576 | tf_op jit(solution)/shard_map/all_to_all | solution.py:330
  94.2 14.1 %collective-permute-start.24 = (bf16[512,512]{1,0:T(8,128)(2,1)}, bf16[512,512]{1,0:T(8,128)(2,1)S(1)}, u32[]{:S(2)}, u32[]{:S(2)}) collective-permute-start(bf16[512,512]{1,0:T(8,128)(2,1)} %get-tuple-element.40), channel_id=1, source_target_pairs={{0,2},{1,3},{2,0},{3,1},{4,6},{5,7},{6,4},{7,5},{8,10},{9,11},{10,... | collective-permute-start | bytes 1572872 | tf_op jit(solution)/shard_map/ppermute | solution.py:27
  110.4 21.1 %all-to-all-start.2 = ((bf16[8,48,512]{2,1,0:T(8,128)(2,1)}), bf16[8,48,512]{2,1,0:T(8,128)(2,1)S(1)}, u32[]{:S(2)}, u32[]{:S(2)}) async-start(bf16[8,48,512]{2,1,0:T(8,128)(2,1)} %bitcast.5), calls=%async_computation.2 | async-start | bytes 786432 | tf_op jit(solution)/shard_map/all_to_all | solution.py:775
  119.0 9.2 %collective-permute-start.18 = (bf16[256,512]{1,0:T(8,128)(2,1)S(1)}, bf16[256,512]{1,0:T(8,128)(2,1)S(1)}, u32[]{:S(2)}, u32[]{:S(2)}) collective-permute-start(bf16[256,512]{1,0:T(8,128)(2,1)S(1)} %get-tuple-element.33), channel_id=1, source_target_pairs={{0,2},{1,3},{2,0},{3,1},{4,6},{5,7},{6,4},{7,5},{8,10},{9,11},{10,... | collective-permute-start | bytes 786440 | tf_op jit(solution)/shard_map/ppermute | solution.py:27
  120.6 10.0 %collective-permute-start.19 = (bf16[256,512]{1,0:T(8,128)(2,1)S(1)}, bf16[256,512]{1,0:T(8,128)(2,1)S(1)}, u32[]{:S(2)}, u32[]{:S(2)}) collective-permute-start(bf16[256,512]{1,0:T(8,128)(2,1)S(1)} %get-tuple-element.34), channel_id=1, source_target_pairs={{0,3},{1,2},{2,1},{3,0},{4,7},{5,6},{6,5},{7,4},{8,11},{9,10},{10,... | collective-permute-start | bytes 786440 | tf_op jit(solution)/shard_map/ppermute | solution.py:27
  (30 other events, 353.0 us)

commit v4 on v3

--- a/solution.py
+++ b/solution.py
@@ -236,11 +236,21 @@
 
 def project_kernel(masks, own_ref, other_ref, *refs):
     count = len(masks)
-    back_refs, out_refs, rows_s = refs[: -count - 1], refs[-count - 1 : -1], refs[-1]
+    back_refs, out_refs = refs[: -count - 3], refs[-count - 3 : -3]
+    rows_s, weight_s, sems = refs[-3:]
     ep_index, tp_index = lax.axis_index("ep"), lax.axis_index("tp")
     core = lax.rem(tp_index, 2)
     width = own_ref.shape[0]
     cols = out_refs[0].shape[1]
+    copies = []
+    for at, mask in enumerate(masks):
+        columns = pl.ds(pl.multiple_of((tp_index ^ mask) * cols, cols), cols)
+        for which, ref in enumerate((own_ref, other_ref)):
+            copy = pltpu.make_async_copy(
+                ref.at[:, columns], weight_s.at[at, which], sems.at[at, which]
+            )
+            copy.start()
+            copies.append(copy)
     depth = back_refs[0].shape[-1]
     heads = rows_s.shape[1] // depth
     for head in range(heads):
@@ -252,10 +262,11 @@
             rows_s[:, at] = ref[...] if head else ref[ep_index]
     own_rows = rows_s[:, pl.ds(pl.multiple_of(core * width, width), width)]
     other_rows = rows_s[:, pl.ds(pl.multiple_of((1 - core) * width, width), width)]
-    for mask, out_ref in zip(masks, out_refs):
-        at = pl.ds(pl.multiple_of((tp_index ^ mask) * cols, cols), cols)
-        part = jnp.dot(own_rows, own_ref[:, at], preferred_element_type=jnp.float32)
-        part += jnp.dot(other_rows, other_ref[:, at], preferred_element_type=jnp.float32)
+    for at, out_ref in enumerate(out_refs):
+        copies[2 * at].wait()
+        part = jnp.dot(own_rows, weight_s[at, 0], preferred_element_type=jnp.float32)
+        copies[2 * at + 1].wait()
+        part += jnp.dot(other_rows, weight_s[at, 1], preferred_element_type=jnp.float32)
         out_ref[...] = part.astype(out_ref.dtype)
 
 
@@ -267,9 +278,13 @@
     return pl.pallas_call(
         functools.partial(project_kernel, masks),
         out_shape=[shape] * len(masks),
-        in_specs=[vmem] * (2 + len(back)),
+        in_specs=[pl.BlockSpec(memory_space=pl.ANY)] * 2 + [vmem] * len(back),
         out_specs=[vmem] * len(masks),
-        scratch_shapes=[pltpu.VMEM((rows, 2 * own_weight.shape[0]), jnp.bfloat16)],
+        scratch_shapes=[
+            pltpu.VMEM((rows, 2 * own_weight.shape[0]), jnp.bfloat16),
+            pltpu.VMEM((len(masks), 2, own_weight.shape[0], cols), jnp.bfloat16),
+            pltpu.SemaphoreType.DMA((len(masks), 2)),
+        ],
         cost_estimate=pl.CostEstimate(
             flops=4 * rows * own_weight.size * len(masks) // tp_count,
             bytes_accessed=4 * own_weight.size + 4 * rows * own_weight.shape[1],

time: 133 us -> 133 us (level)
  Pallas kernels: 37.8 us -> 36.1 us
    pallas_call x2, Pallas kernels: 6 us -> 4.35 us  [project(): pl.pallas_call(functools.partial(project_kernel, masks), out_shape=[shape...]
  transfers between devices with their start and end apart: 28 -> 28, of which waited for: 8 -> 8; matrix products, arithmetic and copies ran while one was open for 2% -> 2% of each run, Pallas kernels for 26% -> 25%
where the time goes in v4:
time: 133 us; the launch traced here: 132 us
  starting transfers between devices  45.8 us (34%)
  waiting for transfers between devices  40.3 us (30%)
  Pallas kernels  36.1 us (27%)
  local copies, waits for them, and re-layouts  6.14 us (5%)
  matrix products  2.49 us (2%)
    ppermute x17, waiting for transfers between devices, swap(): lax.ppermute(array, axis, [(i, i ^ mask) for i in range(lax.axis_size(axi...  19.7 us
    ppermute x17, starting transfers between devices, swap(): lax.ppermute(array, axis, [(i, i ^ mask) for i in range(lax.axis_size(axi...  19.1 us
    pallas_call x1, Pallas kernels, stick(): pl.pallas_call(functools.partial(stick_kernel, width ** (-0.5) * LOG2E, l...  17.1 us
    ppermute x8, waiting for transfers between devices, send_round(): return lax.ppermute(array, ('ep', 'tp'), pairs)  12.2 us
    ppermute x8, starting transfers between devices, send_round(): return lax.ppermute(array, ('ep', 'tp'), pairs)  10.1 us
    all_to_all x1, waiting for transfers between devices, expert_layer_near(): lax.all_to_all(outgoing, 'ep', split_axis=0, concat_axis=0, tiled=True)  8.33 us
    all_to_all x1, starting transfers between devices, expert_layer_near(): lax.all_to_all(outgoing, 'ep', split_axis=0, concat_axis=0, tiled=True)  7.41 us
    unnamed x52, local copies, waits for them, and re-layouts  6.14 us
  transfers between devices with their start and end apart: 28, of which 8 were waited for; matrix products, arithmetic and copies ran while one was open for 2% of the time, Pallas kernels for 25%

profile of v4, /device:TPU:0, one launch (start us, length us, event | category | flops | bytes accessed | tf_op | source)
XLA Modules:
  0.0 131.7 jit_solution(9377872939296700323)
XLA Ops:
  0.6 2.4 %route.1 = (bf16[384,512]{1,0:T(8,128)(2,1)}, bf16[128,2048]{1,0:T(8,128)(2,1)}, s32[2,128]{1,0:T(2,128)}) custom-call(bf16[128,2048]{1,0:T(8,128)(2,1)} %input_ref.1, f32[1,2048]{1,0:T(1,128)} %bitcast.18, s32[2,128]{1,0:T(2,128)} %bitcast.20), custom_call_target="tpu_custom_call" | custom-call | flops 50331648 | bytes 1572864 | tf_op jit(solution)/shard_map/route/pallas_call | solution.py:660
  3.1 7.4 %all-to-all-start.1 = ((bf16[8,48,512]{2,1,0:T(8,128)(2,1)}), bf16[8,48,512]{2,1,0:T(8,128)(2,1)S(1)}, u32[]{:S(2)}, u32[]{:S(2)}) async-start(bf16[8,48,512]{2,1,0:T(8,128)(2,1)} %bitcast.17), calls=%async_computation.1 | async-start | bytes 786432 | tf_op jit(solution)/shard_map/all_to_all | solution.py:780
  10.5 2.6 %pack.1 = (bf16[784,128]{1,0:T(8,128)(2,1)}, bf16[784,128]{1,0:T(8,128)(2,1)}, bf16[784,128]{1,0:T(8,128)(2,1)}, bf16[784,128]{1,0:T(8,128)(2,1)}, bf16[784,128]...) custom-call(bf16[512,512]{1,0:T(8,128)(2,1)} %k_ref.1, ...), custom_call_target="tpu_custom_call" | custom-call | flops 2097152 | bytes 3145728 | tf_op jit(solution)/shard_map/pack/pallas_call | solution.py:80
  14.7 3.4 %collective-permute-start.2 = (bf16[784,128]{1,0:T(8,128)(2,1)}, bf16[784,128]{1,0:T(8,128)(2,1)S(1)}, u32[]{:S(2)}, u32[]{:S(2)}) collective-permute-start(bf16[784,128]{1,0:T(8,128)(2,1)} %get-tuple-element.24), channel_id=1, source_target_pairs={{0,1},{1,17},{2,3},{3,19},{4,5},{5,21},{6,7},{7,23},{8,9},{9,25},{... | collective-permute-start | bytes 602120 | tf_op jit(solution)/shard_map/ppermute | solution.py:43
  18.1 8.3 %all-to-all-done.1 = bf16[8,48,512]{2,1,0:T(8,128)(2,1)S(1)} async-done(((bf16[8,48,512]{2,1,0:T(8,128)(2,1)}), bf16[8,48,512]{2,1,0:T(8,128)(2,1)S(1)}, u32[]{:S(2)}, u32[]{:S(2)}) %all-to-all-start.1) | async-done | bytes 393248 | tf_op jit(solution)/shard_map/all_to_all | solution.py:780
  30.8 2.2 %collective-permute-start.6 = (bf16[784,128]{1,0:T(8,128)(2,1)}, bf16[784,128]{1,0:T(8,128)(2,1)S(1)}, u32[]{:S(2)}, u32[]{:S(2)}) collective-permute-start(bf16[784,128]{1,0:T(8,128)(2,1)} %get-tuple-element.28), channel_id=1, source_target_pairs={{0,9},{1,25},{2,11},{3,27},{4,13},{5,29},{6,15},{7,31},{8,1},{9,17... | collective-permute-start | bytes 602120 | tf_op jit(solution)/shard_map/ppermute | solution.py:43
  33.1 4.2 %collective-permute-done.3.refs_2_ = bf16[784,128]{1,0:T(8,128)(2,1)S(1)} collective-permute-done((bf16[784,128]{1,0:T(8,128)(2,1)}, bf16[784,128]{1,0:T(8,128)(2,1)S(1)}, u32[]{:S(2)}, u32[]{:S(2)}) %collective-permute-start.3) | collective-permute-done | bytes 200736 | tf_op jit(solution)/shard_map/ppermute | solution.py:43
  37.2 3.7 %collective-permute-done.4.refs_3_ = bf16[784,128]{1,0:T(8,128)(2,1)S(1)} collective-permute-done((bf16[784,128]{1,0:T(8,128)(2,1)}, bf16[784,128]{1,0:T(8,128)(2,1)S(1)}, u32[]{:S(2)}, u32[]{:S(2)}) %collective-permute-start.4) | collective-permute-done | bytes 200736 | tf_op jit(solution)/shard_map/ppermute | solution.py:43
  41.0 4.8 %collective-permute-start.9 = (bf16[784,128]{1,0:T(8,128)(2,1)S(1)}, bf16[784,128]{1,0:T(8,128)(2,1)S(1)}, u32[]{:S(2)}, u32[]{:S(2)}) collective-permute-start(bf16[784,128]{1,0:T(8,128)(2,1)S(1)} %collective-permute-done.1.refs_0_), channel_id=1, source_target_pairs={{0,1},{1,0},{2,3},{3,2},{4,5},{5,4},{6,7},{7,6},{8,9},{9,8},{10,11... | collective-permute-start | bytes 602120 | tf_op jit(solution)/shard_map/ppermute | solution.py:27
  45.8 2.0 %collective-permute-done.6.refs_5_ = bf16[784,128]{1,0:T(8,128)(2,1)S(1)} collective-permute-done((bf16[784,128]{1,0:T(8,128)(2,1)}, bf16[784,128]{1,0:T(8,128)(2,1)S(1)}, u32[]{:S(2)}, u32[]{:S(2)}) %collective-permute-start.6) | collective-permute-done | bytes 200736 | tf_op jit(solution)/shard_map/ppermute | solution.py:43
  48.8 6.3 %collective-permute-start.10 = (bf16[784,128]{1,0:T(8,128)(2,1)S(1)}, bf16[784,128]{1,0:T(8,128)(2,1)S(1)}, u32[]{:S(2)}, u32[]{:S(2)}) collective-permute-start(bf16[784,128]{1,0:T(8,128)(2,1)S(1)} %collective-permute-done.2.refs_1_), channel_id=1, source_target_pairs={{0,1},{1,0},{2,3},{3,2},{4,5},{5,4},{6,7},{7,6},{8,9},{9,8},{10,11... | collective-permute-start | bytes 602120 | tf_op jit(solution)/shard_map/ppermute | solution.py:27
  55.2 2.3 %collective-permute-done.8.refs_7_ = bf16[784,128]{1,0:T(8,128)(2,1)S(1)} collective-permute-done((bf16[784,128]{1,0:T(8,128)(2,1)}, bf16[784,128]{1,0:T(8,128)(2,1)S(1)}, u32[]{:S(2)}, u32[]{:S(2)}) %collective-permute-start.8) | collective-permute-done | bytes 200736 | tf_op jit(solution)/shard_map/ppermute | solution.py:43
  58.7 2.0 %fusion.shared_ref = bf16[128,512]{1,0:T(8,128)(2,1)S(1)} fusion(bf16[128,2048]{1,0:T(8,128)(2,1)S(1)} %copy-done.9, bf16[2048,512]{1,0:T(8,128)(2,1)} %param.26, f32[128,512]{1,0:T(8,128)S(1)} %fusion.1), kind=kOutput, calls=%fused_computation.1 | convolution fusion | flops 268763136 | bytes 3014656 | tf_op jit(solution)/shard_map/dot_general | solution.py:784
  62.2 1.6 %copy-done.4 = bf16[1,512,2048]{2,1,0:T(8,128)(2,1)S(1)} copy-done((bf16[1,512,2048]{2,1,0:T(8,128)(2,1)S(1)}, bf16[1,512,2048]{2,1,0:T(8,128)(2,1)}, u32[]{:S(2)}) %copy-start.4) | copy-done | bytes 2097176
  63.8 4.0 %experts.1 = (bf16[2,512,512]{2,1,0:T(8,128)(2,1)S(1)}, bf16[2,512,512]{2,1,0:T(8,128)(2,1)}) custom-call(bf16[128,512]{1,0:T(8,128)(2,1)S(1)} %fusion.shared_ref, bf16[512,2048]{1,0:T(8,128)(2,1)S(1)} %copy-done.1, bf16[1,2048,512]{2,1,0:T(8,128)(2,1)S(1)} %copy-done.2, bf16[1,2048,512]{2,1,0:T(8,128)(2,1)S(1)} %copy-done.3, ...), custom_call_target="tpu_custom_call" | custom-call | flops 2684354560 | bytes 12582912 | tf_op jit(solution)/shard_map/experts/pallas_call | solution.py:709
  70.7 17.1 %stick.1 = bf16[8,256,128]{2,1,0:T(8,128)(2,1)} custom-call(s32[1,76]{1,0:T(1,128)} %constant.4.clone.table_ref, bf16[784,128]{1,0:T(8,128)(2,1)} %copy-done.10, bf16[784,128]{1,0:T(8,128)(2,1)} %copy-done.11, bf16[784,128]{1,0:T(8,128)(2,1)} %copy-done.12, bf16[784,128]{1,0:T(8,128)(2,1)} %copy-done.13, bf16[784,128]{1,0:T(8,128)(2,1)} %copy-done.14, ...), custom_call_target="tpu_custom_call" | custom-call | flops 6039797760 | bytes 2621440 | tf_op jit(solution)/shard_map/stick/pallas_call | solution.py:209
  87.8 3.5 %all-to-all-start = ((bf16[8,256,128]{2,1,0:T(8,128)(2,1)}), bf16[8,256,128]{2,1,0:T(8,128)(2,1)S(1)}, u32[]{:S(2)}, u32[]{:S(2)}) async-start(bf16[8,256,128]{2,1,0:T(8,128)(2,1)} %stick.1), calls=%async_computation | async-start | bytes 1048576 | tf_op jit(solution)/shard_map/all_to_all | solution.py:345
  91.3 2.9 %near.1 = (f32[512,512]{1,0:T(8,128)}, bf16[512,512]{1,0:T(8,128)(2,1)}) custom-call(bf16[2,512,512]{2,1,0:T(8,128)(2,1)} %copy-done.6, bf16[2,512,512]{2,1,0:T(8,128)(2,1)} %collective-permute-done.23.got_ref), custom_call_target="tpu_custom_call" | custom-call | flops 1048576 | bytes 3145728 | tf_op jit(solution)/shard_map/near/pallas_call | solution.py:603
  95.8 12.6 %collective-permute-done.24.got_ref = bf16[512,512]{1,0:T(8,128)(2,1)S(1)} collective-permute-done((bf16[512,512]{1,0:T(8,128)(2,1)}, bf16[512,512]{1,0:T(8,128)(2,1)S(1)}, u32[]{:S(2)}, u32[]{:S(2)}) %collective-permute-start.24) | collective-permute-done | bytes 524320 | tf_op jit(solution)/shard_map/ppermute | solution.py:27
  110.4 5.6 %all-to-all-start.2 = ((bf16[8,48,512]{2,1,0:T(8,128)(2,1)}), bf16[8,48,512]{2,1,0:T(8,128)(2,1)S(1)}, u32[]{:S(2)}, u32[]{:S(2)}) async-start(bf16[8,48,512]{2,1,0:T(8,128)(2,1)} %bitcast.5), calls=%async_computation.2 | async-start | bytes 786432 | tf_op jit(solution)/shard_map/all_to_all | solution.py:790
  116.0 2.2 %project.3 = (bf16[256,512]{1,0:T(8,128)(2,1)S(1)}, bf16[256,512]{1,0:T(8,128)(2,1)S(1)}) custom-call(bf16[512,2048]{1,0:T(8,128)(2,1)} %own_ref.3, bf16[512,2048]{1,0:T(8,128)(2,1)} %collective-permute-done.other_ref, bf16[8,256,128]{2,1,0:T(8,128)(2,1)S(1)} %all-to-all-done.refs_0_), custom_call_target="tpu_custom_call" | custom-call | flops 536870912 | bytes 6291456 | tf_op jit(solution)/shard_map/project/pallas_call | solution.py:278
  119.8 2.2 %project.2 = (bf16[256,512]{1,0:T(8,128)(2,1)S(1)}, bf16[256,512]{1,0:T(8,128)(2,1)S(1)}) custom-call(bf16[512,2048]{1,0:T(8,128)(2,1)} %own_ref.3, bf16[512,2048]{1,0:T(8,128)(2,1)} %collective-permute-done.other_ref, bf16[8,256,128]{2,1,0:T(8,128)(2,1)S(1)} %all-to-all-done.refs_0_), custom_call_target="tpu_custom_call" | custom-call | flops 536870912 | bytes 6291456 | tf_op jit(solution)/shard_map/project/pallas_call | solution.py:278
  122.7 4.8 %collective-permute-done.18.refs_2_ = bf16[256,512]{1,0:T(8,128)(2,1)S(1)} collective-permute-done((bf16[256,512]{1,0:T(8,128)(2,1)S(1)}, bf16[256,512]{1,0:T(8,128)(2,1)S(1)}, u32[]{:S(2)}, u32[]{:S(2)}) %collective-permute-start.18) | collective-permute-done | bytes 262176 | tf_op jit(solution)/shard_map/ppermute | solution.py:27
  127.5 2.3 %collective-permute-done.19.refs_3_ = bf16[256,512]{1,0:T(8,128)(2,1)S(1)} collective-permute-done((bf16[256,512]{1,0:T(8,128)(2,1)S(1)}, bf16[256,512]{1,0:T(8,128)(2,1)S(1)}, u32[]{:S(2)}, u32[]{:S(2)}) %collective-permute-start.19) | collective-permute-done | bytes 262176 | tf_op jit(solution)/shard_map/ppermute | solution.py:27
  (96 shorter events, 20.3 us)
Async XLA Ops:
  3.1 23.4 %all-to-all-start.1 = ((bf16[8,48,512]{2,1,0:T(8,128)(2,1)}), bf16[8,48,512]{2,1,0:T(8,128)(2,1)S(1)}, u32[]{:S(2)}, u32[]{:S(2)}) async-start(bf16[8,48,512]{2,1,0:T(8,128)(2,1)} %bitcast.17), calls=%async_computation.1 | async-start | bytes 786432 | tf_op jit(solution)/shard_map/all_to_all | solution.py:780
  13.1 17.6 %collective-permute-start.1 = (bf16[784,128]{1,0:T(8,128)(2,1)}, bf16[784,128]{1,0:T(8,128)(2,1)S(1)}, u32[]{:S(2)}, u32[]{:S(2)}) collective-permute-start(bf16[784,128]{1,0:T(8,128)(2,1)} %get-tuple-element.23), channel_id=1, source_target_pairs={{0,0},{1,16},{2,2},{3,18},{4,4},{5,20},{6,6},{7,22},{8,8},{9,24},{... | collective-permute-start | bytes 602120 | tf_op jit(solution)/shard_map/ppermute | solution.py:43
  14.7 16.1 %collective-permute-start.2 = (bf16[784,128]{1,0:T(8,128)(2,1)}, bf16[784,128]{1,0:T(8,128)(2,1)S(1)}, u32[]{:S(2)}, u32[]{:S(2)}) collective-permute-start(bf16[784,128]{1,0:T(8,128)(2,1)} %get-tuple-element.24), channel_id=1, source_target_pairs={{0,1},{1,17},{2,3},{3,19},{4,5},{5,21},{6,7},{7,23},{8,9},{9,25},{... | collective-permute-start | bytes 602120 | tf_op jit(solution)/shard_map/ppermute | solution.py:43
  26.5 21.4 %collective-permute-start.21 = (bf16[384,512]{1,0:T(8,128)(2,1)S(1)}, bf16[384,512]{1,0:T(8,128)(2,1)S(1)}, u32[]{:S(2)}, u32[]{:S(2)}) collective-permute-start(bf16[384,512]{1,0:T(8,128)(2,1)S(1)} %bitcast.12), channel_id=1, source_target_pairs={{0,2},{1,3},{2,0},{3,1},{4,6},{5,7},{6,4},{7,5},{8,10},{9,11},{10,... | collective-permute-start | bytes 1179656 | tf_op jit(solution)/shard_map/ppermute | solution.py:27
  28.0 9.2 %collective-permute-start.3 = (bf16[784,128]{1,0:T(8,128)(2,1)}, bf16[784,128]{1,0:T(8,128)(2,1)S(1)}, u32[]{:S(2)}, u32[]{:S(2)}) collective-permute-start(bf16[784,128]{1,0:T(8,128)(2,1)} %get-tuple-element.25), channel_id=1, source_target_pairs={{0,4},{1,20},{2,6},{3,22},{4,8},{5,24},{6,10},{7,26},{8,12},{9,28}... | collective-permute-start | bytes 602120 | tf_op jit(solution)/shard_map/ppermute | solution.py:43
  29.5 11.4 %collective-permute-start.4 = (bf16[784,128]{1,0:T(8,128)(2,1)}, bf16[784,128]{1,0:T(8,128)(2,1)S(1)}, u32[]{:S(2)}, u32[]{:S(2)}) collective-permute-start(bf16[784,128]{1,0:T(8,128)(2,1)} %get-tuple-element.26), channel_id=1, source_target_pairs={{0,5},{1,21},{2,7},{3,23},{4,9},{5,25},{6,11},{7,27},{8,13},{9,29}... | collective-permute-start | bytes 602120 | tf_op jit(solution)/shard_map/ppermute | solution.py:43
  30.8 10.2 %collective-permute-start.5 = (bf16[784,128]{1,0:T(8,128)(2,1)}, bf16[784,128]{1,0:T(8,128)(2,1)S(1)}, u32[]{:S(2)}, u32[]{:S(2)}) collective-permute-start(bf16[784,128]{1,0:T(8,128)(2,1)} %get-tuple-element.27), channel_id=1, source_target_pairs={{0,8},{1,24},{2,10},{3,26},{4,12},{5,28},{6,14},{7,30},{8,0},{9,16... | collective-permute-start | bytes 602120 | tf_op jit(solution)/shard_map/ppermute | solution.py:43
  30.8 17.0 %collective-permute-start.6 = (bf16[784,128]{1,0:T(8,128)(2,1)}, bf16[784,128]{1,0:T(8,128)(2,1)S(1)}, u32[]{:S(2)}, u32[]{:S(2)}) collective-permute-start(bf16[784,128]{1,0:T(8,128)(2,1)} %get-tuple-element.28), channel_id=1, source_target_pairs={{0,9},{1,25},{2,11},{3,27},{4,13},{5,29},{6,15},{7,31},{8,1},{9,17... | collective-permute-start | bytes 602120 | tf_op jit(solution)/shard_map/ppermute | solution.py:43
  37.2 11.6 %collective-permute-start.7 = (bf16[784,128]{1,0:T(8,128)(2,1)}, bf16[784,128]{1,0:T(8,128)(2,1)S(1)}, u32[]{:S(2)}, u32[]{:S(2)}) collective-permute-start(bf16[784,128]{1,0:T(8,128)(2,1)} %get-tuple-element.29), channel_id=1, source_target_pairs={{0,12},{1,28},{2,14},{3,30},{4,0},{5,16},{6,2},{7,18},{8,4},{9,20}... | collective-permute-start | bytes 602120 | tf_op jit(solution)/shard_map/ppermute | solution.py:43
  40.9 16.6 %collective-permute-start.8 = (bf16[784,128]{1,0:T(8,128)(2,1)}, bf16[784,128]{1,0:T(8,128)(2,1)S(1)}, u32[]{:S(2)}, u32[]{:S(2)}) collective-permute-start(bf16[784,128]{1,0:T(8,128)(2,1)} %get-tuple-element.30), channel_id=1, source_target_pairs={{0,13},{1,29},{2,15},{3,31},{4,1},{5,17},{6,3},{7,19},{8,5},{9,21}... | collective-permute-start | bytes 602120 | tf_op jit(solution)/shard_map/ppermute | solution.py:43
  41.0 16.5 %collective-permute-start.9 = (bf16[784,128]{1,0:T(8,128)(2,1)S(1)}, bf16[784,128]{1,0:T(8,128)(2,1)S(1)}, u32[]{:S(2)}, u32[]{:S(2)}) collective-permute-start(bf16[784,128]{1,0:T(8,128)(2,1)S(1)} %collective-permute-done.1.refs_0_), channel_id=1, source_target_pairs={{0,1},{1,0},{2,3},{3,2},{4,5},{5,4},{6,7},{7,6},{8,9},{9,8},{10,11... | collective-permute-start | bytes 602120 | tf_op jit(solution)/shard_map/ppermute | solution.py:27
  47.8 13.7 %collective-permute-start.20 = (bf16[384,512]{1,0:T(8,128)(2,1)S(1)}, bf16[384,512]{1,0:T(8,128)(2,1)S(1)}, u32[]{:S(2)}, u32[]{:S(2)}) collective-permute-start(bf16[384,512]{1,0:T(8,128)(2,1)S(1)} %bitcast.13), channel_id=1, source_target_pairs={{0,1},{1,0},{2,3},{3,2},{4,5},{5,4},{6,7},{7,6},{8,9},{9,8},{10,11... | collective-permute-start | bytes 1179656 | tf_op jit(solution)/shard_map/ppermute | solution.py:27
  47.8 14.2 %collective-permute-start.22 = (bf16[384,512]{1,0:T(8,128)(2,1)S(1)}, bf16[384,512]{1,0:T(8,128)(2,1)S(1)}, u32[]{:S(2)}, u32[]{:S(2)}) collective-permute-start(bf16[384,512]{1,0:T(8,128)(2,1)S(1)} %collective-permute-done.21.refs_2_), channel_id=1, source_target_pairs={{0,1},{1,0},{2,3},{3,2},{4,5},{5,4},{6,7},{7,6},{8,9},{9,8},{10,11... | collective-permute-start | bytes 1179656 | tf_op jit(solution)/shard_map/ppermute | solution.py:27
  48.8 11.9 %collective-permute-start.10 = (bf16[784,128]{1,0:T(8,128)(2,1)S(1)}, bf16[784,128]{1,0:T(8,128)(2,1)S(1)}, u32[]{:S(2)}, u32[]{:S(2)}) collective-permute-start(bf16[784,128]{1,0:T(8,128)(2,1)S(1)} %collective-permute-done.2.refs_1_), channel_id=1, source_target_pairs={{0,1},{1,0},{2,3},{3,2},{4,5},{5,4},{6,7},{7,6},{8,9},{9,8},{10,11... | collective-permute-start | bytes 602120 | tf_op jit(solution)/shard_map/ppermute | solution.py:27
  60.8 55.2 %collective-permute-start = (bf16[512,2048]{1,0:T(8,128)(2,1)}, bf16[512,2048]{1,0:T(8,128)(2,1)}, u32[]{:S(2)}, u32[]{:S(2)}) collective-permute-start(bf16[512,2048]{1,0:T(8,128)(2,1)} %own_ref.3), channel_id=1, source_target_pairs={{0,1},{1,0},{2,3},{3,2},{4,5},{5,4},{6,7},{7,6},{8,9},{9,8},{10,11... | collective-permute-start | bytes 6291464 | tf_op jit(solution)/shard_map/ppermute | solution.py:27
  60.9 7.8 %collective-permute-start.13 = (bf16[784,128]{1,0:T(8,128)(2,1)S(1)}, bf16[784,128]{1,0:T(8,128)(2,1)S(1)}, u32[]{:S(2)}, u32[]{:S(2)}) collective-permute-start(bf16[784,128]{1,0:T(8,128)(2,1)S(1)} %collective-permute-done.5.refs_4_), channel_id=1, source_target_pairs={{0,1},{1,0},{2,3},{3,2},{4,5},{5,4},{6,7},{7,6},{8,9},{9,8},{10,11... | collective-permute-start | bytes 602120 | tf_op jit(solution)/shard_map/ppermute | solution.py:27
  61.4 7.8 %collective-permute-start.14 = (bf16[784,128]{1,0:T(8,128)(2,1)S(1)}, bf16[784,128]{1,0:T(8,128)(2,1)S(1)}, u32[]{:S(2)}, u32[]{:S(2)}) collective-permute-start(bf16[784,128]{1,0:T(8,128)(2,1)S(1)} %collective-permute-done.6.refs_5_), channel_id=1, source_target_pairs={{0,1},{1,0},{2,3},{3,2},{4,5},{5,4},{6,7},{7,6},{8,9},{9,8},{10,11... | collective-permute-start | bytes 602120 | tf_op jit(solution)/shard_map/ppermute | solution.py:27
  68.8 22.6 %collective-permute-start.23 = (bf16[2,512,512]{2,1,0:T(8,128)(2,1)}, bf16[2,512,512]{2,1,0:T(8,128)(2,1)}, u32[]{:S(2)}, u32[]{:S(2)}) collective-permute-start(bf16[2,512,512]{2,1,0:T(8,128)(2,1)} %get-tuple-element.38), channel_id=1, source_target_pairs={{0,1},{1,0},{2,3},{3,2},{4,5},{5,4},{6,7},{7,6},{8,9},{9,8},{10,11... | collective-permute-start | bytes 3145736 | tf_op jit(solution)/shard_map/ppermute | solution.py:27
  87.8 22.6 %all-to-all-start = ((bf16[8,256,128]{2,1,0:T(8,128)(2,1)}), bf16[8,256,128]{2,1,0:T(8,128)(2,1)S(1)}, u32[]{:S(2)}, u32[]{:S(2)}) async-start(bf16[8,256,128]{2,1,0:T(8,128)(2,1)} %stick.1), calls=%async_computation | async-start | bytes 1048576 | tf_op jit(solution)/shard_map/all_to_all | solution.py:345
  94.2 14.1 %collective-permute-start.24 = (bf16[512,512]{1,0:T(8,128)(2,1)}, bf16[512,512]{1,0:T(8,128)(2,1)S(1)}, u32[]{:S(2)}, u32[]{:S(2)}) collective-permute-start(bf16[512,512]{1,0:T(8,128)(2,1)} %get-tuple-element.40), channel_id=1, source_target_pairs={{0,2},{1,3},{2,0},{3,1},{4,6},{5,7},{6,4},{7,5},{8,10},{9,11},{10,... | collective-permute-start | bytes 1572872 | tf_op jit(solution)/shard_map/ppermute | solution.py:27
  110.4 20.3 %all-to-all-start.2 = ((bf16[8,48,512]{2,1,0:T(8,128)(2,1)}), bf16[8,48,512]{2,1,0:T(8,128)(2,1)S(1)}, u32[]{:S(2)}, u32[]{:S(2)}) async-start(bf16[8,48,512]{2,1,0:T(8,128)(2,1)} %bitcast.5), calls=%async_computation.2 | async-start | bytes 786432 | tf_op jit(solution)/shard_map/all_to_all | solution.py:790
  118.2 9.2 %collective-permute-start.18 = (bf16[256,512]{1,0:T(8,128)(2,1)S(1)}, bf16[256,512]{1,0:T(8,128)(2,1)S(1)}, u32[]{:S(2)}, u32[]{:S(2)}) collective-permute-start(bf16[256,512]{1,0:T(8,128)(2,1)S(1)} %get-tuple-element.33), channel_id=1, source_target_pairs={{0,2},{1,3},{2,0},{3,1},{4,6},{5,7},{6,4},{7,5},{8,10},{9,11},{10,... | collective-permute-start | bytes 786440 | tf_op jit(solution)/shard_map/ppermute | solution.py:27
  119.8 10.0 %collective-permute-start.19 = (bf16[256,512]{1,0:T(8,128)(2,1)S(1)}, bf16[256,512]{1,0:T(8,128)(2,1)S(1)}, u32[]{:S(2)}, u32[]{:S(2)}) collective-permute-start(bf16[256,512]{1,0:T(8,128)(2,1)S(1)} %get-tuple-element.34), channel_id=1, source_target_pairs={{0,3},{1,2},{2,1},{3,0},{4,7},{5,6},{6,5},{7,4},{8,11},{9,10},{10,... | collective-permute-start | bytes 786440 | tf_op jit(solution)/shard_map/ppermute | solution.py:27
  122.0 7.8 %collective-permute-start.17 = (bf16[256,512]{1,0:T(8,128)(2,1)S(1)}, bf16[256,512]{1,0:T(8,128)(2,1)S(1)}, u32[]{:S(2)}, u32[]{:S(2)}) collective-permute-start(bf16[256,512]{1,0:T(8,128)(2,1)S(1)} %get-tuple-element.32), channel_id=1, source_target_pairs={{0,1},{1,0},{2,3},{3,2},{4,5},{5,4},{6,7},{7,6},{8,9},{9,8},{10,11... | collective-permute-start | bytes 786440 | tf_op jit(solution)/shard_map/ppermute | solution.py:27
  (30 other events, 353.7 us)
